TPU v7x, 128 devices: a whole 4x4x4 slice. The times are simulated.
128 devices in a mesh: dp: 4 (over x), kv: 16 (over z, y), tp: 2 (over core).
Axes of the slice: x: 4, y: 4, z: 4, core: 2. Of those that a mesh axis runs over, the one named last changes fastest.
Arguments:
- tokens: bfloat16 [512, 2048], P('dp', 'kv'), may hold values from -18 to 18
- mix_gain: float32 [2048], P('kv'), may hold values from 0.1 to 1.9
- w_query: bfloat16 [2048, 1024], P('kv', 'tp'), may hold values from -0.125 to 0.125
- w_key: bfloat16 [2048, 1024], P('kv', 'tp'), may hold values from -0.125 to 0.125
- w_value: bfloat16 [2048, 2048], P('kv', 'tp'), may hold values from -0.125 to 0.125
- w_outgate: bfloat16 [2048, 2048], P('kv', 'tp'), may hold values from -0.125 to 0.125
- w_gates: bfloat16 [2048, 16], replicated, may hold values from -0.25 to 0.25
- forget_bias: float32 [8], P('tp'), may hold values from -1 to 3
- memory: float32 [512, 8, 128, 256], P(('dp', 'kv'), 'tp'), may hold values from -4 to 4
- normalizer: float32 [512, 8, 128], P(('dp', 'kv'), 'tp'), may hold values from -4 to 4
- stabilizer: float32 [512, 8], P(('dp', 'kv'), 'tp'), may hold values from -4 to 4
- head_gain: float32 [8, 256], P('tp'), may hold values from 0.1 to 1.9
- w_out: bfloat16 [2048, 2048], P('tp', 'kv'), may hold values from -0.125 to 0.125
- mlp_gain: float32 [2048], replicated, may hold values from 0.1 to 1.9
- w_gate: bfloat16 [2048, 5632], P(None, ('kv', 'tp')), may hold values from -0.125 to 0.125
- w_up: bfloat16 [2048, 5632], P(None, ('kv', 'tp')), may hold values from -0.125 to 0.125
- w_down: bfloat16 [5632, 2048], P(('kv', 'tp')), may hold values from -0.15625 to 0.15625
Outputs:
- mixed_out: bfloat16 [512, 2048], P('dp', ('kv', 'tp'))
- new_memory: float32 [512, 8, 128, 256], P(('dp', 'kv'), 'tp')
- new_normalizer: float32 [512, 8, 128], P(('dp', 'kv'), 'tp')
- new_stabilizer: float32 [512, 8], P(('dp', 'kv'), 'tp')
All inputs are finite; a program needn't handle non-finite values.
Results may differ from a plain program's by a relative error of at most 0.02.
Values may be sent and summed in bfloat16 or wider, within the bound.
No kernel may reach another device: no remote copies, remote signals or barrier semaphores. Data moves between devices by JAX's collectives and lax.ppermute only.
A program may use at most 64 MiB of HBM per device.

v0:
```python
import jax
import jax.numpy as jnp
from jax import lax
from jax.sharding import PartitionSpec as P

QK = 128
VD = 256


EPSILON = 1e-06


def cut_along(value, dim, devices):
    before, after = (value.shape[:dim], value.shape[dim + 1 :])
    return jnp.moveaxis(value.reshape(*before, devices, -1, *after), dim, 0)


def sum_at_owner(value, axis, dim):
    devices = lax.axis_size(axis)
    blocks = lax.all_to_all(cut_along(value, dim, devices), axis, 0, 0, tiled=True)
    return jnp.sum(blocks.astype(jnp.float32), axis=0)


def side_by_side(arrays, axis, dim, along):
    both = jnp.concatenate(arrays, axis=along)
    whole, at, gathered = (sum_at_owner(both, axis, dim), 0, [])
    for a in arrays:
        gathered.append(lax.slice_in_dim(whole, at, at + a.shape[along], axis=along))
        at += a.shape[along]
    return tuple(gathered)


def from_everyone(value, axis):
    devices = lax.axis_size(axis)
    return lax.all_to_all(
        jnp.broadcast_to(value[None], (devices, *value.shape)), axis, 0, 0, tiled=True
    )


def joined_along(blocks, dim):
    shape = list(blocks.shape[1:])
    shape[dim] *= blocks.shape[0]
    return jnp.moveaxis(blocks, 0, dim).reshape(shape)


def gathered_copies(value, axis, dim):
    blocks = from_everyone(value, axis)
    return joined_along(blocks, dim)


def over_copies(value, axis):
    everything = from_everyone(value, axis)
    return jnp.sum(everything.astype(jnp.float32), axis=0)


def front_half(
    query_sum,
    key_sum,
    gate_sum,
    square_sum,
    model_width,
    forget_bias,
    memory,
    normalizer,
    stabilizer,
):
    local_heads = forget_bias.shape[0]
    seq_rows = query_sum.shape[0]
    inverse = lax.rsqrt(square_sum / model_width + EPSILON)
    query_rows = (query_sum * inverse).astype(jnp.bfloat16)
    key_rows = (key_sum * (inverse * QK ** (-0.5))).astype(jnp.bfloat16)
    gate_pre = gate_sum * inverse
    input_pre = gate_pre[:, :local_heads]
    log_forget = jax.nn.log_sigmoid(gate_pre[:, local_heads:] + forget_bias)
    new_stabilizer = jnp.maximum(log_forget + stabilizer, input_pre)
    forget_scale = jnp.exp(log_forget + stabilizer - new_stabilizer)
    input_scale = jnp.exp(input_pre - new_stabilizer)
    query_heads = query_rows.astype(jnp.float32).reshape(seq_rows, local_heads, QK)
    key_heads = key_rows.astype(jnp.float32).reshape(seq_rows, local_heads, QK)
    new_normalizer = forget_scale[..., None] * normalizer + input_scale[..., None] * key_heads
    denominator = jnp.sum(query_heads * new_normalizer, axis=2)
    carried = jnp.einsum("bhd,bhde->bhe", query_heads, memory)
    query_key = jnp.sum(query_heads * key_heads, axis=2)
    return (
        inverse,
        new_stabilizer,
        forget_scale,
        input_scale,
        key_heads,
        new_normalizer,
        denominator,
        carried,
        query_key,
    )


def back_half(value_sum, outgate_sum, front_state, memory, head_gain):
    (
        inverse,
        new_stabilizer,
        forget_scale,
        input_scale,
        key_heads,
        new_normalizer,
        denominator,
        carried,
        query_key,
    ) = front_state
    seq_rows, local_heads = forget_scale.shape
    value_rows = (value_sum * inverse).astype(jnp.bfloat16)
    outgate = (outgate_sum * inverse).astype(jnp.bfloat16)
    value_heads = value_rows.astype(jnp.float32).reshape(seq_rows, local_heads, VD)
    new_memory = (
        forget_scale[..., None, None] * memory
        + (input_scale[..., None] * key_heads)[..., None] * value_heads[:, :, None, :]
    )
    numerator = (
        forget_scale[..., None] * carried + (input_scale * query_key)[..., None] * value_heads
    )
    head_out = numerator / jnp.maximum(jnp.abs(denominator), 1.0)[..., None]
    normed = (
        head_out
        * lax.rsqrt(jnp.mean(head_out * head_out, axis=2, keepdims=True) + EPSILON)
        * head_gain
    )
    mixed_heads = (
        normed.reshape(seq_rows, local_heads * VD) * jax.nn.sigmoid(outgate.astype(jnp.float32))
    ).astype(jnp.bfloat16)
    return (new_memory, mixed_heads)


def body(
    tokens,
    mix_gain,
    w_query,
    w_key,
    w_value,
    w_outgate,
    w_gates,
    forget_bias,
    memory,
    normalizer,
    stabilizer,
    head_gain,
    w_out,
    mlp_gain,
    w_gate,
    w_up,
    w_down,
):
    activations = tokens.astype(jnp.float32)
    block_cols = tokens.shape[1]
    model_width = block_cols * lax.axis_size("kv")
    square_part = jnp.sum(activations * activations, axis=1, keepdims=True)
    scaled = (activations * mix_gain).astype(jnp.bfloat16)
    local_heads = forget_bias.shape[0]
    total_heads = w_gates.shape[1] // 2
    head_start = lax.axis_index("tp") * local_heads
    gate_rows = lax.dynamic_slice_in_dim(w_gates, lax.axis_index("kv") * block_cols, block_cols, 0)
    gate_cols = jnp.concatenate(
        [
            lax.dynamic_slice_in_dim(gate_rows, head_start, local_heads, 1),
            lax.dynamic_slice_in_dim(gate_rows, total_heads + head_start, local_heads, 1),
        ],
        axis=1,
    )
    query_part = jnp.dot(scaled, w_query, preferred_element_type=jnp.float32)
    key_part = jnp.dot(scaled, w_key, preferred_element_type=jnp.float32)
    value_part = jnp.dot(scaled, w_value, preferred_element_type=jnp.float32)
    outgate_part = jnp.dot(scaled, w_outgate, preferred_element_type=jnp.float32)
    gate_part = jnp.dot(scaled, gate_cols, preferred_element_type=jnp.float32)
    query_sum, key_sum, value_sum, outgate_sum, gate_sum, square_sum = side_by_side(
        (
            query_part.astype(jnp.bfloat16),
            key_part.astype(jnp.bfloat16),
            value_part.astype(jnp.bfloat16),
            outgate_part.astype(jnp.bfloat16),
            gate_part.astype(jnp.bfloat16),
            square_part.astype(jnp.bfloat16),
        ),
        "kv",
        0,
        1,
    )
    front_state = front_half(
        query_sum,
        key_sum,
        gate_sum,
        square_sum,
        model_width,
        forget_bias,
        memory,
        normalizer,
        stabilizer,
    )
    new_memory, mixed_heads = back_half(value_sum, outgate_sum, front_state, memory, head_gain)
    new_stabilizer = front_state[1]
    new_normalizer = front_state[5]
    branch_part = jnp.dot(
        gathered_copies(mixed_heads, "kv", 0), w_out, preferred_element_type=jnp.float32
    )
    branch = over_copies(branch_part.astype(jnp.bfloat16), "tp").astype(jnp.float32)
    residual = (activations + branch).astype(jnp.bfloat16)
    gathered = gathered_copies(residual, "kv", 1)
    gathered_float = gathered.astype(jnp.float32)
    inverse_two = lax.rsqrt(
        jnp.mean(gathered_float * gathered_float, axis=1, keepdims=True) + EPSILON
    )
    mlp_in = (gathered_float * inverse_two * mlp_gain).astype(jnp.bfloat16)
    gate_value = jnp.dot(mlp_in, w_gate, preferred_element_type=jnp.float32)
    up_value = jnp.dot(mlp_in, w_up, preferred_element_type=jnp.float32)
    hidden = (jax.nn.silu(gate_value) * up_value).astype(jnp.bfloat16)
    down_part = jnp.dot(hidden, w_down, preferred_element_type=jnp.float32)
    out_cols = block_cols // lax.axis_size("tp")
    own_residual = lax.dynamic_slice_in_dim(
        residual.astype(jnp.float32), lax.axis_index("tp") * out_cols, out_cols, 1
    )
    summed = sum_at_owner(down_part.astype(jnp.bfloat16), ("kv", "tp"), 1)
    mixed_out = (summed + own_residual).astype(jnp.bfloat16)
    return (mixed_out, new_memory, new_normalizer, new_stabilizer)


def solution(mesh):
    in_specs = (
        P("dp", "kv"),
        P("kv"),
        P("kv", "tp"),
        P("kv", "tp"),
        P("kv", "tp"),
        P("kv", "tp"),
        P(),
        P("tp"),
        P(("dp", "kv"), "tp", None, None),
        P(("dp", "kv"), "tp", None),
        P(("dp", "kv"), "tp"),
        P("tp", None),
        P("tp", "kv"),
        P(),
        P(None, ("kv", "tp")),
        P(None, ("kv", "tp")),
        P(("kv", "tp"), None),
    )
    out_specs = (
        P("dp", ("kv", "tp")),
        P(("dp", "kv"), "tp", None, None),
        P(("dp", "kv"), "tp", None),
        P(("dp", "kv"), "tp"),
    )
    return jax.shard_map(body, mesh=mesh, in_specs=in_specs, out_specs=out_specs, check_vma=False)
```

profile of v0, /device:TPU:1, one launch (start us, length us, event | category | flops | bytes accessed | tf_op | source)
XLA Modules:
  0.0 87.8 jit_solution(3687271985800106806)
XLA Ops:
  0.7 0.9 %fusion.14 = bf16[128]{0:T(256)(128)(2,1)S(1)} fusion(bf16[128,128]{1,0:T(8,128)(2,1)} %param.17), kind=kLoop, calls=%fused_computation.31 | loop fusion | flops 49024 | bytes 33024 | tf_op jit(solution)/shard_map/reduce_sum | solution.py:154
  1.6 0.9 fusion.46
  2.5 0.9 %convolution_convert_fusion.6 = bf16[128,8]{0,1:T(8,128)(2,1)S(1)} fusion(bf16[128,128]{1,0:T(8,128)(2,1)} %param.17, f32[128]{0:T(128)} %param.18, bf16[128,4]{0,1:T(4,128)(2,1)S(1)} %get-tuple-element.32, bf16[128,4]{0,1:T(4,128)(2,1)S(1)} %get-tuple-element.31), kind=kOutput, calls=%fused_computation.14 | convolution fusion | flops 316416 | bytes 37376 | tf_op jit(solution)/shard_map/dot_general | solution.py:171
  3.7 1.1 %fusion.2 = bf16[16,8,512]{2,1,0:T(8,128)(2,1)S(1)} fusion(bf16[128,512]{1,0:T(8,128)(2,1)} %param.19, bf16[128,128]{1,0:T(8,128)(2,1)} %param.17, f32[128]{0:T(128)} %param.18), kind=kOutput, calls=%fused_computation.9 | convolution fusion | flops 16891904 | bytes 295424 | tf_op jit(solution)/shard_map/dot_general | solution.py:167
  4.9 1.1 %fusion.3 = bf16[16,8,512]{2,1,0:T(8,128)(2,1)S(1)} fusion(bf16[128,512]{1,0:T(8,128)(2,1)} %param.20, bf16[128,128]{1,0:T(8,128)(2,1)} %param.17, f32[128]{0:T(128)} %param.18), kind=kOutput, calls=%fused_computation.10 | convolution fusion | flops 16891904 | bytes 295424 | tf_op jit(solution)/shard_map/dot_general | solution.py:168
  6.0 1.2 %fusion = bf16[16,8,1024]{2,1,0:T(8,128)(2,1)S(1)} fusion(bf16[128,1024]{1,0:T(8,128)(2,1)} %param.21, bf16[128,128]{1,0:T(8,128)(2,1)} %param.17, f32[128]{0:T(128)} %param.18), kind=kOutput, calls=%fused_computation.5 | convolution fusion | flops 33734656 | bytes 557568 | tf_op jit(solution)/shard_map/dot_general | solution.py:169
  7.2 1.2 %fusion.1 = bf16[16,8,1024]{2,1,0:T(8,128)(2,1)S(1)} fusion(bf16[128,1024]{1,0:T(8,128)(2,1)} %param.22, bf16[128,128]{1,0:T(8,128)(2,1)} %param.17, f32[128]{0:T(128)} %param.18), kind=kOutput, calls=%fused_computation.6 | convolution fusion | flops 33734656 | bytes 557568 | tf_op jit(solution)/shard_map/dot_general | solution.py:170
  8.4 1.1 %concatenate.23 = bf16[16,8,3081]{2,1,0:T(8,128)(2,1)} concatenate(bf16[16,8,512]{2,1,0:T(8,128)(2,1)S(1)} %fusion.2, bf16[16,8,512]{2,1,0:T(8,128)(2,1)S(1)} %fusion.3, bf16[16,8,1024]{2,1,0:T(8,128)(2,1)S(1)} %fusion, bf16[16,8,1024]{2,1,0:T(8,128)(2,1)S(1)} %fusion.1, bf16[16,8,8]{2,1,0:T(8,128)(2,1)S(1)} %bitcast.60, bf16[16,8,1]{2,1,0:T(8,128)(2,1)S(1)} %convert_element_type.131), dimensions={2} | concatenate | bytes 1577472 | tf_op jit(solution)/shard_map/concatenate | solution.py:25
  9.5 8.7 %all-to-all-start = ((bf16[16,8,3081]{2,1,0:T(8,128)(2,1)}), bf16[16,8,3081]{2,1,0:T(8,128)(2,1)S(1)}, u32[]{:S(2)}, u32[]{:S(2)}) async-start(bf16[16,8,3081]{2,1,0:T(8,128)(2,1)} %concatenate.23), calls=%async_computation | async-start | bytes 1638400 | tf_op jit(solution)/shard_map/all_to_all | solution.py:20
  18.3 13.5 %all-to-all-done = bf16[16,8,3081]{2,1,0:T(8,128)(2,1)S(1)} async-done(((bf16[16,8,3081]{2,1,0:T(8,128)(2,1)}), bf16[16,8,3081]{2,1,0:T(8,128)(2,1)S(1)}, u32[]{:S(2)}, u32[]{:S(2)}) %all-to-all-start) | async-done | bytes 788768 | tf_op jit(solution)/shard_map/all_to_all | solution.py:20
  32.5 0.7 fusion.21
  33.4 2.6 %fusion.25 = f32[8,4,1,256]{3,2,1,0:T(1,128)S(1)} fusion(f32[8,4,128,256]{3,2,1,0:T(8,128)} %param.25, bf16[8,4,128,1]{2,0,1,3:T(8,128)(2,1)S(1)} %get-tuple-element.28), kind=kOutput, calls=%fused_computation.53 | convolution fusion | flops 2097152 | bytes 4235264 | tf_op jit(solution)/shard_map/bhd,bhde->bhe/dot_general | solution.py:82
  36.4 11.2 %all_to_all.25 = bf16[16,8,1024]{2,1,0:T(8,128)(2,1)S(1)} all-to-all(bf16[16,8,1024]{2,1,0:T(8,128)(2,1)S(1)} %broadcast_in_dim.6), channel_id=1, replica_groups=mesh['dp'=4,'kv'=16,'tp'=2] {'kv'}, dimensions={0} | all-to-all | bytes 524288 | tf_op jit(solution)/shard_map/all_to_all | solution.py:35
  47.9 5.8 %all_to_all.26 = bf16[2,128,128]{2,1,0:T(8,128)(2,1)S(1)} all-to-all(bf16[2,128,128]{2,1,0:T(8,128)(2,1)S(1)} %broadcast_in_dim.7), channel_id=1, replica_groups=mesh['dp'=4,'kv'=16,'tp'=2] {'tp'}, dimensions={0} | all-to-all | bytes 131072 | tf_op jit(solution)/shard_map/all_to_all | solution.py:35
  54.0 13.4 %all_to_all.27 = bf16[16,128,128]{1,2,0:T(8,128)(2,1)S(1)} all-to-all(bf16[16,128,128]{1,2,0:T(8,128)(2,1)S(1)} %broadcast_in_dim.8), channel_id=1, replica_groups=mesh['dp'=4,'kv'=16,'tp'=2] {'kv'}, dimensions={0} | all-to-all | bytes 1048576 | tf_op jit(solution)/shard_map/all_to_all | solution.py:35
  67.6 0.3 fusion.6
  68.0 0.3 fusion.47
  68.4 0.7 convolution_convert_fusion
  69.0 1.0 %copy.95 = bf16[128,2048]{0,1:T(8,128)(2,1)} copy(bf16[128,2048]{1,0:T(8,128)(2,1)S(1)} %convolution_convert_fusion) | data formatting | bytes 1048576 | tf_op jit(solution)/shard_map/convert_element_type | solution.py:218
  70.0 5.3 %all-to-all-start.4 = ((bf16[32,128,64]{1,2,0:T(8,128)(2,1)}), bf16[32,128,64]{1,2,0:T(8,128)(2,1)S(1)}, u32[]{:S(2)}, u32[]{:S(2)}) async-start(bf16[32,128,64]{1,2,0:T(8,128)(2,1)} %bitcast.16), calls=%async_computation.4 | async-start | bytes 1048576 | tf_op jit(solution)/shard_map/all_to_all | solution.py:20
  75.3 0.7 copy.99
  76.0 4.0 %multiply_add_fusion = f32[8,4,128,256]{3,2,1,0:T(8,128)} fusion(f32[8,4,128,256]{3,2,1,0:T(8,128)} %param.25, f32[8,4,256]{2,1,0:T(4,128)S(1)} %copy.97, f32[8,4,128]{2,1,0:T(4,128)S(1)} %get-tuple-element.25, f32[8,4]{1,0:T(8,128)S(1)} %get-tuple-element.26), kind=kLoop, calls=%fused_computation | loop fusion | flops 3145728 | bytes 8437888 | tf_op jit(solution)/shard_map/add | solution.py:114
  79.9 6.9 %all-to-all-done.4 = bf16[32,128,64]{1,2,0:T(8,128)(2,1)S(1)} async-done(((bf16[32,128,64]{1,2,0:T(8,128)(2,1)}), bf16[32,128,64]{1,2,0:T(8,128)(2,1)S(1)}, u32[]{:S(2)}, u32[]{:S(2)}) %all-to-all-start.4) | async-done | bytes 524320 | tf_op jit(solution)/shard_map/all_to_all | solution.py:20
  87.1 0.7 copy.98
  (52 shorter events, 2.8 us)
Async XLA Ops:
  0.6 67.7 %copy-start = (bf16[176,2048]{1,0:T(8,128)(2,1)S(1)}, bf16[176,2048]{1,0:T(8,128)(2,1)}, u32[]{:S(2)}) copy-start(bf16[176,2048]{1,0:T(8,128)(2,1)} %param.33) | copy-start | bytes 2162692
  0.6 17.6 %copy-start.8 = (f32[8,4]{0,1:T(4,128)S(1)}, f32[8,4]{0,1:T(4,128)}, u32[]{:S(2)}) copy-start(f32[8,4]{0,1:T(4,128)} %param.27) | copy-start | bytes 388
  0.7 31.6 %copy-start.9 = (f32[4]{0:T(128)S(1)}, f32[4]{0:T(128)}, u32[]{:S(2)}) copy-start(f32[4]{0:T(128)} %param.24) | copy-start | bytes 52
  0.7 31.8 %copy-start.5 = (f32[8,4,128]{2,1,0:T(4,128)S(1)}, f32[8,4,128]{2,1,0:T(4,128)}, u32[]{:S(2)}) copy-start(f32[8,4,128]{2,1,0:T(4,128)} %param.26) | copy-start | bytes 49156
  8.4 27.8 %copy-start.7 = (f32[4,256]{1,0:T(4,128)S(1)}, f32[4,256]{1,0:T(4,128)}, u32[]{:S(2)}) copy-start(f32[4,256]{1,0:T(4,128)} %param.28) | copy-start | bytes 12292
  9.5 38.2 %copy-start.4 = (bf16[1024,128]{1,0:T(8,128)(2,1)S(1)}, bf16[1024,128]{1,0:T(8,128)(2,1)}, u32[]{:S(2)}) copy-start(bf16[1024,128]{1,0:T(8,128)(2,1)} %param.29) | copy-start | bytes 786436
  9.5 44.2 %copy-start.1 = (bf16[128,128]{1,0:T(8,128)(2,1)S(1)}, bf16[128,128]{1,0:T(8,128)(2,1)}, u32[]{:S(2)}) copy-start(bf16[128,128]{1,0:T(8,128)(2,1)} %param.17) | copy-start | bytes 98308
  9.5 22.3 %all-to-all-start = ((bf16[16,8,3081]{2,1,0:T(8,128)(2,1)}), bf16[16,8,3081]{2,1,0:T(8,128)(2,1)S(1)}, u32[]{:S(2)}, u32[]{:S(2)}) async-start(bf16[16,8,3081]{2,1,0:T(8,128)(2,1)} %concatenate.23), calls=%async_computation | async-start | bytes 1638400 | tf_op jit(solution)/shard_map/all_to_all | solution.py:20
  33.4 34.3 %copy-start.6 = (f32[2048]{0:T(1024)S(1)}, f32[2048]{0:T(1024)}, u32[]{:S(2)}) copy-start(f32[2048]{0:T(1024)} %param.30) | copy-start | bytes 24580
  33.4 34.6 %copy-start.2 = (bf16[2048,176]{0,1:T(8,128)(2,1)S(1)}, bf16[2048,176]{0,1:T(8,128)(2,1)}, u32[]{:S(2)}) copy-start(bf16[2048,176]{0,1:T(8,128)(2,1)} %param.31) | copy-start | bytes 2162692
  36.0 32.3 %copy-start.3 = (bf16[2048,176]{0,1:T(8,128)(2,1)S(1)}, bf16[2048,176]{0,1:T(8,128)(2,1)}, u32[]{:S(2)}) copy-start(bf16[2048,176]{0,1:T(8,128)(2,1)} %param.32) | copy-start | bytes 2162692
  70.0 16.8 %all-to-all-start.4 = ((bf16[32,128,64]{1,2,0:T(8,128)(2,1)}), bf16[32,128,64]{1,2,0:T(8,128)(2,1)S(1)}, u32[]{:S(2)}, u32[]{:S(2)}) async-start(bf16[32,128,64]{1,2,0:T(8,128)(2,1)} %bitcast.16), calls=%async_computation.4 | async-start | bytes 1048576 | tf_op jit(solution)/shard_map/all_to_all | solution.py:20
where the time goes:
time: 88.4 us; the launch traced here: 87.8 us
  blocking collectives  30.4 us (34%)
  waiting for transfers between devices  20.4 us (23%)
  starting transfers between devices  14 us (16%)
  matrix products  9.37 us (11%)
  other arithmetic  7.4 us (8%)
  local copies, waits for them, and re-layouts  5.34 us (6%)
  between operations  0.91 us (1%)
    all_to_all x3, blocking collectives, from_everyone(): lax.all_to_all(jnp.broadcast_to(value[None], (devices, *value.shape)), ax...  30.4 us
    all_to_all x2, waiting for transfers between devices, sum_at_owner(): lax.all_to_all(cut_along(value, dim, devices), axis, 0, 0, tiled=True)  20.4 us
    all_to_all x2, starting transfers between devices, sum_at_owner(): lax.all_to_all(cut_along(value, dim, devices), axis, 0, 0, tiled=True)  14 us
    add x1, other arithmetic, back_half(): forget_scale[..., None, None] * memory  3.97 us
    dot_general x1, matrix products, front_half(): carried = jnp.einsum('bhd,bhde->bhe', query_heads, memory)  2.64 us
  transfers between devices with their start and end apart: 2, of which 2 were waited for; matrix products, arithmetic and copies ran while one was open for 5% of the time, Pallas kernels for 0%

commit v1 on v0

v1 whole, which is shorter than its diff:
```python
import jax
import jax.numpy as jnp
from jax import lax
from jax.experimental import pallas as pl
from jax.experimental.pallas import tpu as pltpu
from jax.sharding import PartitionSpec as P

QK = 128
VD = 256
EPSILON = 1e-06
LANES = 128
F32 = jnp.float32
BF16 = jnp.bfloat16
NT = (((1,), (1,)), ((), ()))
VMEM = pltpu.MemorySpace.VMEM
SMEM = pltpu.MemorySpace.SMEM
HBM = pltpu.MemorySpace.HBM


def spec(space):
    return pl.BlockSpec(memory_space=space)


def project_kernel(tokens, gain, wq, wk, wv, wo, wg, out, bq, bk, bv, bo, bg, sems):
    copies = []
    cols = tokens.shape[1]
    kv = lax.axis_index("kv")
    gate_src = wg.at[:, pl.ds(pl.multiple_of(kv * cols, LANES), cols)]
    for n, (src, dst) in enumerate(((wq, bq), (wk, bk), (gate_src, bg), (wv, bv), (wo, bo))):
        copy = pltpu.make_async_copy(src, dst, sems.at[n])
        copy.start()
        copies.append(copy)
    blocks, rows = out.shape[:2]
    act = tokens[...].astype(F32)
    square = jnp.sum(act * act, axis=1, keepdims=True)
    scaled = (act * gain[...]).astype(BF16)

    def put(value, at):
        width = value.shape[1]
        out[:, :, at : at + width] = value.reshape(blocks, rows, width).astype(BF16)

    at = 0
    for n, buf in ((0, bq), (1, bk)):
        copies[n].wait()
        put(jnp.dot(scaled, buf[...], preferred_element_type=F32), at)
        at += buf.shape[1]
    copies[2].wait()
    gate_count = bg.shape[0]
    wide = jnp.concatenate([bg[...].astype(F32), jnp.zeros((LANES - gate_count, cols), F32)], axis=0)
    gates = lax.dot_general(scaled, wide.astype(BF16), NT, preferred_element_type=F32)
    lane = lax.broadcasted_iota(jnp.int32, gates.shape, 1)
    gates = jnp.where(lane == gate_count, square, gates)
    for n, buf in ((3, bv), (4, bo)):
        copies[n].wait()
        put(jnp.dot(scaled, buf[...], preferred_element_type=F32), at)
        at += buf.shape[1]
    put(gates, at)


def project(tokens, mix_gain, w_query, w_key, w_value, w_outgate, w_gates, blocks):
    rows, cols = tokens.shape
    width = w_query.shape[1] + w_key.shape[1] + w_value.shape[1] + w_outgate.shape[1] + LANES
    weights = (w_query, w_key, w_value, w_outgate)
    return pl.pallas_call(
        project_kernel,
        out_shape=jax.ShapeDtypeStruct((blocks, rows // blocks, width), BF16),
        in_specs=[spec(VMEM)] * 2 + [spec(HBM)] * 5,
        out_specs=spec(VMEM),
        scratch_shapes=[pltpu.VMEM(w.shape, BF16) for w in weights]
        + [pltpu.VMEM((w_gates.shape[1], cols), BF16), pltpu.SemaphoreType.DMA((5,))],
        name="project",
    )(tokens, mix_gain[None], *weights, w_gates.T)


def state_kernel(
    recv, bias, memory, normalizer, stab, gain,
    heads, norm_out, stab_out, forget_out, key_out, value_out,
    mem, sems, *, model_width, total_heads,
):
    seqs, local = memory.shape[0], memory.shape[1]
    copies = []
    for h in range(local):
        copy = pltpu.make_async_copy(memory.at[:, h], mem.at[h], sems.at[h])
        copy.start()
        copies.append(copy)
    tp = lax.axis_index("tp")
    qw, vw = local * QK, local * VD

    def summed(lo, width):
        return jnp.sum(recv[:, :, lo : lo + width].astype(F32), axis=0)

    small = summed(2 * qw + 2 * vw, LANES)
    inverse = lax.rsqrt(small[:, 2 * total_heads : 2 * total_heads + 1] / model_width + EPSILON)
    query = (summed(0, qw) * inverse).astype(BF16).astype(F32)
    key = (summed(qw, qw) * (inverse * QK ** (-0.5))).astype(BF16).astype(F32)
    value = (summed(2 * qw, vw) * inverse).astype(BF16).astype(F32)
    outgate = (summed(2 * qw + vw, vw) * inverse).astype(BF16).astype(F32)
    row = lax.broadcasted_iota(jnp.int32, (seqs, QK), 0)
    diag = lax.broadcasted_iota(jnp.int32, (seqs, seqs), 0) == lax.broadcasted_iota(
        jnp.int32, (seqs, seqs), 1
    )

    def own(at, h):
        both = [small[:, at + t * local + h : at + t * local + h + 1] for t in range(total_heads // local)]
        got = both[0]
        for t in range(1, len(both)):
            got = jnp.where(tp == t, both[t], got)
        return got

    partial = []
    for h in range(local):
        input_pre = own(0, h) * inverse
        log_forget = jax.nn.log_sigmoid(own(total_heads, h) * inverse + bias[h])
        old = jnp.sum(jnp.where(diag, stab[h : h + 1, :], 0.0), axis=1, keepdims=True)
        new = jnp.maximum(log_forget + old, input_pre)
        forget = jnp.exp(log_forget + old - new)
        scale = jnp.exp(input_pre - new)
        stab_out[h : h + 1, :] = jnp.sum(jnp.where(diag, new, 0.0), axis=0, keepdims=True)
        q, k = query[:, h * QK : (h + 1) * QK], key[:, h * QK : (h + 1) * QK]
        scaled_key = scale * k
        new_norm = forget * normalizer[:, h, :] + scaled_key
        norm_out[:, h, :] = new_norm
        key_out[:, h, :] = scaled_key
        v = value[:, h * VD : (h + 1) * VD]
        value_out[:, h, :] = v
        forget_out[:, h, :] = jnp.broadcast_to(forget, (seqs, LANES))
        denom = jnp.maximum(jnp.abs(jnp.sum(q * new_norm, axis=1, keepdims=True)), 1.0)
        query_key = jnp.sum(q * k, axis=1, keepdims=True)
        spread = [jnp.where(row == b, q, 0.0).astype(BF16) for b in range(seqs)]
        partial.append((forget, (scale * query_key) * v, denom, spread))
    for h in range(local):
        forget, fresh, denom, spread = partial[h]
        copies[h].wait()
        carried = jnp.zeros((seqs, VD), F32)
        for b in range(0, seqs, 2):
            left = jnp.concatenate([spread[b], spread[b + 1]], axis=1)
            right = mem[h, b : b + 2].reshape(2 * QK, VD).astype(BF16)
            carried = carried + jnp.dot(left, right, preferred_element_type=F32)
        head_out = (forget * carried + fresh) / denom
        normed = head_out * lax.rsqrt(jnp.mean(head_out * head_out, axis=1, keepdims=True) + EPSILON)
        gate = jax.nn.sigmoid(outgate[:, h * VD : (h + 1) * VD])
        mixed = (normed * gain[h : h + 1, :] * gate).astype(BF16)
        heads[:, :, h * VD : (h + 1) * VD] = jnp.broadcast_to(mixed[None], (heads.shape[0], seqs, VD))


def state_step(recv, forget_bias, memory, normalizer, stabilizer, head_gain, model_width, total_heads):
    blocks = recv.shape[0]
    seqs, local = memory.shape[:2]

    def kernel(*refs):
        state_kernel(*refs, model_width=model_width, total_heads=total_heads)

    return pl.pallas_call(
        kernel,
        out_shape=(
            jax.ShapeDtypeStruct((blocks, seqs, local * VD), BF16),
            jax.ShapeDtypeStruct((seqs, local, QK), F32),
            jax.ShapeDtypeStruct((local, seqs), F32),
            jax.ShapeDtypeStruct((seqs, local, LANES), F32),
            jax.ShapeDtypeStruct((seqs, local, QK), F32),
            jax.ShapeDtypeStruct((seqs, local, VD), F32),
        ),
        in_specs=[spec(VMEM), spec(SMEM), spec(HBM), spec(VMEM), spec(VMEM), spec(VMEM)],
        out_specs=[spec(VMEM)] * 6,
        scratch_shapes=[
            pltpu.VMEM((local, seqs, QK, VD), F32),
            pltpu.SemaphoreType.DMA((local,)),
        ],
        name="state",
    )(recv, forget_bias, memory, normalizer, stabilizer.T, head_gain)


def mixer_kernel(rows_ref, gain, wg, wu, wd, keep, give, mlp):
    blocks, rows, cols = rows_ref.shape
    tp = lax.axis_index("tp")
    total = jnp.zeros((rows, cols), F32)
    for j in range(blocks):
        value = rows_ref[j].astype(F32)
        total = total + value * value
    inverse = lax.rsqrt(jnp.sum(total, axis=1, keepdims=True) / (blocks * cols) + EPSILON)
    for j in range(blocks):
        lo = j * cols
        value = rows_ref[j].astype(F32) * inverse * gain[:, lo : lo + cols]
        mlp[:, lo : lo + cols] = value.astype(BF16)
    gate = lax.dot_general(mlp[...], wg[...], NT, preferred_element_type=F32)
    up = lax.dot_general(mlp[...], wu[...], NT, preferred_element_type=F32)
    hidden = (jax.nn.silu(gate) * up).astype(BF16)
    half = keep.shape[1]
    for j in range(blocks):
        part = jnp.dot(hidden, wd[:, j * cols : (j + 1) * cols], preferred_element_type=F32).T
        first, second = part[:half].astype(BF16), part[half:].astype(BF16)
        keep[j] = jnp.where(tp == 0, first, second)
        give[j] = jnp.where(tp == 0, second, first)


def mixer(gathered, mlp_gain, w_gate, w_up, w_down):
    blocks, rows, cols = gathered.shape
    half = jax.ShapeDtypeStruct((blocks, cols // 2, rows), BF16)
    return pl.pallas_call(
        mixer_kernel,
        out_shape=(half, half),
        in_specs=[spec(VMEM)] * 5,
        out_specs=[spec(VMEM)] * 2,
        scratch_shapes=[pltpu.VMEM((rows, blocks * cols), BF16)],
        name="mixer",
    )(gathered, mlp_gain[None], w_gate.T, w_up.T, w_down)


def other_core(value):
    return lax.ppermute(value, "tp", [(0, 1), (1, 0)])


def exchanged(blocks):
    return lax.all_to_all(blocks, "kv", 0, 0, tiled=True)


def body(
    tokens,
    mix_gain,
    w_query,
    w_key,
    w_value,
    w_outgate,
    w_gates,
    forget_bias,
    memory,
    normalizer,
    stabilizer,
    head_gain,
    w_out,
    mlp_gain,
    w_gate,
    w_up,
    w_down,
):
    devices = lax.axis_size("kv")
    rows, block_cols = tokens.shape
    send = project(tokens, mix_gain, w_query, w_key, w_value, w_outgate, w_gates, devices)
    heads, new_normalizer, new_stabilizer, forget, scaled_key, value = state_step(
        exchanged(send),
        forget_bias,
        memory,
        normalizer,
        stabilizer,
        head_gain,
        block_cols * devices,
        w_gates.shape[1] // 2,
    )
    gathered_heads = exchanged(heads).reshape(rows, -1)
    branch = jnp.dot(gathered_heads, w_out, preferred_element_type=F32).astype(BF16)
    residual = (
        tokens.astype(F32) + (branch.astype(F32) + other_core(branch).astype(F32))
    ).astype(BF16)
    gathered = exchanged(jnp.broadcast_to(residual[None], (devices, *residual.shape)))
    keep, give = mixer(gathered, mlp_gain, w_gate, w_up, w_down)
    pair = (keep.astype(F32) + other_core(give).astype(F32)).astype(BF16)
    late_forget, late_key, late_value, _ = lax.optimization_barrier((forget, scaled_key, value, keep))
    new_memory = (
        late_forget[:, :, :1, None] * memory + late_key[..., None] * late_value[:, :, None, :]
    )
    summed = jnp.sum(exchanged(pair).astype(F32), axis=0)
    out_cols = block_cols // lax.axis_size("tp")
    own = lax.dynamic_slice_in_dim(residual, lax.axis_index("tp") * out_cols, out_cols, 1)
    mixed_out = (summed + own.T.astype(F32)).astype(BF16).T
    return (mixed_out, new_memory, new_normalizer, new_stabilizer.T)


def solution(mesh):
    in_specs = (
        P("dp", "kv"),
        P("kv"),
        P("kv", "tp"),
        P("kv", "tp"),
        P("kv", "tp"),
        P("kv", "tp"),
        P(),
        P("tp"),
        P(("dp", "kv"), "tp", None, None),
        P(("dp", "kv"), "tp", None),
        P(("dp", "kv"), "tp"),
        P("tp", None),
        P("tp", "kv"),
        P(),
        P(None, ("kv", "tp")),
        P(None, ("kv", "tp")),
        P(("kv", "tp"), None),
    )
    out_specs = (
        P("dp", ("kv", "tp")),
        P(("dp", "kv"), "tp", None, None),
        P(("dp", "kv"), "tp", None),
        P(("dp", "kv"), "tp"),
    )
    return jax.shard_map(body, mesh=mesh, in_specs=in_specs, out_specs=out_specs, check_vma=False)
```

time: 88.4 us -> 82.8 us (0.937)
  blocking collectives: 30.4 us -> 48.2 us
  waiting for transfers between devices: 20.4 us -> 6.3 us
  Pallas kernels: 0 us -> 11.8 us
  matrix products: 9.37 us -> 0.28 us
  starting transfers between devices: 14 us -> 7.87 us
  local copies, waits for them, and re-layouts: 5.34 us -> 0.54 us
  other arithmetic: 7.4 us -> 6.37 us
    all_to_all x3, blocking collectives: 30.4 us -> 48.2 us  [exchanged(): return lax.all_to_all(blocks, 'kv', 0, 0, tiled=True)]
    all_to_all x2 -> x1, waiting for transfers between devices: 20.4 us -> 4.38 us  [exchanged(): return lax.all_to_all(blocks, 'kv', 0, 0, tiled=True)]
    pallas_call x0 -> x3, Pallas kernels: none -> 11.8 us  [the longest x1 4.57 us: state_step(): pl.pallas_call(kernel, out_shape=(jax.ShapeDtypeStruct((blocks, seqs, loc...]
    all_to_all x2 -> x1, starting transfers between devices: 14 us -> 3.53 us  [exchanged(): return lax.all_to_all(blocks, 'kv', 0, 0, tiled=True)]
    dot_general x9 -> x1, matrix products: 9.37 us -> 0.28 us  [body(): jnp.dot(gathered_heads, w_out, preferred_element_type=F32).astype(BF16)]
    ppermute x0 -> x2, starting transfers between devices: none -> 4.34 us  [other_core(): return lax.ppermute(value, 'tp', [(0, 1), (1, 0)])]
    reduce_sum x7 -> x1, other arithmetic: 2.28 us -> 0.04 us  [body(): summed = jnp.sum(exchanged(pair).astype(F32), axis=0)]
    ppermute x0 -> x2, waiting for transfers between devices: none -> 1.92 us  [other_core(): return lax.ppermute(value, 'tp', [(0, 1), (1, 0)])]
  transfers between devices with their start and end apart: 2 -> 3, of which waited for: 2 -> 3; matrix products, arithmetic and copies ran while one was open for 5% -> 5% of each run, Pallas kernels for 0% -> 0%
where the time goes in v1:
time: 82.8 us; the launch traced here: 82.1 us
  blocking collectives  48.2 us (58%)
  Pallas kernels  11.8 us (14%)
  starting transfers between devices  7.87 us (10%)
  other arithmetic  6.37 us (8%)
  waiting for transfers between devices  6.3 us (8%)
    all_to_all x3, blocking collectives, exchanged(): return lax.all_to_all(blocks, 'kv', 0, 0, tiled=True)  48.2 us
    pallas_call x1, Pallas kernels, state_step(): pl.pallas_call(kernel, out_shape=(jax.ShapeDtypeStruct((blocks, seqs, loc...  4.57 us
    all_to_all x1, waiting for transfers between devices, exchanged(): return lax.all_to_all(blocks, 'kv', 0, 0, tiled=True)  4.38 us
    ppermute x2, starting transfers between devices, other_core(): return lax.ppermute(value, 'tp', [(0, 1), (1, 0)])  4.34 us
    add x1, other arithmetic, body(): late_forget[:, :, :1, None] * memory  3.97 us
    pallas_call x1, Pallas kernels, mixer(): pl.pallas_call(mixer_kernel, out_shape=(half, half), in_specs=[spec(VMEM)...  3.67 us
    pallas_call x1, Pallas kernels, project(): pl.pallas_call(project_kernel, out_shape=jax.ShapeDtypeStruct((blocks, ro...  3.57 us
    all_to_all x1, starting transfers between devices, exchanged(): return lax.all_to_all(blocks, 'kv', 0, 0, tiled=True)  3.53 us
  transfers between devices with their start and end apart: 3, of which 3 were waited for; matrix products, arithmetic and copies ran while one was open for 5% of the time, Pallas kernels for 0%

profile of v1, /device:TPU:1, one launch (start us, length us, event | category | flops | bytes accessed | tf_op | source)
XLA Modules:
  0.0 82.1 jit_solution(544833347044284373)
XLA Ops:
  0.6 0.0 copy-start
  0.6 3.6 %project.1 = bf16[16,8,3200]{2,1,0:T(8,128)(2,1)} custom-call(bf16[128,128]{1,0:T(8,128)(2,1)} %tokens.1, f32[1,128]{1,0:T(1,128)} %bitcast.24, bf16[128,512]{1,0:T(8,128)(2,1)} %wq.1, bf16[128,512]{1,0:T(8,128)(2,1)} %wk.1, bf16[128,1024]{1,0:T(8,128)(2,1)} %wv.1, bf16[128,1024]{1,0:T(8,128)(2,1)} %wo.1, bf16[16,2048]{1,0:T(8,128)(2,1)} %bitcast.19), custom_call_target="tpu_custom_call" | custom-call | tf_op jit(solution)/shard_map/project/pallas_call | solution.py:64
  4.2 0.0 copy-start.1
  4.2 22.6 %all_to_all.20.refs_0_ = bf16[16,8,3200]{2,1,0:T(8,128)(2,1)} all-to-all(bf16[16,8,3200]{2,1,0:T(8,128)(2,1)} %project.1), channel_id=1, replica_groups=mesh['dp'=4,'kv'=16,'tp'=2] {'kv'}, dimensions={0} | all-to-all | bytes 1638400 | tf_op jit(solution)/shard_map/all_to_all | solution.py:214
  26.8 4.6 %state.1 = (bf16[16,8,1024]{2,1,0:T(8,128)(2,1)}, f32[8,4,128]{2,1,0:T(4,128)}, f32[4,8]{1,0:T(4,128)}, f32[8,4,128]{2,1,0:T(4,128)}, f32[8,4,128]{2,1,0:T(4,128)}, /*index=5*/f32[8,4,256]{2,1,0:T(4,128)}) custom-call(bf16[16,8,3200]{2,1,0:T(8,128)(2,1)} %all_to_all.20.refs_0_, f32[4]{0:T(128)} %refs_1_.1, f32[8,4,128,256]{3,2,1,0:T(8,128)} %refs_2_.1, ...), custom_call_target="tpu_custom_call" | custom-call | tf_op jit(solution)/shard_map/state/pallas_call | solution.py:153
  31.4 0.0 copy-start.4
  31.4 11.3 %all_to_all.21 = bf16[16,8,1024]{2,1,0:T(8,128)(2,1)S(1)} all-to-all(bf16[16,8,1024]{2,1,0:T(8,128)(2,1)} %get-tuple-element.15), channel_id=1, replica_groups=mesh['dp'=4,'kv'=16,'tp'=2] {'kv'}, dimensions={0} | all-to-all | bytes 524288 | tf_op jit(solution)/shard_map/all_to_all | solution.py:214
  42.8 0.3 convolution_convert_fusion
  43.0 2.8 %collective-permute-start = (bf16[128,128]{0,1:T(8,128)(2,1)S(1)}, bf16[128,128]{0,1:T(8,128)(2,1)S(1)}, u32[]{:S(2)}, u32[]{:S(2)}) collective-permute-start(bf16[128,128]{0,1:T(8,128)(2,1)S(1)} %convolution_convert_fusion), channel_id=1, source_target_pairs={{0,1},{1,0},{2,3},{3,2},{4,5},{5,4},{6,7},{7,6},{8,9},{9,8},{10,11... | collective-permute-start | bytes 98312 | tf_op jit(solution)/shard_map/ppermute | solution.py:210
  45.9 0.1 copy.21
  46.0 0.7 collective-permute-done
  46.8 0.1 copy.22
  46.9 0.1 broadcast_in_dim.7
  47.0 14.3 %all_to_all.22.rows_ref = bf16[16,128,128]{2,1,0:T(8,128)(2,1)} all-to-all(bf16[16,128,128]{2,1,0:T(8,128)(2,1)S(1)} %broadcast_in_dim.7), channel_id=1, replica_groups=mesh['dp'=4,'kv'=16,'tp'=2] {'kv'}, dimensions={0} | all-to-all | bytes 1048576 | tf_op jit(solution)/shard_map/all_to_all | solution.py:214
  61.3 3.7 %mixer.1 = (bf16[16,64,128]{2,1,0:T(8,128)(2,1)}, bf16[16,64,128]{2,1,0:T(8,128)(2,1)}) custom-call(bf16[16,128,128]{2,1,0:T(8,128)(2,1)} %all_to_all.22.rows_ref, f32[1,2048]{1,0:T(1,128)} %bitcast.21, bf16[176,2048]{1,0:T(8,128)(2,1)} %bitcast.17, bf16[176,2048]{1,0:T(8,128)(2,1)} %bitcast.18, bf16[176,2048]{1,0:T(8,128)(2,1)} %wd.1), custom_call_target="tpu_custom_call" | custom-call | tf_op jit(solution)/shard_map/mixer/pallas_call | solution.py:199
  64.9 1.5 %collective-permute-start.1 = (bf16[16,64,128]{2,1,0:T(8,128)(2,1)}, bf16[16,64,128]{2,1,0:T(8,128)(2,1)S(1)}, u32[]{:S(2)}, u32[]{:S(2)}) collective-permute-start(bf16[16,64,128]{2,1,0:T(8,128)(2,1)} %get-tuple-element.17), channel_id=1, source_target_pairs={{0,1},{1,0},{2,3},{3,2},{4,5},{5,4},{6,7},{7,6},{8,9},{9,8},{10,11... | collective-permute-start | bytes 786440 | tf_op jit(solution)/shard_map/ppermute | solution.py:210
  66.4 0.1 copy.23
  66.5 0.1 copy.24
  66.6 1.2 %collective-permute-done.1 = bf16[16,64,128]{2,1,0:T(8,128)(2,1)S(1)} collective-permute-done((bf16[16,64,128]{2,1,0:T(8,128)(2,1)}, bf16[16,64,128]{2,1,0:T(8,128)(2,1)S(1)}, u32[]{:S(2)}, u32[]{:S(2)}) %collective-permute-start.1) | collective-permute-done | bytes 262176 | tf_op jit(solution)/shard_map/ppermute | solution.py:210
  67.8 1.7 %add_convert_fusion = bf16[16,64,128]{2,1,0:T(8,128)(2,1)} fusion(bf16[16,64,128]{2,1,0:T(8,128)(2,1)S(1)} %collective-permute-done.1, bf16[16,64,128]{2,1,0:T(8,128)(2,1)} %get-tuple-element.16), kind=kLoop, calls=%fused_computation.3 | loop fusion | flops 524288 | bytes 786432 | tf_op jit(solution)/shard_map/convert_element_type | solution.py:256
  69.5 3.5 %all-to-all-start.3 = ((bf16[16,64,128]{2,1,0:T(8,128)(2,1)}), bf16[16,64,128]{2,1,0:T(8,128)(2,1)S(1)}, u32[]{:S(2)}, u32[]{:S(2)}) async-start(bf16[16,64,128]{2,1,0:T(8,128)(2,1)} %add_convert_fusion), calls=%async_computation.3 | async-start | bytes 524288 | tf_op jit(solution)/shard_map/all_to_all | solution.py:214
  73.1 4.0 %multiply_add_fusion = f32[8,4,128,256]{3,2,1,0:T(8,128)} fusion(f32[8,4,128,256]{3,2,1,0:T(8,128)} %refs_2_.1, f32[8,4,256]{2,1,0:T(4,128)S(1)} %copy-done.2, f32[8,4,128]{2,1,0:T(4,128)S(1)} %copy-done.3, f32[8,4]{1,0:T(8,128)S(1)} %copy.24), kind=kLoop, calls=%fused_computation | loop fusion | flops 3145728 | bytes 8437888 | tf_op jit(solution)/shard_map/add | solution.py:259
  77.0 4.4 %all-to-all-done.3 = bf16[16,64,128]{2,1,0:T(8,128)(2,1)S(1)} async-done(((bf16[16,64,128]{2,1,0:T(8,128)(2,1)}), bf16[16,64,128]{2,1,0:T(8,128)(2,1)S(1)}, u32[]{:S(2)}, u32[]{:S(2)}) %all-to-all-start.3) | async-done | bytes 262176 | tf_op jit(solution)/shard_map/all_to_all | solution.py:214
  81.5 0.6 fusion.1
  (9 shorter events, 0.1 us)
Async XLA Ops:
  0.6 42.1 %copy-start = (bf16[1024,128]{1,0:T(8,128)(2,1)S(1)}, bf16[1024,128]{1,0:T(8,128)(2,1)}, u32[]{:S(2)}) copy-start(bf16[1024,128]{1,0:T(8,128)(2,1)} %param.29) | copy-start | bytes 786436
  4.2 41.7 %copy-start.1 = (bf16[128,128]{1,0:T(8,128)(2,1)S(1)}, bf16[128,128]{1,0:T(8,128)(2,1)}, u32[]{:S(2)}) copy-start(bf16[128,128]{1,0:T(8,128)(2,1)} %tokens.1) | copy-start | bytes 98308
  31.4 35.0 %copy-start.4 = (f32[8,4,128]{2,1,0:T(4,128)S(1)}, f32[8,4,128]{2,1,0:T(4,128)}, u32[]{:S(2)}) copy-start(f32[8,4,128]{2,1,0:T(4,128)} %get-tuple-element.21) | copy-start | bytes 49156
  31.4 41.6 %copy-start.2 = (f32[8,4,256]{2,1,0:T(4,128)S(1)}, f32[8,4,256]{2,1,0:T(4,128)}, u32[]{:S(2)}) copy-start(f32[8,4,256]{2,1,0:T(4,128)} %get-tuple-element.23) | copy-start | bytes 98308
  31.4 41.6 %copy-start.3 = (f32[8,4,128]{2,1,0:T(4,128)S(1)}, f32[8,4,128]{2,1,0:T(4,128)}, u32[]{:S(2)}) copy-start(f32[8,4,128]{2,1,0:T(4,128)} %get-tuple-element.22) | copy-start | bytes 49156
  43.0 3.7 %collective-permute-start = (bf16[128,128]{0,1:T(8,128)(2,1)S(1)}, bf16[128,128]{0,1:T(8,128)(2,1)S(1)}, u32[]{:S(2)}, u32[]{:S(2)}) collective-permute-start(bf16[128,128]{0,1:T(8,128)(2,1)S(1)} %convolution_convert_fusion), channel_id=1, source_target_pairs={{0,1},{1,0},{2,3},{3,2},{4,5},{5,4},{6,7},{7,6},{8,9},{9,8},{10,11... | collective-permute-start | bytes 98312 | tf_op jit(solution)/shard_map/ppermute | solution.py:210
  64.9 2.9 %collective-permute-start.1 = (bf16[16,64,128]{2,1,0:T(8,128)(2,1)}, bf16[16,64,128]{2,1,0:T(8,128)(2,1)S(1)}, u32[]{:S(2)}, u32[]{:S(2)}) collective-permute-start(bf16[16,64,128]{2,1,0:T(8,128)(2,1)} %get-tuple-element.17), channel_id=1, source_target_pairs={{0,1},{1,0},{2,3},{3,2},{4,5},{5,4},{6,7},{7,6},{8,9},{9,8},{10,11... | collective-permute-start | bytes 786440 | tf_op jit(solution)/shard_map/ppermute | solution.py:210
  69.5 11.9 %all-to-all-start.3 = ((bf16[16,64,128]{2,1,0:T(8,128)(2,1)}), bf16[16,64,128]{2,1,0:T(8,128)(2,1)S(1)}, u32[]{:S(2)}, u32[]{:S(2)}) async-start(bf16[16,64,128]{2,1,0:T(8,128)(2,1)} %add_convert_fusion), calls=%async_computation.3 | async-start | bytes 524288 | tf_op jit(solution)/shard_map/all_to_all | solution.py:214

commit v2 on v1

--- a/solution.py
+++ b/solution.py
@@ -21,40 +21,46 @@
     return pl.BlockSpec(memory_space=space)
 
 
-def project_kernel(tokens, gain, wq, wk, wv, wo, wg, out, bq, bk, bv, bo, bg, sems):
-    copies = []
+def stay(*arrays):
+    return [pltpu.with_memory_space_constraint(a, HBM) for a in arrays]
+
+
+def fetch(pairs, sems):
+    copies = [pltpu.make_async_copy(src, dst, sems.at[n]) for n, (src, dst) in enumerate(pairs)]
+    for copy in copies:
+        copy.start()
+    return copies
+
+
+def project_kernel(tokens, gain, wq, wk, wv, wo, wg, out, bt, bn, bq, bk, bv, bo, bg, sems):
     cols = tokens.shape[1]
     kv = lax.axis_index("kv")
     gate_src = wg.at[:, pl.ds(pl.multiple_of(kv * cols, LANES), cols)]
-    for n, (src, dst) in enumerate(((wq, bq), (wk, bk), (gate_src, bg), (wv, bv), (wo, bo))):
-        copy = pltpu.make_async_copy(src, dst, sems.at[n])
-        copy.start()
-        copies.append(copy)
+    copies = fetch(
+        ((tokens, bt), (gain, bn), (wq, bq), (wk, bk), (gate_src, bg), (wv, bv), (wo, bo)), sems
+    )
     blocks, rows = out.shape[:2]
-    act = tokens[...].astype(F32)
+    copies[0].wait()
+    copies[1].wait()
+    act = bt[...].astype(F32)
     square = jnp.sum(act * act, axis=1, keepdims=True)
-    scaled = (act * gain[...]).astype(BF16)
+    scaled = (act * bn[...]).astype(BF16)
 
     def put(value, at):
         width = value.shape[1]
         out[:, :, at : at + width] = value.reshape(blocks, rows, width).astype(BF16)
 
     at = 0
-    for n, buf in ((0, bq), (1, bk)):
+    for n, buf in ((2, bq), (3, bk), (5, bv), (6, bo)):
         copies[n].wait()
         put(jnp.dot(scaled, buf[...], preferred_element_type=F32), at)
         at += buf.shape[1]
-    copies[2].wait()
+    copies[4].wait()
     gate_count = bg.shape[0]
     wide = jnp.concatenate([bg[...].astype(F32), jnp.zeros((LANES - gate_count, cols), F32)], axis=0)
     gates = lax.dot_general(scaled, wide.astype(BF16), NT, preferred_element_type=F32)
     lane = lax.broadcasted_iota(jnp.int32, gates.shape, 1)
-    gates = jnp.where(lane == gate_count, square, gates)
-    for n, buf in ((3, bv), (4, bo)):
-        copies[n].wait()
-        put(jnp.dot(scaled, buf[...], preferred_element_type=F32), at)
-        at += buf.shape[1]
-    put(gates, at)
+    put(jnp.where(lane == gate_count, square, gates), at)
 
 
 def project(tokens, mix_gain, w_query, w_key, w_value, w_outgate, w_gates, blocks):
@@ -64,25 +70,27 @@
     return pl.pallas_call(
         project_kernel,
         out_shape=jax.ShapeDtypeStruct((blocks, rows // blocks, width), BF16),
-        in_specs=[spec(VMEM)] * 2 + [spec(HBM)] * 5,
+        in_specs=[spec(HBM)] * 7,
         out_specs=spec(VMEM),
-        scratch_shapes=[pltpu.VMEM(w.shape, BF16) for w in weights]
-        + [pltpu.VMEM((w_gates.shape[1], cols), BF16), pltpu.SemaphoreType.DMA((5,))],
+        scratch_shapes=[pltpu.VMEM((rows, cols), BF16), pltpu.VMEM((1, cols), F32)]
+        + [pltpu.VMEM(w.shape, BF16) for w in weights]
+        + [pltpu.VMEM((w_gates.shape[1], cols), BF16), pltpu.SemaphoreType.DMA((7,))],
+        compiler_params=pltpu.CompilerParams(vmem_limit_bytes=8 << 20),
         name="project",
-    )(tokens, mix_gain[None], *weights, w_gates.T)
+    )(*stay(tokens, mix_gain[None], *weights, w_gates.T))
 
 
 def state_kernel(
-    recv, bias, memory, normalizer, stab, gain,
+    recv, bias_src, memory, norm_src, stab_src, gain_src,
     heads, norm_out, stab_out, forget_out, key_out, value_out,
-    mem, sems, *, model_width, total_heads,
+    bias, normalizer, stab, gain, mem, sems, *, model_width, total_heads,
 ):
     seqs, local = memory.shape[0], memory.shape[1]
-    copies = []
-    for h in range(local):
-        copy = pltpu.make_async_copy(memory.at[:, h], mem.at[h], sems.at[h])
-        copy.start()
-        copies.append(copy)
+    copies = fetch(
+        ((bias_src, bias), (norm_src, normalizer), (stab_src, stab), (gain_src, gain))
+        + tuple((memory.at[:, h], mem.at[h]) for h in range(local)),
+        sems,
+    )
     tp = lax.axis_index("tp")
     qw, vw = local * QK, local * VD
 
@@ -99,6 +107,8 @@
     diag = lax.broadcasted_iota(jnp.int32, (seqs, seqs), 0) == lax.broadcasted_iota(
         jnp.int32, (seqs, seqs), 1
     )
+    for copy in copies[:4]:
+        copy.wait()
 
     def own(at, h):
         both = [small[:, at + t * local + h : at + t * local + h + 1] for t in range(total_heads // local)]
@@ -110,7 +120,7 @@
     partial = []
     for h in range(local):
         input_pre = own(0, h) * inverse
-        log_forget = jax.nn.log_sigmoid(own(total_heads, h) * inverse + bias[h])
+        log_forget = jax.nn.log_sigmoid(own(total_heads, h) * inverse + bias[:, h : h + 1])
         old = jnp.sum(jnp.where(diag, stab[h : h + 1, :], 0.0), axis=1, keepdims=True)
         new = jnp.maximum(log_forget + old, input_pre)
         forget = jnp.exp(log_forget + old - new)
@@ -130,7 +140,7 @@
         partial.append((forget, (scale * query_key) * v, denom, spread))
     for h in range(local):
         forget, fresh, denom, spread = partial[h]
-        copies[h].wait()
+        copies[4 + h].wait()
         carried = jnp.zeros((seqs, VD), F32)
         for b in range(0, seqs, 2):
             left = jnp.concatenate([spread[b], spread[b + 1]], axis=1)
@@ -160,14 +170,19 @@
             jax.ShapeDtypeStruct((seqs, local, QK), F32),
             jax.ShapeDtypeStruct((seqs, local, VD), F32),
         ),
-        in_specs=[spec(VMEM), spec(SMEM), spec(HBM), spec(VMEM), spec(VMEM), spec(VMEM)],
+        in_specs=[spec(VMEM)] + [spec(HBM)] * 5,
         out_specs=[spec(VMEM)] * 6,
         scratch_shapes=[
+            pltpu.VMEM((1, local), F32),
+            pltpu.VMEM((seqs, local, QK), F32),
+            pltpu.VMEM((local, seqs), F32),
+            pltpu.VMEM((local, VD), F32),
             pltpu.VMEM((local, seqs, QK, VD), F32),
-            pltpu.SemaphoreType.DMA((local,)),
+            pltpu.SemaphoreType.DMA((4 + local,)),
         ],
+        compiler_params=pltpu.CompilerParams(vmem_limit_bytes=16 << 20),
         name="state",
-    )(recv, forget_bias, memory, normalizer, stabilizer.T, head_gain)
+    )(recv, *stay(forget_bias[None], memory, normalizer, stabilizer.T, head_gain))
 
 
 def mixer_kernel(rows_ref, gain, wg, wu, wd, keep, give, mlp):
@@ -202,6 +217,7 @@
         in_specs=[spec(VMEM)] * 5,
         out_specs=[spec(VMEM)] * 2,
         scratch_shapes=[pltpu.VMEM((rows, blocks * cols), BF16)],
+        compiler_params=pltpu.CompilerParams(vmem_limit_bytes=16 << 20),
         name="mixer",
     )(gathered, mlp_gain[None], w_gate.T, w_up.T, w_down)
 

time: 82.8 us -> 74.2 us (0.90)
  Pallas kernels: 11.8 us -> 6.31 us
  blocking collectives: 48.2 us -> 46.3 us
  other arithmetic: 6.37 us -> 5.42 us
    pallas_call x1, Pallas kernels: 3.67 us -> 1.18 us  [mixer(): pl.pallas_call(mixer_kernel, out_shape=(half, half), in_specs=[spec(VMEM)...]
    all_to_all x3, blocking collectives: 48.2 us -> 46.3 us  [exchanged(): return lax.all_to_all(blocks, 'kv', 0, 0, tiled=True)]
    pallas_call x1, Pallas kernels: 3.57 us -> 1.96 us  [project(): pl.pallas_call(project_kernel, out_shape=jax.ShapeDtypeStruct((blocks, ro...]
    pallas_call x1, Pallas kernels: 4.57 us -> 3.17 us  [state_step(): pl.pallas_call(kernel, out_shape=(jax.ShapeDtypeStruct((blocks, seqs, loc...]
    convert_element_type x1, other arithmetic: 1.72 us -> 0.77 us  [body(): pair = (keep.astype(F32) + other_core(give).astype(F32)).astype(BF16)]
  transfers between devices with their start and end apart: 3 -> 3, of which waited for: 3 -> 3; matrix products, arithmetic and copies ran while one was open for 5% -> 6% of each run, Pallas kernels for 0% -> 0%
where the time goes in v2:
time: 74.2 us; the launch traced here: 73.8 us
  blocking collectives  46.3 us (62%)
  starting transfers between devices  8.05 us (11%)
  Pallas kernels  6.31 us (9%)
  waiting for transfers between devices  6.12 us (8%)
  other arithmetic  5.42 us (7%)
    all_to_all x3, blocking collectives, exchanged(): return lax.all_to_all(blocks, 'kv', 0, 0, tiled=True)  46.3 us
    ppermute x2, starting transfers between devices, other_core(): return lax.ppermute(value, 'tp', [(0, 1), (1, 0)])  4.52 us
    all_to_all x1, waiting for transfers between devices, exchanged(): return lax.all_to_all(blocks, 'kv', 0, 0, tiled=True)  4.4 us
    add x1, other arithmetic, body(): late_forget[:, :, :1, None] * memory  3.97 us
    all_to_all x1, starting transfers between devices, exchanged(): return lax.all_to_all(blocks, 'kv', 0, 0, tiled=True)  3.53 us
    pallas_call x1, Pallas kernels, state_step(): pl.pallas_call(kernel, out_shape=(jax.ShapeDtypeStruct((blocks, seqs, loc...  3.17 us
    pallas_call x1, Pallas kernels, project(): pl.pallas_call(project_kernel, out_shape=jax.ShapeDtypeStruct((blocks, ro...  1.96 us
    ppermute x2, waiting for transfers between devices, other_core(): return lax.ppermute(value, 'tp', [(0, 1), (1, 0)])  1.72 us
  transfers between devices with their start and end apart: 3, of which 3 were waited for; matrix products, arithmetic and copies ran while one was open for 6% of the time, Pallas kernels for 0%

profile of v2, /device:TPU:1, one launch (start us, length us, event | category | flops | bytes accessed | tf_op | source)
XLA Modules:
  0.0 73.8 jit_solution(2667990321658588110)
XLA Ops:
  0.6 0.0 copy-start
  0.6 2.0 %project.1 = bf16[16,8,3200]{2,1,0:T(8,128)(2,1)S(1)} custom-call(bf16[128,128]{1,0:T(8,128)(2,1)} %tokens.1, f32[1,128]{1,0:T(1,128)} %bitcast.25, bf16[128,512]{1,0:T(8,128)(2,1)} %wq.1, bf16[128,512]{1,0:T(8,128)(2,1)} %wk.1, bf16[128,1024]{1,0:T(8,128)(2,1)} %wv.1, bf16[128,1024]{1,0:T(8,128)(2,1)} %wo.1, bf16[16,2048]{1,0:T(8,128)(2,1)} %bitcast.22), custom_call_target="tpu_custom_call" | custom-call | tf_op jit(solution)/shard_map/project/pallas_call | solution.py:70
  2.6 0.0 copy-start.5
  2.6 22.3 %all_to_all.20.refs_0_ = bf16[16,8,3200]{2,1,0:T(8,128)(2,1)S(1)} all-to-all(bf16[16,8,3200]{2,1,0:T(8,128)(2,1)S(1)} %project.1), channel_id=1, replica_groups=mesh['dp'=4,'kv'=16,'tp'=2] {'kv'}, dimensions={0} | all-to-all | bytes 1638400 | tf_op jit(solution)/shard_map/all_to_all | solution.py:230
  24.9 3.2 %state.1 = (bf16[16,8,1024]{2,1,0:T(8,128)(2,1)S(1)}, f32[8,4,128]{2,1,0:T(4,128)}, f32[4,8]{1,0:T(4,128)}, f32[8,4,128]{2,1,0:T(4,128)S(1)}, f32[8,4,128]{2,1,0:T(4,128)S(1)}, /*index=5*/f32[8,4,256]{2,1,0:T(4,128)S(1)}) custom-call(bf16[16,8,3200]{2,1,0:T(8,128)(2,1)S(1)} %all_to_all.20.refs_0_, f32[1,4]{1,0:T(1,128)} %bitcast.26, ...), custom_call_target="tpu_custom_call" | custom-call | tf_op jit(solution)/shard_map/state/pallas_call | solution.py:163
  28.1 10.7 %all_to_all.21 = bf16[16,8,1024]{2,1,0:T(8,128)(2,1)S(1)} all-to-all(bf16[16,8,1024]{2,1,0:T(8,128)(2,1)S(1)} %get-tuple-element.15), channel_id=1, replica_groups=mesh['dp'=4,'kv'=16,'tp'=2] {'kv'}, dimensions={0} | all-to-all | bytes 524288 | tf_op jit(solution)/shard_map/all_to_all | solution.py:230
  38.8 0.3 convolution_convert_fusion
  39.0 2.7 %collective-permute-start = (bf16[128,128]{0,1:T(8,128)(2,1)S(1)}, bf16[128,128]{0,1:T(8,128)(2,1)S(1)}, u32[]{:S(2)}, u32[]{:S(2)}) collective-permute-start(bf16[128,128]{0,1:T(8,128)(2,1)S(1)} %convolution_convert_fusion), channel_id=1, source_target_pairs={{0,1},{1,0},{2,3},{3,2},{4,5},{5,4},{6,7},{7,6},{8,9},{9,8},{10,11... | collective-permute-start | bytes 98312 | tf_op jit(solution)/shard_map/ppermute | solution.py:226
  41.8 0.1 copy.21
  41.9 0.7 %collective-permute-done = bf16[128,128]{0,1:T(8,128)(2,1)S(1)} collective-permute-done((bf16[128,128]{0,1:T(8,128)(2,1)S(1)}, bf16[128,128]{0,1:T(8,128)(2,1)S(1)}, u32[]{:S(2)}, u32[]{:S(2)}) %collective-permute-start) | collective-permute-done | bytes 32800 | tf_op jit(solution)/shard_map/ppermute | solution.py:226
  42.6 0.1 copy.22
  42.8 0.1 broadcast_in_dim.20
  42.9 13.4 %all_to_all.22.rows_ref = bf16[16,128,128]{2,1,0:T(8,128)(2,1)S(1)} all-to-all(bf16[16,128,128]{2,1,0:T(8,128)(2,1)S(1)} %broadcast_in_dim.20), channel_id=1, replica_groups=mesh['dp'=4,'kv'=16,'tp'=2] {'kv'}, dimensions={0} | all-to-all | bytes 1048576 | tf_op jit(solution)/shard_map/all_to_all | solution.py:230
  56.3 0.0 copy-done.2
  56.3 1.2 %mixer.1 = (bf16[16,64,128]{2,1,0:T(8,128)(2,1)S(1)}, bf16[16,64,128]{2,1,0:T(8,128)(2,1)S(1)}) custom-call(bf16[16,128,128]{2,1,0:T(8,128)(2,1)S(1)} %all_to_all.22.rows_ref, f32[1,2048]{1,0:T(1,128)S(1)} %bitcast.21, bf16[176,2048]{1,0:T(8,128)(2,1)S(1)} %bitcast.18, bf16[176,2048]{1,0:T(8,128)(2,1)S(1)} %bitcast.19, bf16[176,2048]{1,0:T(8,128)(2,1)S(1)} %copy-done.3), custom_call_target="tpu_custom_call" | custom-call | tf_op jit(solution)/shard_map/mixer/pallas_call | solution.py:214
  57.5 1.8 %collective-permute-start.1 = (bf16[16,64,128]{2,1,0:T(8,128)(2,1)S(1)}, bf16[16,64,128]{2,1,0:T(8,128)(2,1)S(1)}, u32[]{:S(2)}, u32[]{:S(2)}) collective-permute-start(bf16[16,64,128]{2,1,0:T(8,128)(2,1)S(1)} %get-tuple-element.17), channel_id=1, source_target_pairs={{0,1},{1,0},{2,3},{3,2},{4,5},{5,4},{6,7},{7,6},{8,9},{9,8},{10,11... | collective-permute-start | bytes 786440 | tf_op jit(solution)/shard_map/ppermute | solution.py:226
  59.3 0.1 copy.23
  59.4 0.1 copy.24
  59.4 1.0 %collective-permute-done.1 = bf16[16,64,128]{2,1,0:T(8,128)(2,1)S(1)} collective-permute-done((bf16[16,64,128]{2,1,0:T(8,128)(2,1)S(1)}, bf16[16,64,128]{2,1,0:T(8,128)(2,1)S(1)}, u32[]{:S(2)}, u32[]{:S(2)}) %collective-permute-start.1) | collective-permute-done | bytes 262176 | tf_op jit(solution)/shard_map/ppermute | solution.py:226
  60.4 0.8 %add_convert_fusion = bf16[16,64,128]{2,1,0:T(8,128)(2,1)} fusion(bf16[16,64,128]{2,1,0:T(8,128)(2,1)S(1)} %collective-permute-done.1, bf16[16,64,128]{2,1,0:T(8,128)(2,1)S(1)} %get-tuple-element.16), kind=kLoop, calls=%fused_computation.3 | loop fusion | flops 524288 | bytes 786432 | tf_op jit(solution)/shard_map/convert_element_type | solution.py:272
  61.2 3.5 %all-to-all-start.3 = ((bf16[16,64,128]{2,1,0:T(8,128)(2,1)}), bf16[16,64,128]{2,1,0:T(8,128)(2,1)S(1)}, u32[]{:S(2)}, u32[]{:S(2)}) async-start(bf16[16,64,128]{2,1,0:T(8,128)(2,1)} %add_convert_fusion), calls=%async_computation.3 | async-start | bytes 524288 | tf_op jit(solution)/shard_map/all_to_all | solution.py:230
  64.7 4.0 %multiply_add_fusion = f32[8,4,128,256]{3,2,1,0:T(8,128)} fusion(f32[8,4,128,256]{3,2,1,0:T(8,128)} %refs_2_.1, f32[8,4,256]{2,1,0:T(4,128)S(1)} %get-tuple-element.23, f32[8,4,128]{2,1,0:T(4,128)S(1)} %get-tuple-element.22, f32[8,4]{1,0:T(8,128)S(1)} %copy.24), kind=kLoop, calls=%fused_computation | loop fusion | flops 3145728 | bytes 8437888 | tf_op jit(solution)/shard_map/add | solution.py:275
  68.7 4.4 %all-to-all-done.3 = bf16[16,64,128]{2,1,0:T(8,128)(2,1)S(1)} async-done(((bf16[16,64,128]{2,1,0:T(8,128)(2,1)}), bf16[16,64,128]{2,1,0:T(8,128)(2,1)S(1)}, u32[]{:S(2)}, u32[]{:S(2)}) %all-to-all-start.3) | async-done | bytes 262176 | tf_op jit(solution)/shard_map/all_to_all | solution.py:230
  73.1 0.6 fusion.1
  (11 shorter events, 0.1 us)
Async XLA Ops:
  0.6 38.1 %copy-start = (bf16[1024,128]{1,0:T(8,128)(2,1)S(1)}, bf16[1024,128]{1,0:T(8,128)(2,1)}, u32[]{:S(2)}) copy-start(bf16[1024,128]{1,0:T(8,128)(2,1)} %param.29) | copy-start | bytes 786436
  2.6 39.1 %copy-start.5 = (bf16[128,128]{1,0:T(8,128)(2,1)S(1)}, bf16[128,128]{1,0:T(8,128)(2,1)}, u32[]{:S(2)}) copy-start(bf16[128,128]{1,0:T(8,128)(2,1)} %tokens.1) | copy-start | bytes 98308
  24.9 31.4 %copy-start.1 = (bf16[2048,176]{0,1:T(8,128)(2,1)S(1)}, bf16[2048,176]{0,1:T(8,128)(2,1)}, u32[]{:S(2)}) copy-start(bf16[2048,176]{0,1:T(8,128)(2,1)} %param.31) | copy-start | bytes 2162692
  24.9 31.4 %copy-start.2 = (bf16[2048,176]{0,1:T(8,128)(2,1)S(1)}, bf16[2048,176]{0,1:T(8,128)(2,1)}, u32[]{:S(2)}) copy-start(bf16[2048,176]{0,1:T(8,128)(2,1)} %param.32) | copy-start | bytes 2162692
  24.9 31.4 %copy-start.3 = (bf16[176,2048]{1,0:T(8,128)(2,1)S(1)}, bf16[176,2048]{1,0:T(8,128)(2,1)}, u32[]{:S(2)}) copy-start(bf16[176,2048]{1,0:T(8,128)(2,1)} %wd.1) | copy-start | bytes 2162692
  24.9 31.4 %copy-start.4 = (f32[2048]{0:T(1024)S(1)}, f32[2048]{0:T(1024)}, u32[]{:S(2)}) copy-start(f32[2048]{0:T(1024)} %param.30) | copy-start | bytes 24580
  39.0 3.6 %collective-permute-start = (bf16[128,128]{0,1:T(8,128)(2,1)S(1)}, bf16[128,128]{0,1:T(8,128)(2,1)S(1)}, u32[]{:S(2)}, u32[]{:S(2)}) collective-permute-start(bf16[128,128]{0,1:T(8,128)(2,1)S(1)} %convolution_convert_fusion), channel_id=1, source_target_pairs={{0,1},{1,0},{2,3},{3,2},{4,5},{5,4},{6,7},{7,6},{8,9},{9,8},{10,11... | collective-permute-start | bytes 98312 | tf_op jit(solution)/shard_map/ppermute | solution.py:226
  57.5 3.0 %collective-permute-start.1 = (bf16[16,64,128]{2,1,0:T(8,128)(2,1)S(1)}, bf16[16,64,128]{2,1,0:T(8,128)(2,1)S(1)}, u32[]{:S(2)}, u32[]{:S(2)}) collective-permute-start(bf16[16,64,128]{2,1,0:T(8,128)(2,1)S(1)} %get-tuple-element.17), channel_id=1, source_target_pairs={{0,1},{1,0},{2,3},{3,2},{4,5},{5,4},{6,7},{7,6},{8,9},{9,8},{10,11... | collective-permute-start | bytes 786440 | tf_op jit(solution)/shard_map/ppermute | solution.py:226
  61.2 11.9 %all-to-all-start.3 = ((bf16[16,64,128]{2,1,0:T(8,128)(2,1)}), bf16[16,64,128]{2,1,0:T(8,128)(2,1)S(1)}, u32[]{:S(2)}, u32[]{:S(2)}) async-start(bf16[16,64,128]{2,1,0:T(8,128)(2,1)} %add_convert_fusion), calls=%async_computation.3 | async-start | bytes 524288 | tf_op jit(solution)/shard_map/all_to_all | solution.py:230

commit v3 on v2

--- a/solution.py
+++ b/solution.py
@@ -76,21 +76,16 @@
         + [pltpu.VMEM(w.shape, BF16) for w in weights]
         + [pltpu.VMEM((w_gates.shape[1], cols), BF16), pltpu.SemaphoreType.DMA((7,))],
         compiler_params=pltpu.CompilerParams(vmem_limit_bytes=8 << 20),
+        cost_estimate=pl.CostEstimate(flops=10**10, bytes_accessed=10**7, transcendentals=0),
         name="project",
     )(*stay(tokens, mix_gain[None], *weights, w_gates.T))
 
 
 def state_kernel(
-    recv, bias_src, memory, norm_src, stab_src, gain_src,
-    heads, norm_out, stab_out, forget_out, key_out, value_out,
-    bias, normalizer, stab, gain, mem, sems, *, model_width, total_heads,
+    recv, bias, memory, normalizer, stab, gain,
+    heads, norm_out, stab_out, forget_out, key_out, value_out, *, model_width, total_heads,
 ):
     seqs, local = memory.shape[0], memory.shape[1]
-    copies = fetch(
-        ((bias_src, bias), (norm_src, normalizer), (stab_src, stab), (gain_src, gain))
-        + tuple((memory.at[:, h], mem.at[h]) for h in range(local)),
-        sems,
-    )
     tp = lax.axis_index("tp")
     qw, vw = local * QK, local * VD
 
@@ -107,8 +102,6 @@
     diag = lax.broadcasted_iota(jnp.int32, (seqs, seqs), 0) == lax.broadcasted_iota(
         jnp.int32, (seqs, seqs), 1
     )
-    for copy in copies[:4]:
-        copy.wait()
 
     def own(at, h):
         both = [small[:, at + t * local + h : at + t * local + h + 1] for t in range(total_heads // local)]
@@ -130,21 +123,20 @@
         scaled_key = scale * k
         new_norm = forget * normalizer[:, h, :] + scaled_key
         norm_out[:, h, :] = new_norm
+        v = value[:, h * VD : (h + 1) * VD]
+        forget_out[:, h, :] = jnp.broadcast_to(forget, (seqs, LANES))
         key_out[:, h, :] = scaled_key
-        v = value[:, h * VD : (h + 1) * VD]
         value_out[:, h, :] = v
-        forget_out[:, h, :] = jnp.broadcast_to(forget, (seqs, LANES))
         denom = jnp.maximum(jnp.abs(jnp.sum(q * new_norm, axis=1, keepdims=True)), 1.0)
         query_key = jnp.sum(q * k, axis=1, keepdims=True)
         spread = [jnp.where(row == b, q, 0.0).astype(BF16) for b in range(seqs)]
         partial.append((forget, (scale * query_key) * v, denom, spread))
     for h in range(local):
         forget, fresh, denom, spread = partial[h]
-        copies[4 + h].wait()
         carried = jnp.zeros((seqs, VD), F32)
         for b in range(0, seqs, 2):
             left = jnp.concatenate([spread[b], spread[b + 1]], axis=1)
-            right = mem[h, b : b + 2].reshape(2 * QK, VD).astype(BF16)
+            right = jnp.concatenate([memory[b, h], memory[b + 1, h]], axis=0).astype(BF16)
             carried = carried + jnp.dot(left, right, preferred_element_type=F32)
         head_out = (forget * carried + fresh) / denom
         normed = head_out * lax.rsqrt(jnp.mean(head_out * head_out, axis=1, keepdims=True) + EPSILON)
@@ -170,19 +162,48 @@
             jax.ShapeDtypeStruct((seqs, local, QK), F32),
             jax.ShapeDtypeStruct((seqs, local, VD), F32),
         ),
-        in_specs=[spec(VMEM)] + [spec(HBM)] * 5,
+        in_specs=[spec(VMEM)] * 6,
         out_specs=[spec(VMEM)] * 6,
-        scratch_shapes=[
-            pltpu.VMEM((1, local), F32),
-            pltpu.VMEM((seqs, local, QK), F32),
-            pltpu.VMEM((local, seqs), F32),
-            pltpu.VMEM((local, VD), F32),
-            pltpu.VMEM((local, seqs, QK, VD), F32),
-            pltpu.SemaphoreType.DMA((4 + local,)),
-        ],
         compiler_params=pltpu.CompilerParams(vmem_limit_bytes=16 << 20),
         name="state",
-    )(recv, *stay(forget_bias[None], memory, normalizer, stabilizer.T, head_gain))
+    )(recv, forget_bias[None], memory, normalizer, stabilizer.T, head_gain)
+
+
+def memory_kernel(memory, forget, key, value, *rest, first):
+    target, fresh, sems = rest[-3:]
+    seqs = memory.shape[0]
+    writes = []
+    for n in range(fresh.shape[0]):
+        h = first + n
+        key_cols = key[:, h, :].T
+        for b in range(seqs):
+            decay = forget[b : b + 1, h, :1]
+            fresh[n, b] = decay * memory[b, h] + key_cols[:, b : b + 1] * value[b : b + 1, h, :]
+        write = pltpu.make_async_copy(fresh.at[n], target.at[:, h], sems.at[n])
+        write.start()
+        writes.append(write)
+    for write in writes:
+        write.wait()
+
+
+def memory_step(memory, forget, key, value, first, count, partial=None):
+    def kernel(*refs):
+        memory_kernel(*refs, first=first)
+
+    extra = [] if partial is None else stay(partial)
+    return pl.pallas_call(
+        kernel,
+        out_shape=HBM(memory.shape, F32),
+        in_specs=[spec(VMEM)] * 4 + [spec(HBM)] * len(extra),
+        out_specs=spec(HBM),
+        input_output_aliases={4: 0} if extra else {},
+        scratch_shapes=[
+            pltpu.VMEM((count, memory.shape[0]) + memory.shape[2:], F32),
+            pltpu.SemaphoreType.DMA((count,)),
+        ],
+        compiler_params=pltpu.CompilerParams(vmem_limit_bytes=6 << 20),
+        name="memory",
+    )(memory, forget, key, value, *extra)
 
 
 def mixer_kernel(rows_ref, gain, wg, wu, wd, keep, give, mlp):
@@ -220,6 +241,76 @@
         compiler_params=pltpu.CompilerParams(vmem_limit_bytes=16 << 20),
         name="mixer",
     )(gathered, mlp_gain[None], w_gate.T, w_up.T, w_down)
+
+
+def branch_kernel(heads, w_out, out):
+    rows = heads[...].reshape(out.shape[0], w_out.shape[0])
+    out[...] = jnp.dot(rows, w_out[...], preferred_element_type=F32).astype(BF16)
+
+
+def branch_step(heads, w_out):
+    return pl.pallas_call(
+        branch_kernel,
+        out_shape=jax.ShapeDtypeStruct((heads.shape[0] * heads.shape[1], w_out.shape[1]), BF16),
+        in_specs=[spec(VMEM)] * 2,
+        out_specs=spec(VMEM),
+        compiler_params=pltpu.CompilerParams(vmem_limit_bytes=4 << 20),
+        name="branch",
+    )(heads, w_out)
+
+
+def pair_kernel(keep, got, after, out):
+    out[...] = (keep[...].astype(F32) + got[...].astype(F32)).astype(BF16)
+
+
+def pair_step(keep, got, after):
+    return pl.pallas_call(
+        pair_kernel,
+        out_shape=jax.ShapeDtypeStruct(keep.shape, BF16),
+        in_specs=[spec(VMEM)] * 2 + [spec(HBM)],
+        out_specs=spec(VMEM),
+        compiler_params=pltpu.CompilerParams(vmem_limit_bytes=4 << 20),
+        name="pair",
+    )(keep, got, *stay(after))
+
+
+def residual_kernel(tokens, branch, other, after, spread, own):
+    total = tokens[...].astype(F32) + (branch[...].astype(F32) + other[...].astype(F32))
+    rounded = total.astype(BF16)
+    spread[...] = jnp.broadcast_to(rounded[None], spread.shape)
+    turned = rounded.astype(F32).T
+    half = own.shape[0]
+    own[...] = jnp.where(lax.axis_index("tp") == 0, turned[:half], turned[half:]).astype(BF16)
+
+
+def residual_step(tokens, branch, other, after, blocks):
+    rows, cols = tokens.shape
+    return pl.pallas_call(
+        residual_kernel,
+        out_shape=(
+            jax.ShapeDtypeStruct((blocks, rows, cols), BF16),
+            jax.ShapeDtypeStruct((cols // 2, rows), BF16),
+        ),
+        in_specs=[spec(VMEM)] * 3 + [spec(HBM)],
+        out_specs=[spec(VMEM)] * 2,
+        compiler_params=pltpu.CompilerParams(vmem_limit_bytes=4 << 20),
+        name="residual",
+    )(tokens, branch, other, *stay(after))
+
+
+def finish_kernel(recv, own, out):
+    out[...] = (jnp.sum(recv[...].astype(F32), axis=0) + own[...].astype(F32)).astype(BF16)
+
+
+def finish(recv, own):
+    return pl.pallas_call(
+        finish_kernel,
+        out_shape=jax.ShapeDtypeStruct(own.shape, BF16),
+        in_specs=[spec(VMEM)] * 2,
+        out_specs=spec(VMEM),
+        compiler_params=pltpu.CompilerParams(vmem_limit_bytes=4 << 20),
+        name="finish",
+    )(recv, own)
 
 
 def other_core(value):
@@ -252,7 +343,7 @@
     devices = lax.axis_size("kv")
     rows, block_cols = tokens.shape
     send = project(tokens, mix_gain, w_query, w_key, w_value, w_outgate, w_gates, devices)
-    heads, new_normalizer, new_stabilizer, forget, scaled_key, value = state_step(
+    heads, new_normalizer, new_stabilizer, forget, key, value = state_step(
         exchanged(send),
         forget_bias,
         memory,
@@ -262,22 +353,17 @@
         block_cols * devices,
         w_gates.shape[1] // 2,
     )
-    gathered_heads = exchanged(heads).reshape(rows, -1)
-    branch = jnp.dot(gathered_heads, w_out, preferred_element_type=F32).astype(BF16)
-    residual = (
-        tokens.astype(F32) + (branch.astype(F32) + other_core(branch).astype(F32))
-    ).astype(BF16)
-    gathered = exchanged(jnp.broadcast_to(residual[None], (devices, *residual.shape)))
+    branch = branch_step(exchanged(heads), w_out)
+    half = memory.shape[1] // 2
+    forget, key, value, _ = lax.optimization_barrier((forget, key, value, branch))
+    first_half = memory_step(memory, forget, key, value, 0, half)
+    spread, own = residual_step(tokens, branch, other_core(branch), first_half, devices)
+    gathered = exchanged(spread)
     keep, give = mixer(gathered, mlp_gain, w_gate, w_up, w_down)
-    pair = (keep.astype(F32) + other_core(give).astype(F32)).astype(BF16)
-    late_forget, late_key, late_value, _ = lax.optimization_barrier((forget, scaled_key, value, keep))
-    new_memory = (
-        late_forget[:, :, :1, None] * memory + late_key[..., None] * late_value[:, :, None, :]
-    )
-    summed = jnp.sum(exchanged(pair).astype(F32), axis=0)
-    out_cols = block_cols // lax.axis_size("tp")
-    own = lax.dynamic_slice_in_dim(residual, lax.axis_index("tp") * out_cols, out_cols, 1)
-    mixed_out = (summed + own.T.astype(F32)).astype(BF16).T
+    forget, key, value, _ = lax.optimization_barrier((forget, key, value, give))
+    new_memory = memory_step(memory, forget, key, value, half, half, first_half)
+    pair = pair_step(keep, other_core(give), new_memory)
+    mixed_out = finish(exchanged(pair), own).T
     return (mixed_out, new_memory, new_normalizer, new_stabilizer.T)
 
 

time: 74.2 us -> 72.3 us (0.974)
  blocking collectives: 46.3 us -> 57.9 us
  waiting for transfers between devices: 6.12 us -> 0.01 us
  other arithmetic: 5.42 us -> 0 us
  starting transfers between devices: 8.05 us -> 4.26 us
  Pallas kernels: 6.31 us -> 8.97 us
    all_to_all x3 -> x4, blocking collectives: 46.3 us -> 57.9 us  [exchanged(): return lax.all_to_all(blocks, 'kv', 0, 0, tiled=True)]
    pallas_call x0 -> x6, Pallas kernels: none -> 4.6 us  [the longest x2 3.55 us: memory_step(): pl.pallas_call(kernel, out_shape=HBM(memory.shape, F32), in_specs=[spec(V...]
    all_to_all x1 -> x0, waiting for transfers between devices: 4.4 us -> none  [exchanged(): return lax.all_to_all(blocks, 'kv', 0, 0, tiled=True)]
    add x1 -> x0, other arithmetic: 3.97 us -> none  [body(): late_forget[:, :, :1, None] * memory]
    all_to_all x1 -> x0, starting transfers between devices: 3.53 us -> none  [exchanged(): return lax.all_to_all(blocks, 'kv', 0, 0, tiled=True)]
    pallas_call x1, Pallas kernels: 3.17 us -> 1.13 us  [state_step(): pl.pallas_call(kernel, out_shape=(jax.ShapeDtypeStruct((blocks, seqs, loc...]
    ppermute x2, waiting for transfers between devices: 1.72 us -> 0.01 us  [other_core(): return lax.ppermute(value, 'tp', [(0, 1), (1, 0)])]
    convert_element_type x3 -> x0, other arithmetic: 1.41 us -> none  [the longest x1 0.77 us: body(): pair = (keep.astype(F32) + other_core(give).astype(F32)).astype(BF16)]
  transfers between devices with their start and end apart: 3 -> 2, of which waited for: 3 -> 0; matrix products, arithmetic and copies ran while one was open for 6% -> 0% of each run, Pallas kernels for 0% -> 5%
where the time goes in v3:
time: 72.3 us; the launch traced here: 72.1 us
  blocking collectives  57.9 us (80%)
  Pallas kernels  8.97 us (12%)
  starting transfers between devices  4.26 us (6%)
  between operations  0.83 us (1%)
    all_to_all x4, blocking collectives, exchanged(): return lax.all_to_all(blocks, 'kv', 0, 0, tiled=True)  57.9 us
    ppermute x2, starting transfers between devices, other_core(): return lax.ppermute(value, 'tp', [(0, 1), (1, 0)])  4.26 us
    pallas_call x2, Pallas kernels, memory_step(): pl.pallas_call(kernel, out_shape=HBM(memory.shape, F32), in_specs=[spec(V...  3.55 us
    pallas_call x1, Pallas kernels, project(): pl.pallas_call(project_kernel, out_shape=jax.ShapeDtypeStruct((blocks, ro...  2.06 us
  transfers between devices with their start and end apart: 2, of which 0 were waited for; matrix products, arithmetic and copies ran while one was open for 0% of the time, Pallas kernels for 5%

profile of v3, /device:TPU:1, one launch (start us, length us, event | category | flops | bytes accessed | tf_op | source)
XLA Modules:
  0.0 72.1 jit_solution(59622791395767962)
XLA Ops:
  0.7 2.1 %project.1 = bf16[16,8,3200]{2,1,0:T(8,128)(2,1)S(1)} custom-call(bf16[128,128]{1,0:T(8,128)(2,1)} %tokens.3, f32[1,128]{1,0:T(1,128)} %bitcast.17, bf16[128,512]{1,0:T(8,128)(2,1)} %wq.1, bf16[128,512]{1,0:T(8,128)(2,1)} %wk.1, bf16[128,1024]{1,0:T(8,128)(2,1)} %wv.1, bf16[128,1024]{1,0:T(8,128)(2,1)} %wo.1, bf16[16,2048]{1,0:T(8,128)(2,1)} %bitcast.15), custom_call_target="tpu_custom_call" | custom-call | flops 10000000000 | bytes 10000000 | tf_op jit(solution)/shard_map/project/pallas_call | solution.py:70
  2.8 0.0 copy-start.4
  2.8 22.4 %all_to_all.20.refs_0_ = bf16[16,8,3200]{2,1,0:T(8,128)(2,1)S(1)} all-to-all(bf16[16,8,3200]{2,1,0:T(8,128)(2,1)S(1)} %project.1), channel_id=1, replica_groups=mesh['dp'=4,'kv'=16,'tp'=2] {'kv'}, dimensions={0} | all-to-all | bytes 1638400 | tf_op jit(solution)/shard_map/all_to_all | solution.py:321
  25.2 0.0 copy-done.6
  25.2 1.1 %state.1 = (bf16[16,8,1024]{2,1,0:T(8,128)(2,1)S(1)}, f32[8,4,128]{2,1,0:T(4,128)}, f32[4,8]{1,0:T(4,128)}, f32[8,4,128]{2,1,0:T(4,128)S(1)}, f32[8,4,128]{2,1,0:T(4,128)S(1)}, /*index=5*/f32[8,4,256]{2,1,0:T(4,128)S(1)}) custom-call(bf16[16,8,3200]{2,1,0:T(8,128)(2,1)S(1)} %all_to_all.20.refs_0_, f32[1,4]{1,0:T(1,128)S(1)} %bitcast.13, ...), custom_call_target="tpu_custom_call" | custom-call | tf_op jit(solution)/shard_map/state/pallas_call | solution.py:155
  26.3 10.7 %all_to_all.21.heads = bf16[16,8,1024]{2,1,0:T(8,128)(2,1)S(1)} all-to-all(bf16[16,8,1024]{2,1,0:T(8,128)(2,1)S(1)} %get-tuple-element.20), channel_id=1, replica_groups=mesh['dp'=4,'kv'=16,'tp'=2] {'kv'}, dimensions={0} | all-to-all | bytes 524288 | tf_op jit(solution)/shard_map/all_to_all | solution.py:321
  37.0 0.0 copy-done.4
  37.0 0.2 branch.1
  37.2 2.7 %collective-permute-start = (bf16[128,128]{1,0:T(8,128)(2,1)S(1)}, bf16[128,128]{1,0:T(8,128)(2,1)S(1)}, u32[]{:S(2)}, u32[]{:S(2)}) collective-permute-start(bf16[128,128]{1,0:T(8,128)(2,1)S(1)} %branch.1), channel_id=1, source_target_pairs={{0,1},{1,0},{2,3},{3,2},{4,5},{5,4},{6,7},{7,6},{8,9},{9,8},{10,11... | collective-permute-start | bytes 98312 | tf_op jit(solution)/shard_map/ppermute | solution.py:317
  39.9 1.8 %memory.2.after.refs_4_ = f32[8,4,128,256]{3,2,1,0:T(8,128)} custom-call(f32[8,4,128,256]{3,2,1,0:T(8,128)S(1)} %copy-done, f32[8,4,128]{2,1,0:T(4,128)S(1)} %get-tuple-element.30.refs_1_, f32[8,4,128]{2,1,0:T(4,128)S(1)} %get-tuple-element.31.refs_2_, f32[8,4,256]{2,1,0:T(4,128)S(1)} %get-tuple-element.32.refs_3_), custom_call_target="tpu_custom_call" | custom-call | tf_op jit(solution)/shard_map/memory/pallas_call | solution.py:194
  41.7 0.0 copy-start.1
  41.7 0.0 copy-start.2
  41.7 0.0 copy-start.3
  41.8 0.0 copy-start.7
  41.8 0.0 collective-permute-done.other
  41.8 0.1 residual.1
  41.9 13.8 %all_to_all.22.rows_ref = bf16[16,128,128]{2,1,0:T(8,128)(2,1)S(1)} all-to-all(bf16[16,128,128]{2,1,0:T(8,128)(2,1)S(1)} %get-tuple-element.27), channel_id=1, replica_groups=mesh['dp'=4,'kv'=16,'tp'=2] {'kv'}, dimensions={0} | all-to-all | bytes 1048576 | tf_op jit(solution)/shard_map/all_to_all | solution.py:321
  55.7 1.2 %mixer.1 = (bf16[16,64,128]{2,1,0:T(8,128)(2,1)S(1)}, bf16[16,64,128]{2,1,0:T(8,128)(2,1)S(1)}) custom-call(bf16[16,128,128]{2,1,0:T(8,128)(2,1)S(1)} %all_to_all.22.rows_ref, f32[1,2048]{1,0:T(1,128)S(1)} %bitcast.11, bf16[176,2048]{1,0:T(8,128)(2,1)S(1)} %bitcast.9, bf16[176,2048]{1,0:T(8,128)(2,1)S(1)} %bitcast.10, bf16[176,2048]{1,0:T(8,128)(2,1)S(1)} %copy-done.3), custom_call_target="tpu_custom_call" | custom-call | tf_op jit(solution)/shard_map/mixer/pallas_call | solution.py:235
  56.9 1.5 %collective-permute-start.1 = (bf16[16,64,128]{2,1,0:T(8,128)(2,1)S(1)}, bf16[16,64,128]{2,1,0:T(8,128)(2,1)S(1)}, u32[]{:S(2)}, u32[]{:S(2)}) collective-permute-start(bf16[16,64,128]{2,1,0:T(8,128)(2,1)S(1)} %get-tuple-element.29), channel_id=1, source_target_pairs={{0,1},{1,0},{2,3},{3,2},{4,5},{5,4},{6,7},{7,6},{8,9},{9,8},{10,11... | collective-permute-start | bytes 786440 | tf_op jit(solution)/shard_map/ppermute | solution.py:317
  58.4 1.8 %memory.3.after = f32[8,4,128,256]{3,2,1,0:T(8,128)} custom-call(f32[8,4,128,256]{3,2,1,0:T(8,128)S(1)} %copy-done, f32[8,4,128]{2,1,0:T(4,128)S(1)} %get-tuple-element.30.refs_1_, f32[8,4,128]{2,1,0:T(4,128)S(1)} %get-tuple-element.31.refs_2_, f32[8,4,256]{2,1,0:T(4,128)S(1)} %get-tuple-element.32.refs_3_, ...), custom_call_target="tpu_custom_call", output_to_operand_aliasing={{}: (4, {})} | custom-call | tf_op jit(solution)/shard_map/memory/pallas_call | solution.py:194
  60.2 0.0 collective-permute-done.1.got
  60.2 0.1 pair.1
  60.3 11.1 %all_to_all.23.recv = bf16[16,64,128]{2,1,0:T(8,128)(2,1)S(1)} all-to-all(bf16[16,64,128]{2,1,0:T(8,128)(2,1)S(1)} %pair.1), channel_id=1, replica_groups=mesh['dp'=4,'kv'=16,'tp'=2] {'kv'}, dimensions={0} | all-to-all | bytes 524288 | tf_op jit(solution)/shard_map/all_to_all | solution.py:321
  71.4 0.6 finish.1
  (15 shorter events, 0.0 us)
Async XLA Ops:
  0.6 24.5 %copy-start = (f32[8,4,128,256]{3,2,1,0:T(8,128)S(1)}, f32[8,4,128,256]{3,2,1,0:T(8,128)}, u32[]{:S(2)}) copy-start(f32[8,4,128,256]{3,2,1,0:T(8,128)} %refs_0_.3) | copy-start | bytes 12582916
  0.6 24.5 %copy-start.6 = (f32[8,4,128]{2,1,0:T(4,128)S(1)}, f32[8,4,128]{2,1,0:T(4,128)}, u32[]{:S(2)}) copy-start(f32[8,4,128]{2,1,0:T(4,128)} %refs_3_.1) | copy-start | bytes 49156
  0.7 24.5 %copy-start.8 = (f32[4,256]{1,0:T(4,128)S(1)}, f32[4,256]{1,0:T(4,128)}, u32[]{:S(2)}) copy-start(f32[4,256]{1,0:T(4,128)} %refs_5_.1) | copy-start | bytes 12292
  0.7 24.5 %copy-start.9 = (f32[8,4]{0,1:T(4,128)S(1)}, f32[8,4]{0,1:T(4,128)}, u32[]{:S(2)}) copy-start(f32[8,4]{0,1:T(4,128)} %param.27) | copy-start | bytes 388
  0.7 24.5 %copy-start.10 = (f32[4]{0:T(128)S(1)}, f32[4]{0:T(128)}, u32[]{:S(2)}) copy-start(f32[4]{0:T(128)} %param.24) | copy-start | bytes 52
  2.8 34.2 %copy-start.4 = (bf16[1024,128]{1,0:T(8,128)(2,1)S(1)}, bf16[1024,128]{1,0:T(8,128)(2,1)}, u32[]{:S(2)}) copy-start(bf16[1024,128]{1,0:T(8,128)(2,1)} %w_out.1) | copy-start | bytes 786436
  37.2 4.6 %collective-permute-start = (bf16[128,128]{1,0:T(8,128)(2,1)S(1)}, bf16[128,128]{1,0:T(8,128)(2,1)S(1)}, u32[]{:S(2)}, u32[]{:S(2)}) collective-permute-start(bf16[128,128]{1,0:T(8,128)(2,1)S(1)} %branch.1), channel_id=1, source_target_pairs={{0,1},{1,0},{2,3},{3,2},{4,5},{5,4},{6,7},{7,6},{8,9},{9,8},{10,11... | collective-permute-start | bytes 98312 | tf_op jit(solution)/shard_map/ppermute | solution.py:317
  39.9 1.8 %copy-start.5 = (bf16[128,128]{1,0:T(8,128)(2,1)S(1)}, bf16[128,128]{1,0:T(8,128)(2,1)}, u32[]{:S(2)}) copy-start(bf16[128,128]{1,0:T(8,128)(2,1)} %tokens.3) | copy-start | bytes 98308
  41.7 14.0 %copy-start.1 = (bf16[2048,176]{0,1:T(8,128)(2,1)S(1)}, bf16[2048,176]{0,1:T(8,128)(2,1)}, u32[]{:S(2)}) copy-start(bf16[2048,176]{0,1:T(8,128)(2,1)} %param.31) | copy-start | bytes 2162692
  41.7 14.0 %copy-start.2 = (bf16[2048,176]{0,1:T(8,128)(2,1)S(1)}, bf16[2048,176]{0,1:T(8,128)(2,1)}, u32[]{:S(2)}) copy-start(bf16[2048,176]{0,1:T(8,128)(2,1)} %param.32) | copy-start | bytes 2162692
  41.7 14.0 %copy-start.3 = (bf16[176,2048]{1,0:T(8,128)(2,1)S(1)}, bf16[176,2048]{1,0:T(8,128)(2,1)}, u32[]{:S(2)}) copy-start(bf16[176,2048]{1,0:T(8,128)(2,1)} %wd.1) | copy-start | bytes 2162692
  41.8 14.0 %copy-start.7 = (f32[2048]{0:T(1024)S(1)}, f32[2048]{0:T(1024)}, u32[]{:S(2)}) copy-start(f32[2048]{0:T(1024)} %param.30) | copy-start | bytes 24580
  56.9 3.3 %collective-permute-start.1 = (bf16[16,64,128]{2,1,0:T(8,128)(2,1)S(1)}, bf16[16,64,128]{2,1,0:T(8,128)(2,1)S(1)}, u32[]{:S(2)}, u32[]{:S(2)}) collective-permute-start(bf16[16,64,128]{2,1,0:T(8,128)(2,1)S(1)} %get-tuple-element.29), channel_id=1, source_target_pairs={{0,1},{1,0},{2,3},{3,2},{4,5},{5,4},{6,7},{7,6},{8,9},{9,8},{10,11... | collective-permute-start | bytes 786440 | tf_op jit(solution)/shard_map/ppermute | solution.py:317

commit v4 on v3

--- a/solution.py
+++ b/solution.py
@@ -9,6 +9,7 @@
 VD = 256
 EPSILON = 1e-06
 LANES = 128
+SUBLANES = 8
 F32 = jnp.float32
 BF16 = jnp.bfloat16
 NT = (((1,), (1,)), ((), ()))
@@ -169,94 +170,117 @@
     )(recv, forget_bias[None], memory, normalizer, stabilizer.T, head_gain)
 
 
-def memory_kernel(memory, forget, key, value, *rest, first):
-    target, fresh, sems = rest[-3:]
+def memory_kernel(*refs, first, count, kept):
+    memory, forget, key, value = refs[:4]
+    small = refs[4 : 4 + kept]
+    target = refs[-3 - kept]
+    small_out = refs[len(refs) - 2 - kept : len(refs) - 2]
+    fresh, sems = refs[-2:]
     seqs = memory.shape[0]
     writes = []
-    for n in range(fresh.shape[0]):
+
+    def send(src, dst):
+        write = pltpu.make_async_copy(src, dst, sems.at[len(writes)])
+        write.start()
+        writes.append(write)
+
+    for src, dst in zip(small, small_out):
+        send(src, dst)
+    for n in range(count):
         h = first + n
         key_cols = key[:, h, :].T
         for b in range(seqs):
             decay = forget[b : b + 1, h, :1]
             fresh[n, b] = decay * memory[b, h] + key_cols[:, b : b + 1] * value[b : b + 1, h, :]
-        write = pltpu.make_async_copy(fresh.at[n], target.at[:, h], sems.at[n])
-        write.start()
-        writes.append(write)
+            if b % 2:
+                send(fresh.at[n, b - 1 : b + 1], target.at[b - 1 : b + 1, h])
     for write in writes:
         write.wait()
 
 
-def memory_step(memory, forget, key, value, first, count, partial=None):
+def memory_step(memory, forget, key, value, first, count, partial=None, small=()):
     def kernel(*refs):
-        memory_kernel(*refs, first=first)
+        memory_kernel(*refs, first=first, count=count, kept=len(small))
 
     extra = [] if partial is None else stay(partial)
-    return pl.pallas_call(
+    outs = [HBM(memory.shape, F32)] + [HBM(a.shape, F32) for a in small]
+    got = pl.pallas_call(
         kernel,
-        out_shape=HBM(memory.shape, F32),
-        in_specs=[spec(VMEM)] * 4 + [spec(HBM)] * len(extra),
-        out_specs=spec(HBM),
+        out_shape=outs,
+        in_specs=[spec(VMEM)] * (4 + len(small)) + [spec(HBM)] * len(extra),
+        out_specs=[spec(HBM)] * len(outs),
         input_output_aliases={4: 0} if extra else {},
         scratch_shapes=[
             pltpu.VMEM((count, memory.shape[0]) + memory.shape[2:], F32),
-            pltpu.SemaphoreType.DMA((count,)),
+            pltpu.SemaphoreType.DMA((count * memory.shape[0] // 2 + len(small),)),
         ],
         compiler_params=pltpu.CompilerParams(vmem_limit_bytes=6 << 20),
+        cost_estimate=pl.CostEstimate(flops=0, bytes_accessed=0, transcendentals=0),
         name="memory",
-    )(memory, forget, key, value, *extra)
-
-
-def mixer_kernel(rows_ref, gain, wg, wu, wd, keep, give, mlp):
-    blocks, rows, cols = rows_ref.shape
+    )(memory, forget, key, value, *small, *extra)
+    return got if small else got[0]
+
+
+def mixer_kernel(mine, other, after, wg, wu, wd, keep, give, mlp):
+    blocks, tall, rows = mine.shape
+    half = keep.shape[1]
+    cols = 2 * half
     tp = lax.axis_index("tp")
-    total = jnp.zeros((rows, cols), F32)
+    low = tp == 0
+    square = jnp.zeros((tall - half, rows), F32)
     for j in range(blocks):
-        value = rows_ref[j].astype(F32)
-        total = total + value * value
-    inverse = lax.rsqrt(jnp.sum(total, axis=1, keepdims=True) / (blocks * cols) + EPSILON)
-    for j in range(blocks):
-        lo = j * cols
-        value = rows_ref[j].astype(F32) * inverse * gain[:, lo : lo + cols]
-        mlp[:, lo : lo + cols] = value.astype(BF16)
-    gate = lax.dot_general(mlp[...], wg[...], NT, preferred_element_type=F32)
-    up = lax.dot_general(mlp[...], wu[...], NT, preferred_element_type=F32)
-    hidden = (jax.nn.silu(gate) * up).astype(BF16)
-    half = keep.shape[1]
+        square = square + (mine[j, half:].astype(F32) + other[j, half:].astype(F32))
+        mlp[pl.ds(pl.multiple_of(j * cols + tp * half, half), half), :] = mine[j, :half]
+        mlp[pl.ds(pl.multiple_of(j * cols + (1 - tp) * half, half), half), :] = other[j, :half]
+    inverse = lax.rsqrt(jnp.sum(square, axis=0, keepdims=True) / (blocks * cols) + EPSILON)
+    gate = jnp.dot(wg[...], mlp[...], preferred_element_type=F32) * inverse
+    up = jnp.dot(wu[...], mlp[...], preferred_element_type=F32) * inverse
+    hidden = (jax.nn.silu(gate) * up).T.astype(BF16)
     for j in range(blocks):
         part = jnp.dot(hidden, wd[:, j * cols : (j + 1) * cols], preferred_element_type=F32).T
         first, second = part[:half].astype(BF16), part[half:].astype(BF16)
-        keep[j] = jnp.where(tp == 0, first, second)
-        give[j] = jnp.where(tp == 0, second, first)
-
-
-def mixer(gathered, mlp_gain, w_gate, w_up, w_down):
-    blocks, rows, cols = gathered.shape
-    half = jax.ShapeDtypeStruct((blocks, cols // 2, rows), BF16)
+        keep[j] = jnp.where(low, first, second)
+        give[j] = jnp.where(low, second, first)
+
+
+def mixer(mine, other, after, w_gate, w_up, w_down, half):
+    blocks, _, rows = mine.shape
+    result = jax.ShapeDtypeStruct((blocks, half, rows), BF16)
     return pl.pallas_call(
         mixer_kernel,
-        out_shape=(half, half),
-        in_specs=[spec(VMEM)] * 5,
+        out_shape=(result, result),
+        in_specs=[spec(VMEM)] * 2 + [spec(HBM)] + [spec(VMEM)] * 3,
         out_specs=[spec(VMEM)] * 2,
-        scratch_shapes=[pltpu.VMEM((rows, blocks * cols), BF16)],
+        scratch_shapes=[pltpu.VMEM((2 * blocks * half, rows), BF16)],
         compiler_params=pltpu.CompilerParams(vmem_limit_bytes=16 << 20),
         name="mixer",
-    )(gathered, mlp_gain[None], w_gate.T, w_up.T, w_down)
-
-
-def branch_kernel(heads, w_out, out):
-    rows = heads[...].reshape(out.shape[0], w_out.shape[0])
-    out[...] = jnp.dot(rows, w_out[...], preferred_element_type=F32).astype(BF16)
-
-
-def branch_step(heads, w_out):
+    )(mine, other, *stay(after), w_gate.T, w_up.T, w_down)
+
+
+def halves(turned):
+    half = turned.shape[0] // 2
+    low = lax.axis_index("tp") == 0
+    first, second = turned[:half], turned[half:]
+    return jnp.where(low, first, second), jnp.where(low, second, first)
+
+
+def branch_kernel(heads, w_out, wg, wu, wd, keep, give):
+    rows = heads[...].reshape(heads.shape[0] * heads.shape[1], w_out.shape[0])
+    mine, other = halves(jnp.dot(rows, w_out[...], preferred_element_type=F32).T)
+    keep[...] = mine.astype(BF16)
+    give[...] = other.astype(BF16)
+
+
+def branch_step(heads, w_out, *early):
+    result = jax.ShapeDtypeStruct((w_out.shape[1] // 2, heads.shape[0] * heads.shape[1]), BF16)
     return pl.pallas_call(
         branch_kernel,
-        out_shape=jax.ShapeDtypeStruct((heads.shape[0] * heads.shape[1], w_out.shape[1]), BF16),
-        in_specs=[spec(VMEM)] * 2,
-        out_specs=spec(VMEM),
+        out_shape=(result, result),
+        in_specs=[spec(VMEM)] * (2 + len(early)),
+        out_specs=[spec(VMEM)] * 2,
         compiler_params=pltpu.CompilerParams(vmem_limit_bytes=4 << 20),
         name="branch",
-    )(heads, w_out)
+    )(heads, w_out, *early)
 
 
 def pair_kernel(keep, got, after, out):
@@ -274,28 +298,35 @@
     )(keep, got, *stay(after))
 
 
-def residual_kernel(tokens, branch, other, after, spread, own):
-    total = tokens[...].astype(F32) + (branch[...].astype(F32) + other[...].astype(F32))
-    rounded = total.astype(BF16)
-    spread[...] = jnp.broadcast_to(rounded[None], spread.shape)
-    turned = rounded.astype(F32).T
-    half = own.shape[0]
-    own[...] = jnp.where(lax.axis_index("tp") == 0, turned[:half], turned[half:]).astype(BF16)
-
-
-def residual_step(tokens, branch, other, after, blocks):
-    rows, cols = tokens.shape
+def residual_kernel(tokens, keep, got, gain, after, spread, own):
+    half, rows = own.shape
+    mine, _ = halves(tokens[...].astype(F32).T)
+    column, _ = halves(gain[pl.ds(lax.axis_index("kv"), 1), :].T)
+    rounded = (mine + (keep[...].astype(F32) + got[...].astype(F32))).astype(BF16)
+    own[...] = rounded
+    value = rounded.astype(F32)
+    square = jnp.sum(value * value, axis=0, keepdims=True)
+    coarse = square.astype(BF16).astype(F32)
+    line = lax.broadcasted_iota(jnp.int32, (spread.shape[1] - half, rows), 0)
+    tail = jnp.where(line == 0, coarse, jnp.where(line == 1, square - coarse, 0.0))
+    scaled = (value * column).astype(BF16)
+    spread[:, :half] = jnp.broadcast_to(scaled[None], (spread.shape[0], half, rows))
+    spread[:, half:] = jnp.broadcast_to(tail.astype(BF16)[None], (spread.shape[0],) + tail.shape)
+
+
+def residual_step(tokens, keep, got, mlp_gain, after, blocks):
+    half, rows = keep.shape
     return pl.pallas_call(
         residual_kernel,
         out_shape=(
-            jax.ShapeDtypeStruct((blocks, rows, cols), BF16),
-            jax.ShapeDtypeStruct((cols // 2, rows), BF16),
+            jax.ShapeDtypeStruct((blocks, half + SUBLANES, rows), BF16),
+            jax.ShapeDtypeStruct(keep.shape, BF16),
         ),
-        in_specs=[spec(VMEM)] * 3 + [spec(HBM)],
+        in_specs=[spec(VMEM)] * 4 + [spec(HBM)],
         out_specs=[spec(VMEM)] * 2,
         compiler_params=pltpu.CompilerParams(vmem_limit_bytes=4 << 20),
         name="residual",
-    )(tokens, branch, other, *stay(after))
+    )(tokens, keep, got, mlp_gain.reshape(blocks, 2 * half), *stay(after))
 
 
 def finish_kernel(recv, own, out):
@@ -343,7 +374,7 @@
     devices = lax.axis_size("kv")
     rows, block_cols = tokens.shape
     send = project(tokens, mix_gain, w_query, w_key, w_value, w_outgate, w_gates, devices)
-    heads, new_normalizer, new_stabilizer, forget, key, value = state_step(
+    heads, new_normalizer, new_stabilizer, forget, key, value_heads = state_step(
         exchanged(send),
         forget_bias,
         memory,
@@ -353,15 +384,18 @@
         block_cols * devices,
         w_gates.shape[1] // 2,
     )
-    branch = branch_step(exchanged(heads), w_out)
-    half = memory.shape[1] // 2
-    forget, key, value, _ = lax.optimization_barrier((forget, key, value, branch))
-    first_half = memory_step(memory, forget, key, value, 0, half)
-    spread, own = residual_step(tokens, branch, other_core(branch), first_half, devices)
-    gathered = exchanged(spread)
-    keep, give = mixer(gathered, mlp_gain, w_gate, w_up, w_down)
-    forget, key, value, _ = lax.optimization_barrier((forget, key, value, give))
-    new_memory = memory_step(memory, forget, key, value, half, half, first_half)
+    def behind(value):
+        return lax.optimization_barrier((forget, key, value_heads, value))[:3]
+
+    keep, give = branch_step(exchanged(heads), w_out, w_gate.T, w_up.T, w_down)
+    part, new_normalizer, new_stabilizer = memory_step(
+        memory, *behind(give), 0, 1, small=(new_normalizer, new_stabilizer)
+    )
+    spread, own = residual_step(tokens, keep, other_core(give), mlp_gain, part, devices)
+    mine = exchanged(spread)
+    part = memory_step(memory, *behind(mine), 1, 1, part)
+    keep, give = mixer(mine, other_core(mine), part, w_gate, w_up, w_down, own.shape[0])
+    new_memory = memory_step(memory, *behind(give), 2, memory.shape[1] - 2, part)
     pair = pair_step(keep, other_core(give), new_memory)
     mixed_out = finish(exchanged(pair), own).T
     return (mixed_out, new_memory, new_normalizer, new_stabilizer.T)

time: 72.3 us -> 70 us (0.968)
  blocking collectives: 57.9 us -> 55.4 us
    all_to_all x4, blocking collectives: 57.9 us -> 55.4 us  [exchanged(): return lax.all_to_all(blocks, 'kv', 0, 0, tiled=True)]
    pallas_call x4 -> x5, Pallas kernels: 4.94 us -> 5.49 us  [the longest x3 4.07 us: memory_step(): pl.pallas_call(kernel, out_shape=outs, in_specs=[spec(VMEM)] * (4 + len(s...]
    ppermute x2 -> x3, starting transfers between devices: 4.26 us -> 4.27 us  [other_core(): return lax.ppermute(value, 'tp', [(0, 1), (1, 0)])]
  transfers between devices with their start and end apart: 2 -> 3, of which waited for: 0 -> 0; matrix products, arithmetic and copies ran while one was open for 0% -> 0% of each run, Pallas kernels for 5% -> 6%
where the time goes in v4:
time: 70 us; the launch traced here: 69.7 us
  blocking collectives  55.4 us (79%)
  Pallas kernels  9.05 us (13%)
  starting transfers between devices  4.27 us (6%)
  between operations  0.87 us (1%)
    all_to_all x4, blocking collectives, exchanged(): return lax.all_to_all(blocks, 'kv', 0, 0, tiled=True)  55.4 us
    ppermute x3, starting transfers between devices, other_core(): return lax.ppermute(value, 'tp', [(0, 1), (1, 0)])  4.27 us
    pallas_call x3, Pallas kernels, memory_step(): pl.pallas_call(kernel, out_shape=outs, in_specs=[spec(VMEM)] * (4 + len(s...  4.07 us
    pallas_call x1, Pallas kernels, project(): pl.pallas_call(project_kernel, out_shape=jax.ShapeDtypeStruct((blocks, ro...  2.06 us
  transfers between devices with their start and end apart: 3, of which 0 were waited for; matrix products, arithmetic and copies ran while one was open for 0% of the time, Pallas kernels for 6%

profile of v4, /device:TPU:1, one launch (start us, length us, event | category | flops | bytes accessed | tf_op | source)
XLA Modules:
  0.0 69.7 jit_solution(14719973328171522503)
XLA Ops:
  0.7 2.1 %project.1 = bf16[16,8,3200]{2,1,0:T(8,128)(2,1)S(1)} custom-call(bf16[128,128]{1,0:T(8,128)(2,1)} %tokens.3, f32[1,128]{1,0:T(1,128)} %bitcast.19, bf16[128,512]{1,0:T(8,128)(2,1)} %wq.1, bf16[128,512]{1,0:T(8,128)(2,1)} %wk.1, bf16[128,1024]{1,0:T(8,128)(2,1)} %wv.1, bf16[128,1024]{1,0:T(8,128)(2,1)} %wo.1, bf16[16,2048]{1,0:T(8,128)(2,1)} %bitcast.17), custom_call_target="tpu_custom_call" | custom-call | flops 10000000000 | bytes 10000000 | tf_op jit(solution)/shard_map/project/pallas_call | solution.py:71
  2.8 0.0 copy-start.1
  2.8 0.0 copy-start.2
  2.8 0.0 copy-start.3
  2.8 0.0 copy-start.4
  2.8 22.4 %all_to_all.20.refs_0_ = bf16[16,8,3200]{2,1,0:T(8,128)(2,1)S(1)} all-to-all(bf16[16,8,3200]{2,1,0:T(8,128)(2,1)S(1)} %project.1), channel_id=1, replica_groups=mesh['dp'=4,'kv'=16,'tp'=2] {'kv'}, dimensions={0} | all-to-all | bytes 1638400 | tf_op jit(solution)/shard_map/all_to_all | solution.py:352
  25.2 0.6 state.1
  25.8 0.0 copy-start.5
  25.9 0.0 copy-start.7
  25.9 10.7 %all_to_all.21.heads = bf16[16,8,1024]{2,1,0:T(8,128)(2,1)S(1)} all-to-all(bf16[16,8,1024]{2,1,0:T(8,128)(2,1)S(1)} %get-tuple-element.28), channel_id=1, replica_groups=mesh['dp'=4,'kv'=16,'tp'=2] {'kv'}, dimensions={0} | all-to-all | bytes 524288 | tf_op jit(solution)/shard_map/all_to_all | solution.py:352
  36.6 0.3 branch.1
  36.9 2.7 %collective-permute-start = (bf16[64,128]{1,0:T(8,128)(2,1)S(1)}, bf16[64,128]{1,0:T(8,128)(2,1)S(1)}, u32[]{:S(2)}, u32[]{:S(2)}) collective-permute-start(bf16[64,128]{1,0:T(8,128)(2,1)S(1)} %get-tuple-element.30), channel_id=1, source_target_pairs={{0,1},{1,0},{2,3},{3,2},{4,5},{5,4},{6,7},{7,6},{8,9},{9,8},{10,11... | collective-permute-start | bytes 49160 | tf_op jit(solution)/shard_map/ppermute | solution.py:348
  39.6 1.2 %memory.3 = (f32[8,4,128,256]{3,2,1,0:T(8,128)}, f32[8,4,128]{2,1,0:T(4,128)}, f32[4,8]{1,0:T(4,128)}) custom-call(f32[8,4,128,256]{3,2,1,0:T(8,128)S(1)} %copy-done, f32[8,4,128]{2,1,0:T(4,128)S(1)} %get-tuple-element.46.refs_1_, f32[8,4,128]{2,1,0:T(4,128)S(1)} %get-tuple-element.47.refs_2_, f32[8,4,256]{2,1,0:T(4,128)S(1)} %get-tuple-element.48.refs_3_, ...), custom_call_target="tpu_custom_call" | custom-call | tf_op jit(solution)/shard_map/memory/pallas_call | solution.py:207
  40.9 0.2 residual.1
  41.1 11.5 %all_to_all.22.mine = bf16[16,72,128]{2,1,0:T(8,128)(2,1)S(1)} all-to-all(bf16[16,72,128]{2,1,0:T(8,128)(2,1)S(1)} %get-tuple-element.40), channel_id=1, replica_groups=mesh['dp'=4,'kv'=16,'tp'=2] {'kv'}, dimensions={0} | all-to-all | bytes 589824 | tf_op jit(solution)/shard_map/all_to_all | solution.py:352
  52.5 1.2 %collective-permute-start.1 = (bf16[16,72,128]{2,1,0:T(8,128)(2,1)S(1)}, bf16[16,72,128]{2,1,0:T(8,128)(2,1)S(1)}, u32[]{:S(2)}, u32[]{:S(2)}) collective-permute-start(bf16[16,72,128]{2,1,0:T(8,128)(2,1)S(1)} %all_to_all.22.mine), channel_id=1, source_target_pairs={{0,1},{1,0},{2,3},{3,2},{4,5},{5,4},{6,7},{7,6},{8,9},{9,8},{10,11... | collective-permute-start | bytes 884744 | tf_op jit(solution)/shard_map/ppermute | solution.py:348
  53.7 1.2 %memory.4.after.refs_4_ = f32[8,4,128,256]{3,2,1,0:T(8,128)} custom-call(f32[8,4,128,256]{3,2,1,0:T(8,128)S(1)} %copy-done, f32[8,4,128]{2,1,0:T(4,128)S(1)} %get-tuple-element.46.refs_1_, f32[8,4,128]{2,1,0:T(4,128)S(1)} %get-tuple-element.47.refs_2_, f32[8,4,256]{2,1,0:T(4,128)S(1)} %get-tuple-element.48.refs_3_, ...), custom_call_target="tpu_custom_call", output_to_operand_aliasing={{}: (4, {})} | custom-call | tf_op jit(solution)/shard_map/memory/pallas_call | solution.py:207
  54.9 1.1 %mixer.1 = (bf16[16,64,128]{2,1,0:T(8,128)(2,1)S(1)}, bf16[16,64,128]{2,1,0:T(8,128)(2,1)S(1)}) custom-call(bf16[16,72,128]{2,1,0:T(8,128)(2,1)S(1)} %all_to_all.22.mine, bf16[16,72,128]{2,1,0:T(8,128)(2,1)S(1)} %collective-permute-done.1.other, f32[8,4,128,256]{3,2,1,0:T(8,128)} %memory.4.after.refs_4_, bf16[176,2048]{1,0:T(8,128)(2,1)S(1)} %bitcast.10, ...), custom_call_target="tpu_custom_call" | custom-call | tf_op jit(solution)/shard_map/mixer/pallas_call | solution.py:249
  56.1 0.4 collective-permute-start.2
  56.5 1.6 %memory.5.after = f32[8,4,128,256]{3,2,1,0:T(8,128)} custom-call(f32[8,4,128,256]{3,2,1,0:T(8,128)S(1)} %copy-done, f32[8,4,128]{2,1,0:T(4,128)S(1)} %get-tuple-element.46.refs_1_, f32[8,4,128]{2,1,0:T(4,128)S(1)} %get-tuple-element.47.refs_2_, f32[8,4,256]{2,1,0:T(4,128)S(1)} %get-tuple-element.48.refs_3_, ...), custom_call_target="tpu_custom_call", output_to_operand_aliasing={{}: (4, {})} | custom-call | tf_op jit(solution)/shard_map/memory/pallas_call | solution.py:207
  58.1 0.0 collective-permute-done.2.got
  58.1 0.1 pair.1
  58.1 10.9 %all_to_all.23.recv = bf16[16,64,128]{2,1,0:T(8,128)(2,1)S(1)} all-to-all(bf16[16,64,128]{2,1,0:T(8,128)(2,1)S(1)} %pair.1), channel_id=1, replica_groups=mesh['dp'=4,'kv'=16,'tp'=2] {'kv'}, dimensions={0} | all-to-all | bytes 524288 | tf_op jit(solution)/shard_map/all_to_all | solution.py:352
  69.1 0.6 finish.1
  (18 shorter events, 0.0 us)
Async XLA Ops:
  0.6 24.6 %copy-start = (f32[8,4,128,256]{3,2,1,0:T(8,128)S(1)}, f32[8,4,128,256]{3,2,1,0:T(8,128)}, u32[]{:S(2)}) copy-start(f32[8,4,128,256]{3,2,1,0:T(8,128)} %refs_0_.5) | copy-start | bytes 12582916
  0.6 24.6 %copy-start.6 = (f32[8,4,128]{2,1,0:T(4,128)S(1)}, f32[8,4,128]{2,1,0:T(4,128)}, u32[]{:S(2)}) copy-start(f32[8,4,128]{2,1,0:T(4,128)} %refs_3_.1) | copy-start | bytes 49156
  0.7 24.6 %copy-start.8 = (f32[4,256]{1,0:T(4,128)S(1)}, f32[4,256]{1,0:T(4,128)}, u32[]{:S(2)}) copy-start(f32[4,256]{1,0:T(4,128)} %refs_5_.1) | copy-start | bytes 12292
  0.7 24.6 %copy-start.9 = (f32[8,4]{0,1:T(4,128)S(1)}, f32[8,4]{0,1:T(4,128)}, u32[]{:S(2)}) copy-start(f32[8,4]{0,1:T(4,128)} %param.27) | copy-start | bytes 388
  0.7 24.6 %copy-start.10 = (f32[4]{0:T(128)S(1)}, f32[4]{0:T(128)}, u32[]{:S(2)}) copy-start(f32[4]{0:T(128)} %param.24) | copy-start | bytes 52
  2.8 33.8 %copy-start.1 = (bf16[2048,176]{0,1:T(8,128)(2,1)S(1)}, bf16[2048,176]{0,1:T(8,128)(2,1)}, u32[]{:S(2)}) copy-start(bf16[2048,176]{0,1:T(8,128)(2,1)} %param.31) | copy-start | bytes 2162692
  2.8 33.8 %copy-start.2 = (bf16[2048,176]{0,1:T(8,128)(2,1)S(1)}, bf16[2048,176]{0,1:T(8,128)(2,1)}, u32[]{:S(2)}) copy-start(bf16[2048,176]{0,1:T(8,128)(2,1)} %param.32) | copy-start | bytes 2162692
  2.8 33.8 %copy-start.3 = (bf16[176,2048]{1,0:T(8,128)(2,1)S(1)}, bf16[176,2048]{1,0:T(8,128)(2,1)}, u32[]{:S(2)}) copy-start(bf16[176,2048]{1,0:T(8,128)(2,1)} %wd.3) | copy-start | bytes 2162692
  2.8 33.8 %copy-start.4 = (bf16[1024,128]{1,0:T(8,128)(2,1)S(1)}, bf16[1024,128]{1,0:T(8,128)(2,1)}, u32[]{:S(2)}) copy-start(bf16[1024,128]{1,0:T(8,128)(2,1)} %w_out.1) | copy-start | bytes 786436
  25.8 15.0 %copy-start.5 = (bf16[128,128]{1,0:T(8,128)(2,1)S(1)}, bf16[128,128]{1,0:T(8,128)(2,1)}, u32[]{:S(2)}) copy-start(bf16[128,128]{1,0:T(8,128)(2,1)} %tokens.3) | copy-start | bytes 98308
  25.9 15.0 %copy-start.7 = (f32[2048]{0:T(1024)S(1)}, f32[2048]{0:T(1024)}, u32[]{:S(2)}) copy-start(f32[2048]{0:T(1024)} %param.30) | copy-start | bytes 24580
  36.9 4.0 %collective-permute-start = (bf16[64,128]{1,0:T(8,128)(2,1)S(1)}, bf16[64,128]{1,0:T(8,128)(2,1)S(1)}, u32[]{:S(2)}, u32[]{:S(2)}) collective-permute-start(bf16[64,128]{1,0:T(8,128)(2,1)S(1)} %get-tuple-element.30), channel_id=1, source_target_pairs={{0,1},{1,0},{2,3},{3,2},{4,5},{5,4},{6,7},{7,6},{8,9},{9,8},{10,11... | collective-permute-start | bytes 49160 | tf_op jit(solution)/shard_map/ppermute | solution.py:348
  52.5 2.4 %collective-permute-start.1 = (bf16[16,72,128]{2,1,0:T(8,128)(2,1)S(1)}, bf16[16,72,128]{2,1,0:T(8,128)(2,1)S(1)}, u32[]{:S(2)}, u32[]{:S(2)}) collective-permute-start(bf16[16,72,128]{2,1,0:T(8,128)(2,1)S(1)} %all_to_all.22.mine), channel_id=1, source_target_pairs={{0,1},{1,0},{2,3},{3,2},{4,5},{5,4},{6,7},{7,6},{8,9},{9,8},{10,11... | collective-permute-start | bytes 884744 | tf_op jit(solution)/shard_map/ppermute | solution.py:348
  56.1 2.0 %collective-permute-start.2 = (bf16[16,64,128]{2,1,0:T(8,128)(2,1)S(1)}, bf16[16,64,128]{2,1,0:T(8,128)(2,1)S(1)}, u32[]{:S(2)}, u32[]{:S(2)}) collective-permute-start(bf16[16,64,128]{2,1,0:T(8,128)(2,1)S(1)} %get-tuple-element.45), channel_id=1, source_target_pairs={{0,1},{1,0},{2,3},{3,2},{4,5},{5,4},{6,7},{7,6},{8,9},{9,8},{10,11... | collective-permute-start | bytes 786440 | tf_op jit(solution)/shard_map/ppermute | solution.py:348

commit v5 on v4

--- a/solution.py
+++ b/solution.py
@@ -9,7 +9,6 @@
 VD = 256
 EPSILON = 1e-06
 LANES = 128
-SUBLANES = 8
 F32 = jnp.float32
 BF16 = jnp.bfloat16
 NT = (((1,), (1,)), ((), ()))
@@ -170,12 +169,13 @@
     )(recv, forget_bias[None], memory, normalizer, stabilizer.T, head_gain)
 
 
-def memory_kernel(*refs, first, count, kept):
+def memory_kernel(*refs, first, count, kept, scaled):
     memory, forget, key, value = refs[:4]
     small = refs[4 : 4 + kept]
-    target = refs[-3 - kept]
-    small_out = refs[len(refs) - 2 - kept : len(refs) - 2]
+    gain, *weights = refs[4 + kept : 5 + kept + scaled] if scaled else (None,)
+    outs = refs[-3 - kept - scaled : -2]
     fresh, sems = refs[-2:]
+    target, small_out, scaled_out = outs[0], outs[1 : 1 + kept], outs[1 + kept :]
     seqs = memory.shape[0]
     writes = []
 
@@ -186,52 +186,57 @@
 
     for src, dst in zip(small, small_out):
         send(src, dst)
+    key_cols = {}
     for n in range(count):
-        h = first + n
-        key_cols = key[:, h, :].T
-        for b in range(seqs):
-            decay = forget[b : b + 1, h, :1]
-            fresh[n, b] = decay * memory[b, h] + key_cols[:, b : b + 1] * value[b : b + 1, h, :]
-            if b % 2:
-                send(fresh.at[n, b - 1 : b + 1], target.at[b - 1 : b + 1, h])
+        h, b = divmod(first + n, seqs)
+        if h not in key_cols:
+            key_cols[h] = key[:, h, :].T
+        decay = forget[b : b + 1, h, :1]
+        fresh[n] = decay * memory[b, h] + key_cols[h][:, b : b + 1] * value[b : b + 1, h, :]
+        send(fresh.at[n], target.at[b, h])
+    for src, dst in zip(weights, scaled_out):
+        dst[...] = (src[...].astype(F32) * gain[...]).astype(BF16)
     for write in writes:
         write.wait()
 
 
-def memory_step(memory, forget, key, value, first, count, partial=None, small=()):
+def memory_step(memory, forget, key, value, first, count, partial=None, small=(), gain=None, weights=()):
     def kernel(*refs):
-        memory_kernel(*refs, first=first, count=count, kept=len(small))
-
+        memory_kernel(*refs, first=first, count=count, kept=len(small), scaled=len(weights))
+
+    near = [memory, forget, key, value, *small] + ([gain, *weights] if weights else [])
     extra = [] if partial is None else stay(partial)
     outs = [HBM(memory.shape, F32)] + [HBM(a.shape, F32) for a in small]
-    got = pl.pallas_call(
+    kinds = [spec(HBM)] * len(outs) + [spec(VMEM)] * len(weights)
+    outs += [jax.ShapeDtypeStruct(w.shape, BF16) for w in weights]
+    return pl.pallas_call(
         kernel,
         out_shape=outs,
-        in_specs=[spec(VMEM)] * (4 + len(small)) + [spec(HBM)] * len(extra),
-        out_specs=[spec(HBM)] * len(outs),
-        input_output_aliases={4: 0} if extra else {},
+        in_specs=[spec(VMEM)] * len(near) + [spec(HBM)] * len(extra),
+        out_specs=kinds,
+        input_output_aliases={len(near): 0} if extra else {},
         scratch_shapes=[
-            pltpu.VMEM((count, memory.shape[0]) + memory.shape[2:], F32),
-            pltpu.SemaphoreType.DMA((count * memory.shape[0] // 2 + len(small),)),
+            pltpu.VMEM((count,) + memory.shape[2:], F32),
+            pltpu.SemaphoreType.DMA((count + len(small),)),
         ],
         compiler_params=pltpu.CompilerParams(vmem_limit_bytes=6 << 20),
         cost_estimate=pl.CostEstimate(flops=0, bytes_accessed=0, transcendentals=0),
         name="memory",
-    )(memory, forget, key, value, *small, *extra)
-    return got if small else got[0]
+    )(*near, *extra)
 
 
 def mixer_kernel(mine, other, after, wg, wu, wd, keep, give, mlp):
-    blocks, tall, rows = mine.shape
-    half = keep.shape[1]
+    blocks, half, rows = mine.shape
     cols = 2 * half
     tp = lax.axis_index("tp")
     low = tp == 0
-    square = jnp.zeros((tall - half, rows), F32)
+    square = jnp.zeros((half, rows), F32)
     for j in range(blocks):
-        square = square + (mine[j, half:].astype(F32) + other[j, half:].astype(F32))
-        mlp[pl.ds(pl.multiple_of(j * cols + tp * half, half), half), :] = mine[j, :half]
-        mlp[pl.ds(pl.multiple_of(j * cols + (1 - tp) * half, half), half), :] = other[j, :half]
+        mlp[pl.ds(pl.multiple_of(j * cols + tp * half, half), half), :] = mine[j]
+        mlp[pl.ds(pl.multiple_of(j * cols + (1 - tp) * half, half), half), :] = other[j]
+    for j in range(blocks):
+        here, there = mine[j].astype(F32), other[j].astype(F32)
+        square = square + (here * here + there * there)
     inverse = lax.rsqrt(jnp.sum(square, axis=0, keepdims=True) / (blocks * cols) + EPSILON)
     gate = jnp.dot(wg[...], mlp[...], preferred_element_type=F32) * inverse
     up = jnp.dot(wu[...], mlp[...], preferred_element_type=F32) * inverse
@@ -243,8 +248,8 @@
         give[j] = jnp.where(low, second, first)
 
 
-def mixer(mine, other, after, w_gate, w_up, w_down, half):
-    blocks, _, rows = mine.shape
+def mixer(mine, other, after, gate_rows, up_rows, w_down):
+    blocks, half, rows = mine.shape
     result = jax.ShapeDtypeStruct((blocks, half, rows), BF16)
     return pl.pallas_call(
         mixer_kernel,
@@ -254,7 +259,7 @@
         scratch_shapes=[pltpu.VMEM((2 * blocks * half, rows), BF16)],
         compiler_params=pltpu.CompilerParams(vmem_limit_bytes=16 << 20),
         name="mixer",
-    )(mine, other, *stay(after), w_gate.T, w_up.T, w_down)
+    )(mine, other, *stay(after), gate_rows, up_rows, w_down)
 
 
 def halves(turned):
@@ -298,35 +303,25 @@
     )(keep, got, *stay(after))
 
 
-def residual_kernel(tokens, keep, got, gain, after, spread, own):
-    half, rows = own.shape
+def residual_kernel(tokens, keep, got, after, spread, own):
     mine, _ = halves(tokens[...].astype(F32).T)
-    column, _ = halves(gain[pl.ds(lax.axis_index("kv"), 1), :].T)
     rounded = (mine + (keep[...].astype(F32) + got[...].astype(F32))).astype(BF16)
     own[...] = rounded
-    value = rounded.astype(F32)
-    square = jnp.sum(value * value, axis=0, keepdims=True)
-    coarse = square.astype(BF16).astype(F32)
-    line = lax.broadcasted_iota(jnp.int32, (spread.shape[1] - half, rows), 0)
-    tail = jnp.where(line == 0, coarse, jnp.where(line == 1, square - coarse, 0.0))
-    scaled = (value * column).astype(BF16)
-    spread[:, :half] = jnp.broadcast_to(scaled[None], (spread.shape[0], half, rows))
-    spread[:, half:] = jnp.broadcast_to(tail.astype(BF16)[None], (spread.shape[0],) + tail.shape)
-
-
-def residual_step(tokens, keep, got, mlp_gain, after, blocks):
-    half, rows = keep.shape
+    spread[...] = jnp.broadcast_to(rounded[None], spread.shape)
+
+
+def residual_step(tokens, keep, got, after, blocks):
     return pl.pallas_call(
         residual_kernel,
         out_shape=(
-            jax.ShapeDtypeStruct((blocks, half + SUBLANES, rows), BF16),
+            jax.ShapeDtypeStruct((blocks,) + keep.shape, BF16),
             jax.ShapeDtypeStruct(keep.shape, BF16),
         ),
-        in_specs=[spec(VMEM)] * 4 + [spec(HBM)],
+        in_specs=[spec(VMEM)] * 3 + [spec(HBM)],
         out_specs=[spec(VMEM)] * 2,
         compiler_params=pltpu.CompilerParams(vmem_limit_bytes=4 << 20),
         name="residual",
-    )(tokens, keep, got, mlp_gain.reshape(blocks, 2 * half), *stay(after))
+    )(tokens, keep, got, *stay(after))
 
 
 def finish_kernel(recv, own, out):
@@ -387,15 +382,20 @@
     def behind(value):
         return lax.optimization_barrier((forget, key, value_heads, value))[:3]
 
-    keep, give = branch_step(exchanged(heads), w_out, w_gate.T, w_up.T, w_down)
+    units = memory.shape[0] * memory.shape[1]
+    share = units // 3
+    wg, wu = w_gate.T, w_up.T
+    keep, give = branch_step(exchanged(heads), w_out, wg, wu, w_down)
     part, new_normalizer, new_stabilizer = memory_step(
-        memory, *behind(give), 0, 1, small=(new_normalizer, new_stabilizer)
-    )
-    spread, own = residual_step(tokens, keep, other_core(give), mlp_gain, part, devices)
+        memory, *behind(give), 0, share, small=(new_normalizer, new_stabilizer)
+    )
+    spread, own = residual_step(tokens, keep, other_core(give), part, devices)
     mine = exchanged(spread)
-    part = memory_step(memory, *behind(mine), 1, 1, part)
-    keep, give = mixer(mine, other_core(mine), part, w_gate, w_up, w_down, own.shape[0])
-    new_memory = memory_step(memory, *behind(give), 2, memory.shape[1] - 2, part)
+    part, wg, wu = memory_step(
+        memory, *behind(mine), share, share, part, gain=mlp_gain[None], weights=(wg, wu)
+    )
+    keep, give = mixer(mine, other_core(mine), part, wg, wu, w_down)
+    (new_memory,) = memory_step(memory, *behind(give), 2 * share, units - 2 * share, part)
     pair = pair_step(keep, other_core(give), new_memory)
     mixed_out = finish(exchanged(pair), own).T
     return (mixed_out, new_memory, new_normalizer, new_stabilizer.T)

time: 70 us -> 69.6 us (level)
  no operation moved by 1% of the time
where the time goes in v5:
time: 69.6 us; the launch traced here: 69 us
  blocking collectives  54.8 us (79%)
  Pallas kernels  9.37 us (13%)
  starting transfers between devices  3.97 us (6%)
  between operations  0.85 us (1%)
    all_to_all x4, blocking collectives, exchanged(): return lax.all_to_all(blocks, 'kv', 0, 0, tiled=True)  54.8 us
    pallas_call x3, Pallas kernels, memory_step(): pl.pallas_call(kernel, out_shape=outs, in_specs=[spec(VMEM)] * len(near)...  4.44 us
    ppermute x3, starting transfers between devices, other_core(): return lax.ppermute(value, 'tp', [(0, 1), (1, 0)])  3.97 us
    pallas_call x1, Pallas kernels, project(): pl.pallas_call(project_kernel, out_shape=jax.ShapeDtypeStruct((blocks, ro...  2.06 us
  transfers between devices with their start and end apart: 3, of which 0 were waited for; matrix products, arithmetic and copies ran while one was open for 0% of the time, Pallas kernels for 6%

profile of v5, /device:TPU:1, one launch (start us, length us, event | category | flops | bytes accessed | tf_op | source)
XLA Modules:
  0.0 69.0 jit_solution(2623272639744586917)
XLA Ops:
  0.7 2.1 %project.1 = bf16[16,8,3200]{2,1,0:T(8,128)(2,1)S(1)} custom-call(bf16[128,128]{1,0:T(8,128)(2,1)} %tokens.3, f32[1,128]{1,0:T(1,128)} %bitcast.19, bf16[128,512]{1,0:T(8,128)(2,1)} %wq.1, bf16[128,512]{1,0:T(8,128)(2,1)} %wk.1, bf16[128,1024]{1,0:T(8,128)(2,1)} %wv.1, bf16[128,1024]{1,0:T(8,128)(2,1)} %wo.1, bf16[16,2048]{1,0:T(8,128)(2,1)} %bitcast.17), custom_call_target="tpu_custom_call" | custom-call | flops 10000000000 | bytes 10000000 | tf_op jit(solution)/shard_map/project/pallas_call | solution.py:70
  2.8 0.0 copy-start.1
  2.8 0.0 copy-start.2
  2.8 0.0 copy-start.3
  2.8 0.0 copy-start.4
  2.8 22.4 %all_to_all.20.refs_0_ = bf16[16,8,3200]{2,1,0:T(8,128)(2,1)S(1)} all-to-all(bf16[16,8,3200]{2,1,0:T(8,128)(2,1)S(1)} %project.1), channel_id=1, replica_groups=mesh['dp'=4,'kv'=16,'tp'=2] {'kv'}, dimensions={0} | all-to-all | bytes 1638400 | tf_op jit(solution)/shard_map/all_to_all | solution.py:347
  25.2 0.6 state.1
  25.8 0.0 copy-start.5
  25.9 10.7 %all_to_all.21.heads = bf16[16,8,1024]{2,1,0:T(8,128)(2,1)S(1)} all-to-all(bf16[16,8,1024]{2,1,0:T(8,128)(2,1)S(1)} %get-tuple-element.31), channel_id=1, replica_groups=mesh['dp'=4,'kv'=16,'tp'=2] {'kv'}, dimensions={0} | all-to-all | bytes 524288 | tf_op jit(solution)/shard_map/all_to_all | solution.py:347
  36.5 0.3 branch.1
  36.8 2.7 %collective-permute-start = (bf16[64,128]{1,0:T(8,128)(2,1)S(1)}, bf16[64,128]{1,0:T(8,128)(2,1)S(1)}, u32[]{:S(2)}, u32[]{:S(2)}) collective-permute-start(bf16[64,128]{1,0:T(8,128)(2,1)S(1)} %get-tuple-element.33), channel_id=1, source_target_pairs={{0,1},{1,0},{2,3},{3,2},{4,5},{5,4},{6,7},{7,6},{8,9},{9,8},{10,11... | collective-permute-start | bytes 49160 | tf_op jit(solution)/shard_map/ppermute | solution.py:343
  39.6 1.4 %memory.3 = (f32[8,4,128,256]{3,2,1,0:T(8,128)}, f32[8,4,128]{2,1,0:T(4,128)}, f32[4,8]{1,0:T(4,128)}) custom-call(f32[8,4,128,256]{3,2,1,0:T(8,128)S(1)} %copy-done, f32[8,4,128]{2,1,0:T(4,128)S(1)} %get-tuple-element.52.refs_1_, f32[8,4,128]{2,1,0:T(4,128)S(1)} %get-tuple-element.53.refs_2_, f32[8,4,256]{2,1,0:T(4,128)S(1)} %get-tuple-element.54.refs_3_, ...), custom_call_target="tpu_custom_call" | custom-call | tf_op jit(solution)/shard_map/memory/pallas_call | solution.py:212
  41.0 0.0 collective-permute-done.got
  41.0 0.1 residual.1
  41.2 11.1 %all_to_all.22.mine = bf16[16,64,128]{2,1,0:T(8,128)(2,1)S(1)} all-to-all(bf16[16,64,128]{2,1,0:T(8,128)(2,1)S(1)} %get-tuple-element.43), channel_id=1, replica_groups=mesh['dp'=4,'kv'=16,'tp'=2] {'kv'}, dimensions={0} | all-to-all | bytes 524288 | tf_op jit(solution)/shard_map/all_to_all | solution.py:347
  52.3 1.2 %collective-permute-start.1 = (bf16[16,64,128]{2,1,0:T(8,128)(2,1)S(1)}, bf16[16,64,128]{2,1,0:T(8,128)(2,1)S(1)}, u32[]{:S(2)}, u32[]{:S(2)}) collective-permute-start(bf16[16,64,128]{2,1,0:T(8,128)(2,1)S(1)} %all_to_all.22.mine), channel_id=1, source_target_pairs={{0,1},{1,0},{2,3},{3,2},{4,5},{5,4},{6,7},{7,6},{8,9},{9,8},{10,11... | collective-permute-start | bytes 786440 | tf_op jit(solution)/shard_map/ppermute | solution.py:343
  53.4 1.5 %memory.4 = (f32[8,4,128,256]{3,2,1,0:T(8,128)}, bf16[176,2048]{1,0:T(8,128)(2,1)S(1)}, bf16[176,2048]{1,0:T(8,128)(2,1)S(1)}) custom-call(f32[8,4,128,256]{3,2,1,0:T(8,128)S(1)} %copy-done, f32[8,4,128]{2,1,0:T(4,128)S(1)} %get-tuple-element.52.refs_1_, f32[8,4,128]{2,1,0:T(4,128)S(1)} %get-tuple-element.53.refs_2_, ...), custom_call_target="tpu_custom_call", output_to_operand_aliasing={{0}: (7, {})} | custom-call | tf_op jit(solution)/shard_map/memory/pallas_call | solution.py:212
  54.9 1.2 %mixer.1 = (bf16[16,64,128]{2,1,0:T(8,128)(2,1)S(1)}, bf16[16,64,128]{2,1,0:T(8,128)(2,1)S(1)}) custom-call(bf16[16,64,128]{2,1,0:T(8,128)(2,1)S(1)} %all_to_all.22.mine, bf16[16,64,128]{2,1,0:T(8,128)(2,1)S(1)} %collective-permute-done.1.other, f32[8,4,128,256]{3,2,1,0:T(8,128)} %get-tuple-element.47.after.refs_4_, ...), custom_call_target="tpu_custom_call" | custom-call | tf_op jit(solution)/shard_map/mixer/pallas_call | solution.py:254
  56.1 0.1 collective-permute-start.2
  56.2 1.5 %memory.5.after = f32[8,4,128,256]{3,2,1,0:T(8,128)} custom-call(f32[8,4,128,256]{3,2,1,0:T(8,128)S(1)} %copy-done, f32[8,4,128]{2,1,0:T(4,128)S(1)} %get-tuple-element.52.refs_1_, f32[8,4,128]{2,1,0:T(4,128)S(1)} %get-tuple-element.53.refs_2_, f32[8,4,256]{2,1,0:T(4,128)S(1)} %get-tuple-element.54.refs_3_, ...), custom_call_target="tpu_custom_call", output_to_operand_aliasing={{}: (4, {})} | custom-call | tf_op jit(solution)/shard_map/memory/pallas_call | solution.py:212
  57.7 0.0 collective-permute-done.2.got
  57.7 0.1 pair.1
  57.8 10.6 %all_to_all.23.recv = bf16[16,64,128]{2,1,0:T(8,128)(2,1)S(1)} all-to-all(bf16[16,64,128]{2,1,0:T(8,128)(2,1)S(1)} %pair.1), channel_id=1, replica_groups=mesh['dp'=4,'kv'=16,'tp'=2] {'kv'}, dimensions={0} | all-to-all | bytes 524288 | tf_op jit(solution)/shard_map/all_to_all | solution.py:347
  68.4 0.6 finish.1
  (18 shorter events, 0.0 us)
Async XLA Ops:
  0.6 24.6 %copy-start = (f32[8,4,128,256]{3,2,1,0:T(8,128)S(1)}, f32[8,4,128,256]{3,2,1,0:T(8,128)}, u32[]{:S(2)}) copy-start(f32[8,4,128,256]{3,2,1,0:T(8,128)} %refs_0_.5) | copy-start | bytes 12582916
  0.6 24.6 %copy-start.6 = (f32[8,4,128]{2,1,0:T(4,128)S(1)}, f32[8,4,128]{2,1,0:T(4,128)}, u32[]{:S(2)}) copy-start(f32[8,4,128]{2,1,0:T(4,128)} %refs_3_.1) | copy-start | bytes 49156
  0.7 24.6 %copy-start.8 = (f32[4,256]{1,0:T(4,128)S(1)}, f32[4,256]{1,0:T(4,128)}, u32[]{:S(2)}) copy-start(f32[4,256]{1,0:T(4,128)} %refs_5_.1) | copy-start | bytes 12292
  0.7 24.6 %copy-start.9 = (f32[8,4]{0,1:T(4,128)S(1)}, f32[8,4]{0,1:T(4,128)}, u32[]{:S(2)}) copy-start(f32[8,4]{0,1:T(4,128)} %param.27) | copy-start | bytes 388
  0.7 24.6 %copy-start.10 = (f32[4]{0:T(128)S(1)}, f32[4]{0:T(128)}, u32[]{:S(2)}) copy-start(f32[4]{0:T(128)} %param.24) | copy-start | bytes 52
  2.8 33.8 %copy-start.1 = (bf16[2048,176]{0,1:T(8,128)(2,1)S(1)}, bf16[2048,176]{0,1:T(8,128)(2,1)}, u32[]{:S(2)}) copy-start(bf16[2048,176]{0,1:T(8,128)(2,1)} %param.31) | copy-start | bytes 2162692
  2.8 33.8 %copy-start.2 = (bf16[2048,176]{0,1:T(8,128)(2,1)S(1)}, bf16[2048,176]{0,1:T(8,128)(2,1)}, u32[]{:S(2)}) copy-start(bf16[2048,176]{0,1:T(8,128)(2,1)} %param.32) | copy-start | bytes 2162692
  2.8 33.8 %copy-start.3 = (bf16[176,2048]{1,0:T(8,128)(2,1)S(1)}, bf16[176,2048]{1,0:T(8,128)(2,1)}, u32[]{:S(2)}) copy-start(bf16[176,2048]{1,0:T(8,128)(2,1)} %wd.3) | copy-start | bytes 2162692
  2.8 33.8 %copy-start.4 = (bf16[1024,128]{1,0:T(8,128)(2,1)S(1)}, bf16[1024,128]{1,0:T(8,128)(2,1)}, u32[]{:S(2)}) copy-start(bf16[1024,128]{1,0:T(8,128)(2,1)} %w_out.1) | copy-start | bytes 786436
  25.8 15.2 %copy-start.5 = (bf16[128,128]{1,0:T(8,128)(2,1)S(1)}, bf16[128,128]{1,0:T(8,128)(2,1)}, u32[]{:S(2)}) copy-start(bf16[128,128]{1,0:T(8,128)(2,1)} %tokens.3) | copy-start | bytes 98308
  36.8 4.2 %collective-permute-start = (bf16[64,128]{1,0:T(8,128)(2,1)S(1)}, bf16[64,128]{1,0:T(8,128)(2,1)S(1)}, u32[]{:S(2)}, u32[]{:S(2)}) collective-permute-start(bf16[64,128]{1,0:T(8,128)(2,1)S(1)} %get-tuple-element.33), channel_id=1, source_target_pairs={{0,1},{1,0},{2,3},{3,2},{4,5},{5,4},{6,7},{7,6},{8,9},{9,8},{10,11... | collective-permute-start | bytes 49160 | tf_op jit(solution)/shard_map/ppermute | solution.py:343
  39.6 13.9 %copy-start.7 = (f32[2048]{0:T(1024)S(1)}, f32[2048]{0:T(1024)}, u32[]{:S(2)}) copy-start(f32[2048]{0:T(1024)} %param.30) | copy-start | bytes 24580
  52.3 2.7 %collective-permute-start.1 = (bf16[16,64,128]{2,1,0:T(8,128)(2,1)S(1)}, bf16[16,64,128]{2,1,0:T(8,128)(2,1)S(1)}, u32[]{:S(2)}, u32[]{:S(2)}) collective-permute-start(bf16[16,64,128]{2,1,0:T(8,128)(2,1)S(1)} %all_to_all.22.mine), channel_id=1, source_target_pairs={{0,1},{1,0},{2,3},{3,2},{4,5},{5,4},{6,7},{7,6},{8,9},{9,8},{10,11... | collective-permute-start | bytes 786440 | tf_op jit(solution)/shard_map/ppermute | solution.py:343
  56.1 1.6 %collective-permute-start.2 = (bf16[16,64,128]{2,1,0:T(8,128)(2,1)S(1)}, bf16[16,64,128]{2,1,0:T(8,128)(2,1)S(1)}, u32[]{:S(2)}, u32[]{:S(2)}) collective-permute-start(bf16[16,64,128]{2,1,0:T(8,128)(2,1)S(1)} %get-tuple-element.51), channel_id=1, source_target_pairs={{0,1},{1,0},{2,3},{3,2},{4,5},{5,4},{6,7},{7,6},{8,9},{9,8},{10,11... | collective-permute-start | bytes 786440 | tf_op jit(solution)/shard_map/ppermute | solution.py:343

commit v6 on v5

--- a/solution.py
+++ b/solution.py
@@ -50,12 +50,12 @@
         width = value.shape[1]
         out[:, :, at : at + width] = value.reshape(blocks, rows, width).astype(BF16)
 
+    for copy in copies[2:]:
+        copy.wait()
     at = 0
-    for n, buf in ((2, bq), (3, bk), (5, bv), (6, bo)):
-        copies[n].wait()
+    for buf in (bq, bk, bv, bo):
         put(jnp.dot(scaled, buf[...], preferred_element_type=F32), at)
         at += buf.shape[1]
-    copies[4].wait()
     gate_count = bg.shape[0]
     wide = jnp.concatenate([bg[...].astype(F32), jnp.zeros((LANES - gate_count, cols), F32)], axis=0)
     gates = lax.dot_general(scaled, wide.astype(BF16), NT, preferred_element_type=F32)
@@ -384,18 +384,19 @@
 
     units = memory.shape[0] * memory.shape[1]
     share = units // 3
+    early = units // 4
     wg, wu = w_gate.T, w_up.T
     keep, give = branch_step(exchanged(heads), w_out, wg, wu, w_down)
     part, new_normalizer, new_stabilizer = memory_step(
-        memory, *behind(give), 0, share, small=(new_normalizer, new_stabilizer)
+        memory, *behind(give), 0, early, small=(new_normalizer, new_stabilizer)
     )
     spread, own = residual_step(tokens, keep, other_core(give), part, devices)
     mine = exchanged(spread)
     part, wg, wu = memory_step(
-        memory, *behind(mine), share, share, part, gain=mlp_gain[None], weights=(wg, wu)
+        memory, *behind(mine), early, share, part, gain=mlp_gain[None], weights=(wg, wu)
     )
     keep, give = mixer(mine, other_core(mine), part, wg, wu, w_down)
-    (new_memory,) = memory_step(memory, *behind(give), 2 * share, units - 2 * share, part)
+    (new_memory,) = memory_step(memory, *behind(give), early + share, units - early - share, part)
     pair = pair_step(keep, other_core(give), new_memory)
     mixed_out = finish(exchanged(pair), own).T
     return (mixed_out, new_memory, new_normalizer, new_stabilizer.T)

time: 69.6 us -> 69.2 us (level)
  no operation moved by 1% of the time
where the time goes in v6:
time: 69.2 us; the launch traced here: 68.7 us
  blocking collectives  54.8 us (79%)
  Pallas kernels  8.9 us (13%)
  starting transfers between devices  4.03 us (6%)
  between operations  0.85 us (1%)
    all_to_all x4, blocking collectives, exchanged(): return lax.all_to_all(blocks, 'kv', 0, 0, tiled=True)  54.8 us
    pallas_call x3, Pallas kernels, memory_step(): pl.pallas_call(kernel, out_shape=outs, in_specs=[spec(VMEM)] * len(near)...  4.28 us
    ppermute x3, starting transfers between devices, other_core(): return lax.ppermute(value, 'tp', [(0, 1), (1, 0)])  4.03 us
    pallas_call x1, Pallas kernels, project(): pl.pallas_call(project_kernel, out_shape=jax.ShapeDtypeStruct((blocks, ro...  1.77 us
  transfers between devices with their start and end apart: 3, of which 0 were waited for; matrix products, arithmetic and copies ran while one was open for 0% of the time, Pallas kernels for 6%

profile of v6, /device:TPU:1, one launch (start us, length us, event | category | flops | bytes accessed | tf_op | source)
XLA Modules:
  0.0 68.7 jit_solution(13774816837476938226)
XLA Ops:
  0.7 1.8 %project.1 = bf16[16,8,3200]{2,1,0:T(8,128)(2,1)S(1)} custom-call(bf16[128,128]{1,0:T(8,128)(2,1)} %tokens.3, f32[1,128]{1,0:T(1,128)} %bitcast.19, bf16[128,512]{1,0:T(8,128)(2,1)} %wq.1, bf16[128,512]{1,0:T(8,128)(2,1)} %wk.1, bf16[128,1024]{1,0:T(8,128)(2,1)} %wv.1, bf16[128,1024]{1,0:T(8,128)(2,1)} %wo.1, bf16[16,2048]{1,0:T(8,128)(2,1)} %bitcast.17), custom_call_target="tpu_custom_call" | custom-call | flops 10000000000 | bytes 10000000 | tf_op jit(solution)/shard_map/project/pallas_call | solution.py:70
  2.5 0.0 copy-start.1
  2.5 0.0 copy-start.2
  2.5 0.0 copy-start.3
  2.5 0.0 copy-start.4
  2.5 22.4 %all_to_all.20.refs_0_ = bf16[16,8,3200]{2,1,0:T(8,128)(2,1)S(1)} all-to-all(bf16[16,8,3200]{2,1,0:T(8,128)(2,1)S(1)} %project.1), channel_id=1, replica_groups=mesh['dp'=4,'kv'=16,'tp'=2] {'kv'}, dimensions={0} | all-to-all | bytes 1638400 | tf_op jit(solution)/shard_map/all_to_all | solution.py:347
  24.9 0.6 state.1
  25.5 0.0 copy-start.5
  25.6 10.7 %all_to_all.21.heads = bf16[16,8,1024]{2,1,0:T(8,128)(2,1)S(1)} all-to-all(bf16[16,8,1024]{2,1,0:T(8,128)(2,1)S(1)} %get-tuple-element.31), channel_id=1, replica_groups=mesh['dp'=4,'kv'=16,'tp'=2] {'kv'}, dimensions={0} | all-to-all | bytes 524288 | tf_op jit(solution)/shard_map/all_to_all | solution.py:347
  36.3 0.3 branch.1
  36.5 2.7 %collective-permute-start = (bf16[64,128]{1,0:T(8,128)(2,1)S(1)}, bf16[64,128]{1,0:T(8,128)(2,1)S(1)}, u32[]{:S(2)}, u32[]{:S(2)}) collective-permute-start(bf16[64,128]{1,0:T(8,128)(2,1)S(1)} %get-tuple-element.33), channel_id=1, source_target_pairs={{0,1},{1,0},{2,3},{3,2},{4,5},{5,4},{6,7},{7,6},{8,9},{9,8},{10,11... | collective-permute-start | bytes 49160 | tf_op jit(solution)/shard_map/ppermute | solution.py:343
  39.3 1.3 %memory.3 = (f32[8,4,128,256]{3,2,1,0:T(8,128)}, f32[8,4,128]{2,1,0:T(4,128)}, f32[4,8]{1,0:T(4,128)}) custom-call(f32[8,4,128,256]{3,2,1,0:T(8,128)S(1)} %copy-done, f32[8,4,128]{2,1,0:T(4,128)S(1)} %get-tuple-element.52.refs_1_, f32[8,4,128]{2,1,0:T(4,128)S(1)} %get-tuple-element.53.refs_2_, f32[8,4,256]{2,1,0:T(4,128)S(1)} %get-tuple-element.54.refs_3_, ...), custom_call_target="tpu_custom_call" | custom-call | tf_op jit(solution)/shard_map/memory/pallas_call | solution.py:212
  40.6 0.0 collective-permute-done.got
  40.6 0.1 residual.1
  40.7 11.1 %all_to_all.22.mine = bf16[16,64,128]{2,1,0:T(8,128)(2,1)S(1)} all-to-all(bf16[16,64,128]{2,1,0:T(8,128)(2,1)S(1)} %get-tuple-element.43), channel_id=1, replica_groups=mesh['dp'=4,'kv'=16,'tp'=2] {'kv'}, dimensions={0} | all-to-all | bytes 524288 | tf_op jit(solution)/shard_map/all_to_all | solution.py:347
  51.8 1.2 %collective-permute-start.1 = (bf16[16,64,128]{2,1,0:T(8,128)(2,1)S(1)}, bf16[16,64,128]{2,1,0:T(8,128)(2,1)S(1)}, u32[]{:S(2)}, u32[]{:S(2)}) collective-permute-start(bf16[16,64,128]{2,1,0:T(8,128)(2,1)S(1)} %all_to_all.22.mine), channel_id=1, source_target_pairs={{0,1},{1,0},{2,3},{3,2},{4,5},{5,4},{6,7},{7,6},{8,9},{9,8},{10,11... | collective-permute-start | bytes 786440 | tf_op jit(solution)/shard_map/ppermute | solution.py:343
  53.0 1.4 %memory.4 = (f32[8,4,128,256]{3,2,1,0:T(8,128)}, bf16[176,2048]{1,0:T(8,128)(2,1)S(1)}, bf16[176,2048]{1,0:T(8,128)(2,1)S(1)}) custom-call(f32[8,4,128,256]{3,2,1,0:T(8,128)S(1)} %copy-done, f32[8,4,128]{2,1,0:T(4,128)S(1)} %get-tuple-element.52.refs_1_, f32[8,4,128]{2,1,0:T(4,128)S(1)} %get-tuple-element.53.refs_2_, ...), custom_call_target="tpu_custom_call", output_to_operand_aliasing={{0}: (7, {})} | custom-call | tf_op jit(solution)/shard_map/memory/pallas_call | solution.py:212
  54.4 1.1 %mixer.1 = (bf16[16,64,128]{2,1,0:T(8,128)(2,1)S(1)}, bf16[16,64,128]{2,1,0:T(8,128)(2,1)S(1)}) custom-call(bf16[16,64,128]{2,1,0:T(8,128)(2,1)S(1)} %all_to_all.22.mine, bf16[16,64,128]{2,1,0:T(8,128)(2,1)S(1)} %collective-permute-done.1.other, f32[8,4,128,256]{3,2,1,0:T(8,128)} %get-tuple-element.47.after.refs_4_, ...), custom_call_target="tpu_custom_call" | custom-call | tf_op jit(solution)/shard_map/mixer/pallas_call | solution.py:254
  55.6 0.1 collective-permute-start.2
  55.7 1.6 %memory.5.after = f32[8,4,128,256]{3,2,1,0:T(8,128)} custom-call(f32[8,4,128,256]{3,2,1,0:T(8,128)S(1)} %copy-done, f32[8,4,128]{2,1,0:T(4,128)S(1)} %get-tuple-element.52.refs_1_, f32[8,4,128]{2,1,0:T(4,128)S(1)} %get-tuple-element.53.refs_2_, f32[8,4,256]{2,1,0:T(4,128)S(1)} %get-tuple-element.54.refs_3_, ...), custom_call_target="tpu_custom_call", output_to_operand_aliasing={{}: (4, {})} | custom-call | tf_op jit(solution)/shard_map/memory/pallas_call | solution.py:212
  57.3 0.0 collective-permute-done.2.got
  57.3 0.1 pair.1
  57.4 10.7 %all_to_all.23.recv = bf16[16,64,128]{2,1,0:T(8,128)(2,1)S(1)} all-to-all(bf16[16,64,128]{2,1,0:T(8,128)(2,1)S(1)} %pair.1), channel_id=1, replica_groups=mesh['dp'=4,'kv'=16,'tp'=2] {'kv'}, dimensions={0} | all-to-all | bytes 524288 | tf_op jit(solution)/shard_map/all_to_all | solution.py:347
  68.0 0.6 finish.1
  (18 shorter events, 0.0 us)
Async XLA Ops:
  0.6 24.3 %copy-start = (f32[8,4,128,256]{3,2,1,0:T(8,128)S(1)}, f32[8,4,128,256]{3,2,1,0:T(8,128)}, u32[]{:S(2)}) copy-start(f32[8,4,128,256]{3,2,1,0:T(8,128)} %refs_0_.5) | copy-start | bytes 12582916
  0.6 24.3 %copy-start.6 = (f32[8,4,128]{2,1,0:T(4,128)S(1)}, f32[8,4,128]{2,1,0:T(4,128)}, u32[]{:S(2)}) copy-start(f32[8,4,128]{2,1,0:T(4,128)} %refs_3_.1) | copy-start | bytes 49156
  0.7 24.3 %copy-start.8 = (f32[4,256]{1,0:T(4,128)S(1)}, f32[4,256]{1,0:T(4,128)}, u32[]{:S(2)}) copy-start(f32[4,256]{1,0:T(4,128)} %refs_5_.1) | copy-start | bytes 12292
  0.7 24.3 %copy-start.9 = (f32[8,4]{0,1:T(4,128)S(1)}, f32[8,4]{0,1:T(4,128)}, u32[]{:S(2)}) copy-start(f32[8,4]{0,1:T(4,128)} %param.27) | copy-start | bytes 388
  0.7 24.3 %copy-start.10 = (f32[4]{0:T(128)S(1)}, f32[4]{0:T(128)}, u32[]{:S(2)}) copy-start(f32[4]{0:T(128)} %param.24) | copy-start | bytes 52
  2.5 33.8 %copy-start.1 = (bf16[2048,176]{0,1:T(8,128)(2,1)S(1)}, bf16[2048,176]{0,1:T(8,128)(2,1)}, u32[]{:S(2)}) copy-start(bf16[2048,176]{0,1:T(8,128)(2,1)} %param.31) | copy-start | bytes 2162692
  2.5 33.8 %copy-start.2 = (bf16[2048,176]{0,1:T(8,128)(2,1)S(1)}, bf16[2048,176]{0,1:T(8,128)(2,1)}, u32[]{:S(2)}) copy-start(bf16[2048,176]{0,1:T(8,128)(2,1)} %param.32) | copy-start | bytes 2162692
  2.5 33.8 %copy-start.3 = (bf16[176,2048]{1,0:T(8,128)(2,1)S(1)}, bf16[176,2048]{1,0:T(8,128)(2,1)}, u32[]{:S(2)}) copy-start(bf16[176,2048]{1,0:T(8,128)(2,1)} %wd.3) | copy-start | bytes 2162692
  2.5 33.8 %copy-start.4 = (bf16[1024,128]{1,0:T(8,128)(2,1)S(1)}, bf16[1024,128]{1,0:T(8,128)(2,1)}, u32[]{:S(2)}) copy-start(bf16[1024,128]{1,0:T(8,128)(2,1)} %w_out.1) | copy-start | bytes 786436
  25.5 15.0 %copy-start.5 = (bf16[128,128]{1,0:T(8,128)(2,1)S(1)}, bf16[128,128]{1,0:T(8,128)(2,1)}, u32[]{:S(2)}) copy-start(bf16[128,128]{1,0:T(8,128)(2,1)} %tokens.3) | copy-start | bytes 98308
  36.5 4.0 %collective-permute-start = (bf16[64,128]{1,0:T(8,128)(2,1)S(1)}, bf16[64,128]{1,0:T(8,128)(2,1)S(1)}, u32[]{:S(2)}, u32[]{:S(2)}) collective-permute-start(bf16[64,128]{1,0:T(8,128)(2,1)S(1)} %get-tuple-element.33), channel_id=1, source_target_pairs={{0,1},{1,0},{2,3},{3,2},{4,5},{5,4},{6,7},{7,6},{8,9},{9,8},{10,11... | collective-permute-start | bytes 49160 | tf_op jit(solution)/shard_map/ppermute | solution.py:343
  39.3 13.7 %copy-start.7 = (f32[2048]{0:T(1024)S(1)}, f32[2048]{0:T(1024)}, u32[]{:S(2)}) copy-start(f32[2048]{0:T(1024)} %param.30) | copy-start | bytes 24580
  51.8 2.6 %collective-permute-start.1 = (bf16[16,64,128]{2,1,0:T(8,128)(2,1)S(1)}, bf16[16,64,128]{2,1,0:T(8,128)(2,1)S(1)}, u32[]{:S(2)}, u32[]{:S(2)}) collective-permute-start(bf16[16,64,128]{2,1,0:T(8,128)(2,1)S(1)} %all_to_all.22.mine), channel_id=1, source_target_pairs={{0,1},{1,0},{2,3},{3,2},{4,5},{5,4},{6,7},{7,6},{8,9},{9,8},{10,11... | collective-permute-start | bytes 786440 | tf_op jit(solution)/shard_map/ppermute | solution.py:343
  55.6 1.7 %collective-permute-start.2 = (bf16[16,64,128]{2,1,0:T(8,128)(2,1)S(1)}, bf16[16,64,128]{2,1,0:T(8,128)(2,1)S(1)}, u32[]{:S(2)}, u32[]{:S(2)}) collective-permute-start(bf16[16,64,128]{2,1,0:T(8,128)(2,1)S(1)} %get-tuple-element.51), channel_id=1, source_target_pairs={{0,1},{1,0},{2,3},{3,2},{4,5},{5,4},{6,7},{7,6},{8,9},{9,8},{10,11... | collective-permute-start | bytes 786440 | tf_op jit(solution)/shard_map/ppermute | solution.py:343

commit v7 on v6

--- a/solution.py
+++ b/solution.py
@@ -169,13 +169,63 @@
     )(recv, forget_bias[None], memory, normalizer, stabilizer.T, head_gain)
 
 
-def memory_kernel(*refs, first, count, kept, scaled):
+def split_job(gain, wg, wu, gate_sets, up_sets):
+    half = LANES // 2
+    low = lax.broadcasted_iota(jnp.int32, (wg.shape[0], LANES), 1) < half
+    for src, dst in ((wg, gate_sets), (wu, up_sets)):
+        for at in range(0, src.shape[1], 2 * LANES):
+            one, two = (
+                (src[:, lo : lo + LANES].astype(F32) * gain[:, lo : lo + LANES]).astype(BF16)
+                for lo in (at, at + LANES)
+            )
+            first = jnp.where(low, one, pltpu.roll(two, half, 1))
+            second = jnp.where(low, pltpu.roll(one, half, 1), two)
+            dst[0, :, at // 2 : at // 2 + LANES] = first
+            dst[1, :, at // 2 : at // 2 + LANES] = second
+
+
+def partial_sums(rows_ref, gate_sets, up_sets, side):
+    blocks, half, rows = rows_ref.shape
+    square = jnp.zeros((half, rows), F32)
+    for j in range(blocks):
+        value = rows_ref[j].astype(F32)
+        square = square + value * value
+    flat = rows_ref[...].reshape(blocks * half, rows)
+    gate = jnp.dot(gate_sets[side], flat, preferred_element_type=F32)
+    up = jnp.dot(up_sets[side], flat, preferred_element_type=F32)
+    return gate, up, square
+
+
+def near_job(wd, mine, gate_sets, up_sets, turned, gate, up, square):
+    turn_job(wd, turned)
+    gate[...], up[...], square[...] = partial_sums(mine, gate_sets, up_sets, lax.axis_index("tp"))
+
+
+def turn_job(wd, turned):
+    cols = turned.shape[1]
+    for j in range(turned.shape[0]):
+        turned[j] = wd[:, j * cols : (j + 1) * cols].T
+
+
+def down_half(turned, hidden, out, side):
+    blocks, half, rows = out.shape
+    at = pl.multiple_of(side * half, half)
+    for j in range(blocks):
+        part = jnp.dot(turned[j, pl.ds(at, half), :], hidden, preferred_element_type=F32)
+        out[j] = part.astype(BF16)
+
+
+def keep_job(turned, hidden, keep):
+    down_half(turned, hidden[...], keep, lax.axis_index("tp"))
+
+
+def memory_kernel(*refs, first, count, kept, job, reads):
     memory, forget, key, value = refs[:4]
     small = refs[4 : 4 + kept]
-    gain, *weights = refs[4 + kept : 5 + kept + scaled] if scaled else (None,)
-    outs = refs[-3 - kept - scaled : -2]
     fresh, sems = refs[-2:]
-    target, small_out, scaled_out = outs[0], outs[1 : 1 + kept], outs[1 + kept :]
+    made = len(refs) - 2 - reads[1]
+    outs = refs[made - 1 - kept : made]
+    target, small_out = outs[0], outs[1:]
     seqs = memory.shape[0]
     writes = []
 
@@ -194,21 +244,22 @@
         decay = forget[b : b + 1, h, :1]
         fresh[n] = decay * memory[b, h] + key_cols[h][:, b : b + 1] * value[b : b + 1, h, :]
         send(fresh.at[n], target.at[b, h])
-    for src, dst in zip(weights, scaled_out):
-        dst[...] = (src[...].astype(F32) * gain[...]).astype(BF16)
+    job(*refs[4 + kept : 4 + kept + reads[0]], *refs[made:-2])
     for write in writes:
         write.wait()
 
 
-def memory_step(memory, forget, key, value, first, count, partial=None, small=(), gain=None, weights=()):
+def memory_step(memory, forget, key, value, first, count, job, needs, makes, partial=None, small=()):
     def kernel(*refs):
-        memory_kernel(*refs, first=first, count=count, kept=len(small), scaled=len(weights))
-
-    near = [memory, forget, key, value, *small] + ([gain, *weights] if weights else [])
+        memory_kernel(
+            *refs, first=first, count=count, kept=len(small), job=job, reads=(len(needs), len(makes))
+        )
+
+    near = [memory, forget, key, value, *small, *needs]
     extra = [] if partial is None else stay(partial)
     outs = [HBM(memory.shape, F32)] + [HBM(a.shape, F32) for a in small]
-    kinds = [spec(HBM)] * len(outs) + [spec(VMEM)] * len(weights)
-    outs += [jax.ShapeDtypeStruct(w.shape, BF16) for w in weights]
+    kinds = [spec(HBM)] * len(outs) + [spec(VMEM)] * len(makes)
+    outs += [jax.ShapeDtypeStruct(shape, kind) for shape, kind in makes]
     return pl.pallas_call(
         kernel,
         out_shape=outs,
@@ -219,47 +270,38 @@
             pltpu.VMEM((count,) + memory.shape[2:], F32),
             pltpu.SemaphoreType.DMA((count + len(small),)),
         ],
-        compiler_params=pltpu.CompilerParams(vmem_limit_bytes=6 << 20),
+        compiler_params=pltpu.CompilerParams(vmem_limit_bytes=8 << 20),
         cost_estimate=pl.CostEstimate(flops=0, bytes_accessed=0, transcendentals=0),
         name="memory",
     )(*near, *extra)
 
 
-def mixer_kernel(mine, other, after, wg, wu, wd, keep, give, mlp):
-    blocks, half, rows = mine.shape
-    cols = 2 * half
+def mixer_kernel(other, after, near_gate, near_up, near_square, gate_sets, up_sets, turned, give, hidden):
+    blocks, half, _ = other.shape
     tp = lax.axis_index("tp")
-    low = tp == 0
-    square = jnp.zeros((half, rows), F32)
-    for j in range(blocks):
-        mlp[pl.ds(pl.multiple_of(j * cols + tp * half, half), half), :] = mine[j]
-        mlp[pl.ds(pl.multiple_of(j * cols + (1 - tp) * half, half), half), :] = other[j]
-    for j in range(blocks):
-        here, there = mine[j].astype(F32), other[j].astype(F32)
-        square = square + (here * here + there * there)
-    inverse = lax.rsqrt(jnp.sum(square, axis=0, keepdims=True) / (blocks * cols) + EPSILON)
-    gate = jnp.dot(wg[...], mlp[...], preferred_element_type=F32) * inverse
-    up = jnp.dot(wu[...], mlp[...], preferred_element_type=F32) * inverse
-    hidden = (jax.nn.silu(gate) * up).T.astype(BF16)
-    for j in range(blocks):
-        part = jnp.dot(hidden, wd[:, j * cols : (j + 1) * cols], preferred_element_type=F32).T
-        first, second = part[:half].astype(BF16), part[half:].astype(BF16)
-        keep[j] = jnp.where(low, first, second)
-        give[j] = jnp.where(low, second, first)
-
-
-def mixer(mine, other, after, gate_rows, up_rows, w_down):
-    blocks, half, rows = mine.shape
-    result = jax.ShapeDtypeStruct((blocks, half, rows), BF16)
+    gate, up, square = partial_sums(other, gate_sets, up_sets, 1 - tp)
+    square = jnp.sum(square + near_square[...], axis=0, keepdims=True)
+    inverse = lax.rsqrt(square / (2 * blocks * half) + EPSILON)
+    gate = (gate + near_gate[...]) * inverse
+    up = (up + near_up[...]) * inverse
+    value = (jax.nn.silu(gate) * up).astype(BF16)
+    hidden[...] = value
+    down_half(turned, value, give, 1 - tp)
+
+
+def mixer(other, after, *near):
+    blocks, half, rows = other.shape
     return pl.pallas_call(
         mixer_kernel,
-        out_shape=(result, result),
-        in_specs=[spec(VMEM)] * 2 + [spec(HBM)] + [spec(VMEM)] * 3,
+        out_shape=(
+            jax.ShapeDtypeStruct((blocks, half, rows), BF16),
+            jax.ShapeDtypeStruct(near[0].shape, BF16),
+        ),
+        in_specs=[spec(VMEM), spec(HBM)] + [spec(VMEM)] * len(near),
         out_specs=[spec(VMEM)] * 2,
-        scratch_shapes=[pltpu.VMEM((2 * blocks * half, rows), BF16)],
-        compiler_params=pltpu.CompilerParams(vmem_limit_bytes=16 << 20),
+        compiler_params=pltpu.CompilerParams(vmem_limit_bytes=8 << 20),
         name="mixer",
-    )(mine, other, *stay(after), gate_rows, up_rows, w_down)
+    )(other, *stay(after), *near)
 
 
 def halves(turned):
@@ -383,20 +425,27 @@
         return lax.optimization_barrier((forget, key, value_heads, value))[:3]
 
     units = memory.shape[0] * memory.shape[1]
-    share = units // 3
-    early = units // 4
+    early, share = 3 * units // 16, 11 * units // 32
     wg, wu = w_gate.T, w_up.T
     keep, give = branch_step(exchanged(heads), w_out, wg, wu, w_down)
-    part, new_normalizer, new_stabilizer = memory_step(
-        memory, *behind(give), 0, early, small=(new_normalizer, new_stabilizer)
+    sets = (2, wg.shape[0], wg.shape[1] // 2)
+    part, new_normalizer, new_stabilizer, gate_sets, up_sets = memory_step(
+        memory, *behind(give), 0, early, split_job, (mlp_gain[None], wg, wu),
+        ((sets, BF16), (sets, BF16)), small=(new_normalizer, new_stabilizer),
     )
     spread, own = residual_step(tokens, keep, other_core(give), part, devices)
     mine = exchanged(spread)
-    part, wg, wu = memory_step(
-        memory, *behind(mine), early, share, part, gain=mlp_gain[None], weights=(wg, wu)
-    )
-    keep, give = mixer(mine, other_core(mine), part, wg, wu, w_down)
-    (new_memory,) = memory_step(memory, *behind(give), early + share, units - early - share, part)
+    hidden_shape = (wg.shape[0], rows)
+    part, turned, *near = memory_step(
+        memory, *behind(mine), early, share, near_job, (w_down, mine, gate_sets, up_sets),
+        (((devices, block_cols, w_down.shape[0]), BF16), (hidden_shape, F32), (hidden_shape, F32), (own.shape, F32)),
+        part,
+    )
+    give, hidden = mixer(other_core(mine), part, *near, gate_sets, up_sets, turned)
+    new_memory, keep = memory_step(
+        memory, *behind(give), early + share, units - early - share, keep_job, (turned, hidden),
+        ((give.shape, BF16),), part,
+    )
     pair = pair_step(keep, other_core(give), new_memory)
     mixed_out = finish(exchanged(pair), own).T
     return (mixed_out, new_memory, new_normalizer, new_stabilizer.T)

time: 69.2 us -> 68.9 us (level)
  no operation moved by 1% of the time
where the time goes in v7:
time: 68.9 us; the launch traced here: 68.4 us
  blocking collectives  54.8 us (80%)
  Pallas kernels  8.67 us (13%)
  starting transfers between devices  3.97 us (6%)
  between operations  0.86 us (1%)
    all_to_all x4, blocking collectives, exchanged(): return lax.all_to_all(blocks, 'kv', 0, 0, tiled=True)  54.8 us
    pallas_call x3, Pallas kernels, memory_step(): pl.pallas_call(kernel, out_shape=outs, in_specs=[spec(VMEM)] * len(near)...  4.45 us
    ppermute x3, starting transfers between devices, other_core(): return lax.ppermute(value, 'tp', [(0, 1), (1, 0)])  3.97 us
    pallas_call x1, Pallas kernels, project(): pl.pallas_call(project_kernel, out_shape=jax.ShapeDtypeStruct((blocks, ro...  1.77 us
  transfers between devices with their start and end apart: 3, of which 0 were waited for; matrix products, arithmetic and copies ran while one was open for 0% of the time, Pallas kernels for 6%

profile of v7, /device:TPU:1, one launch (start us, length us, event | category | flops | bytes accessed | tf_op | source)
XLA Modules:
  0.0 68.4 jit_solution(3428389461786235949)
XLA Ops:
  0.7 1.8 %project.1 = bf16[16,8,3200]{2,1,0:T(8,128)(2,1)S(1)} custom-call(bf16[128,128]{1,0:T(8,128)(2,1)} %tokens.3, f32[1,128]{1,0:T(1,128)} %bitcast.19, bf16[128,512]{1,0:T(8,128)(2,1)} %wq.1, bf16[128,512]{1,0:T(8,128)(2,1)} %wk.1, bf16[128,1024]{1,0:T(8,128)(2,1)} %wv.1, bf16[128,1024]{1,0:T(8,128)(2,1)} %wo.1, bf16[16,2048]{1,0:T(8,128)(2,1)} %bitcast.17), custom_call_target="tpu_custom_call" | custom-call | flops 10000000000 | bytes 10000000 | tf_op jit(solution)/shard_map/project/pallas_call | solution.py:70
  2.5 0.0 copy-start.1
  2.5 0.0 copy-start.2
  2.5 0.0 copy-start.3
  2.5 0.0 copy-start.4
  2.5 22.4 %all_to_all.20.refs_0_ = bf16[16,8,3200]{2,1,0:T(8,128)(2,1)S(1)} all-to-all(bf16[16,8,3200]{2,1,0:T(8,128)(2,1)S(1)} %project.1), channel_id=1, replica_groups=mesh['dp'=4,'kv'=16,'tp'=2] {'kv'}, dimensions={0} | all-to-all | bytes 1638400 | tf_op jit(solution)/shard_map/all_to_all | solution.py:389
  24.9 0.6 state.1
  25.6 10.7 %all_to_all.21.heads = bf16[16,8,1024]{2,1,0:T(8,128)(2,1)S(1)} all-to-all(bf16[16,8,1024]{2,1,0:T(8,128)(2,1)S(1)} %get-tuple-element.40), channel_id=1, replica_groups=mesh['dp'=4,'kv'=16,'tp'=2] {'kv'}, dimensions={0} | all-to-all | bytes 524288 | tf_op jit(solution)/shard_map/all_to_all | solution.py:389
  36.3 0.0 copy-start.5
  36.3 0.3 branch.1
  36.6 2.7 %collective-permute-start = (bf16[64,128]{1,0:T(8,128)(2,1)S(1)}, bf16[64,128]{1,0:T(8,128)(2,1)S(1)}, u32[]{:S(2)}, u32[]{:S(2)}) collective-permute-start(bf16[64,128]{1,0:T(8,128)(2,1)S(1)} %get-tuple-element.42), channel_id=1, source_target_pairs={{0,1},{1,0},{2,3},{3,2},{4,5},{5,4},{6,7},{7,6},{8,9},{9,8},{10,11... | collective-permute-start | bytes 49160 | tf_op jit(solution)/shard_map/ppermute | solution.py:385
  39.3 1.2 %memory.3 = (f32[8,4,128,256]{3,2,1,0:T(8,128)}, f32[8,4,128]{2,1,0:T(4,128)}, f32[4,8]{1,0:T(4,128)}, bf16[2,176,1024]{2,1,0:T(8,128)(2,1)S(1)}, bf16[2,176,1024]{2,1,0:T(8,128)(2,1)S(1)}) custom-call(f32[8,4,128,256]{3,2,1,0:T(8,128)S(1)} %copy-done, f32[8,4,128]{2,1,0:T(4,128)S(1)} %get-tuple-element.61.refs_1_, ...), custom_call_target="tpu_custom_call" | custom-call | tf_op jit(solution)/shard_map/memory/pallas_call | solution.py:263
  40.5 0.0 collective-permute-done.got
  40.5 0.1 residual.1
  40.7 11.1 %all_to_all.22.refs_5_ = bf16[16,64,128]{2,1,0:T(8,128)(2,1)S(1)} all-to-all(bf16[16,64,128]{2,1,0:T(8,128)(2,1)S(1)} %get-tuple-element.49), channel_id=1, replica_groups=mesh['dp'=4,'kv'=16,'tp'=2] {'kv'}, dimensions={0} | all-to-all | bytes 524288 | tf_op jit(solution)/shard_map/all_to_all | solution.py:389
  51.8 1.2 %collective-permute-start.1 = (bf16[16,64,128]{2,1,0:T(8,128)(2,1)S(1)}, bf16[16,64,128]{2,1,0:T(8,128)(2,1)S(1)}, u32[]{:S(2)}, u32[]{:S(2)}) collective-permute-start(bf16[16,64,128]{2,1,0:T(8,128)(2,1)S(1)} %all_to_all.22.refs_5_), channel_id=1, source_target_pairs={{0,1},{1,0},{2,3},{3,2},{4,5},{5,4},{6,7},{7,6},{8,9},{9,8},{10,11... | collective-permute-start | bytes 786440 | tf_op jit(solution)/shard_map/ppermute | solution.py:385
  52.9 1.6 %memory.4 = (f32[8,4,128,256]{3,2,1,0:T(8,128)}, bf16[16,128,176]{2,1,0:T(8,128)(2,1)S(1)}, f32[176,128]{1,0:T(8,128)S(1)}, f32[176,128]{1,0:T(8,128)S(1)}, f32[64,128]{1,0:T(8,128)S(1)}) custom-call(f32[8,4,128,256]{3,2,1,0:T(8,128)S(1)} %copy-done, f32[8,4,128]{2,1,0:T(4,128)S(1)} %get-tuple-element.61.refs_1_, ...), custom_call_target="tpu_custom_call", output_to_operand_aliasing={{0}: (8, {})} | custom-call | tf_op jit(solution)/shard_map/memory/pallas_call | solution.py:263
  54.5 0.0 collective-permute-done.1.other
  54.5 0.7 %mixer.1 = (bf16[16,64,128]{2,1,0:T(8,128)(2,1)S(1)}, bf16[176,128]{1,0:T(8,128)(2,1)S(1)}) custom-call(bf16[16,64,128]{2,1,0:T(8,128)(2,1)S(1)} %collective-permute-done.1.other, f32[8,4,128,256]{3,2,1,0:T(8,128)} %get-tuple-element.55.after.refs_6_, f32[176,128]{1,0:T(8,128)S(1)} %get-tuple-element.56.near_gate, f32[176,128]{1,0:T(8,128)S(1)} %get-tuple-element.57.near_up, ...), custom_call_target="tpu_custom_call" | custom-call | tf_op jit(solution)/shard_map/mixer/pallas_call | solution.py:294
  55.2 0.1 collective-permute-start.2
  55.3 1.7 %memory.5 = (f32[8,4,128,256]{3,2,1,0:T(8,128)}, bf16[16,64,128]{2,1,0:T(8,128)(2,1)S(1)}) custom-call(f32[8,4,128,256]{3,2,1,0:T(8,128)S(1)} %copy-done, f32[8,4,128]{2,1,0:T(4,128)S(1)} %get-tuple-element.61.refs_1_, f32[8,4,128]{2,1,0:T(4,128)S(1)} %get-tuple-element.62.refs_2_, ...), custom_call_target="tpu_custom_call", output_to_operand_aliasing={{0}: (6, {})} | custom-call | tf_op jit(solution)/shard_map/memory/pallas_call | solution.py:263
  57.0 0.1 pair.1
  57.1 10.6 %all_to_all.23.recv = bf16[16,64,128]{2,1,0:T(8,128)(2,1)S(1)} all-to-all(bf16[16,64,128]{2,1,0:T(8,128)(2,1)S(1)} %pair.1), channel_id=1, replica_groups=mesh['dp'=4,'kv'=16,'tp'=2] {'kv'}, dimensions={0} | all-to-all | bytes 524288 | tf_op jit(solution)/shard_map/all_to_all | solution.py:389
  67.7 0.6 finish.1
  (18 shorter events, 0.0 us)
Async XLA Ops:
  0.6 24.3 %copy-start = (f32[8,4,128,256]{3,2,1,0:T(8,128)S(1)}, f32[8,4,128,256]{3,2,1,0:T(8,128)}, u32[]{:S(2)}) copy-start(f32[8,4,128,256]{3,2,1,0:T(8,128)} %refs_0_.5) | copy-start | bytes 12582916
  0.6 24.3 %copy-start.6 = (f32[8,4,128]{2,1,0:T(4,128)S(1)}, f32[8,4,128]{2,1,0:T(4,128)}, u32[]{:S(2)}) copy-start(f32[8,4,128]{2,1,0:T(4,128)} %refs_3_.1) | copy-start | bytes 49156
  0.7 24.3 %copy-start.8 = (f32[4,256]{1,0:T(4,128)S(1)}, f32[4,256]{1,0:T(4,128)}, u32[]{:S(2)}) copy-start(f32[4,256]{1,0:T(4,128)} %refs_5_.1) | copy-start | bytes 12292
  0.7 24.3 %copy-start.9 = (f32[8,4]{0,1:T(4,128)S(1)}, f32[8,4]{0,1:T(4,128)}, u32[]{:S(2)}) copy-start(f32[8,4]{0,1:T(4,128)} %param.27) | copy-start | bytes 388
  0.7 24.3 %copy-start.10 = (f32[4]{0:T(128)S(1)}, f32[4]{0:T(128)}, u32[]{:S(2)}) copy-start(f32[4]{0:T(128)} %param.24) | copy-start | bytes 52
  2.5 33.8 %copy-start.1 = (bf16[2048,176]{0,1:T(8,128)(2,1)S(1)}, bf16[2048,176]{0,1:T(8,128)(2,1)}, u32[]{:S(2)}) copy-start(bf16[2048,176]{0,1:T(8,128)(2,1)} %param.31) | copy-start | bytes 2162692
  2.5 33.8 %copy-start.2 = (bf16[2048,176]{0,1:T(8,128)(2,1)S(1)}, bf16[2048,176]{0,1:T(8,128)(2,1)}, u32[]{:S(2)}) copy-start(bf16[2048,176]{0,1:T(8,128)(2,1)} %param.32) | copy-start | bytes 2162692
  2.5 33.8 %copy-start.3 = (bf16[176,2048]{1,0:T(8,128)(2,1)S(1)}, bf16[176,2048]{1,0:T(8,128)(2,1)}, u32[]{:S(2)}) copy-start(bf16[176,2048]{1,0:T(8,128)(2,1)} %refs_4_.1) | copy-start | bytes 2162692
  2.5 33.8 %copy-start.4 = (bf16[1024,128]{1,0:T(8,128)(2,1)S(1)}, bf16[1024,128]{1,0:T(8,128)(2,1)}, u32[]{:S(2)}) copy-start(bf16[1024,128]{1,0:T(8,128)(2,1)} %w_out.1) | copy-start | bytes 786436
  24.9 14.4 %copy-start.7 = (f32[2048]{0:T(1024)S(1)}, f32[2048]{0:T(1024)}, u32[]{:S(2)}) copy-start(f32[2048]{0:T(1024)} %param.30) | copy-start | bytes 24580
  36.3 4.2 %copy-start.5 = (bf16[128,128]{1,0:T(8,128)(2,1)S(1)}, bf16[128,128]{1,0:T(8,128)(2,1)}, u32[]{:S(2)}) copy-start(bf16[128,128]{1,0:T(8,128)(2,1)} %tokens.3) | copy-start | bytes 98308
  36.6 3.9 %collective-permute-start = (bf16[64,128]{1,0:T(8,128)(2,1)S(1)}, bf16[64,128]{1,0:T(8,128)(2,1)S(1)}, u32[]{:S(2)}, u32[]{:S(2)}) collective-permute-start(bf16[64,128]{1,0:T(8,128)(2,1)S(1)} %get-tuple-element.42), channel_id=1, source_target_pairs={{0,1},{1,0},{2,3},{3,2},{4,5},{5,4},{6,7},{7,6},{8,9},{9,8},{10,11... | collective-permute-start | bytes 49160 | tf_op jit(solution)/shard_map/ppermute | solution.py:385
  51.8 2.7 %collective-permute-start.1 = (bf16[16,64,128]{2,1,0:T(8,128)(2,1)S(1)}, bf16[16,64,128]{2,1,0:T(8,128)(2,1)S(1)}, u32[]{:S(2)}, u32[]{:S(2)}) collective-permute-start(bf16[16,64,128]{2,1,0:T(8,128)(2,1)S(1)} %all_to_all.22.refs_5_), channel_id=1, source_target_pairs={{0,1},{1,0},{2,3},{3,2},{4,5},{5,4},{6,7},{7,6},{8,9},{9,8},{10,11... | collective-permute-start | bytes 786440 | tf_op jit(solution)/shard_map/ppermute | solution.py:385
  55.2 1.8 %collective-permute-start.2 = (bf16[16,64,128]{2,1,0:T(8,128)(2,1)S(1)}, bf16[16,64,128]{2,1,0:T(8,128)(2,1)S(1)}, u32[]{:S(2)}, u32[]{:S(2)}) collective-permute-start(bf16[16,64,128]{2,1,0:T(8,128)(2,1)S(1)} %get-tuple-element.60), channel_id=1, source_target_pairs={{0,1},{1,0},{2,3},{3,2},{4,5},{5,4},{6,7},{7,6},{8,9},{9,8},{10,11... | collective-permute-start | bytes 786440 | tf_op jit(solution)/shard_map/ppermute | solution.py:385

commit v8 on v7

--- a/solution.py
+++ b/solution.py
@@ -425,7 +425,7 @@
         return lax.optimization_barrier((forget, key, value_heads, value))[:3]
 
     units = memory.shape[0] * memory.shape[1]
-    early, share = 3 * units // 16, 11 * units // 32
+    early, share = 7 * units // 32, 11 * units // 32
     wg, wu = w_gate.T, w_up.T
     keep, give = branch_step(exchanged(heads), w_out, wg, wu, w_down)
     sets = (2, wg.shape[0], wg.shape[1] // 2)

time: 68.9 us -> 68.9 us (level)
  transfers between devices with their start and end apart: 3 -> 3, of which waited for: 0 -> 0; matrix products, arithmetic and copies ran while one was open for 0% -> 0% of each run, Pallas kernels for 6% -> 7%
where the time goes in v8:
time: 68.9 us; the launch traced here: 68.4 us
  blocking collectives  54.8 us (80%)
  Pallas kernels  8.74 us (13%)
  starting transfers between devices  3.97 us (6%)
  between operations  0.85 us (1%)
    all_to_all x4, blocking collectives, exchanged(): return lax.all_to_all(blocks, 'kv', 0, 0, tiled=True)  54.8 us
    pallas_call x3, Pallas kernels, memory_step(): pl.pallas_call(kernel, out_shape=outs, in_specs=[spec(VMEM)] * len(near)...  4.51 us
    ppermute x3, starting transfers between devices, other_core(): return lax.ppermute(value, 'tp', [(0, 1), (1, 0)])  3.97 us
    pallas_call x1, Pallas kernels, project(): pl.pallas_call(project_kernel, out_shape=jax.ShapeDtypeStruct((blocks, ro...  1.77 us
  transfers between devices with their start and end apart: 3, of which 0 were waited for; matrix products, arithmetic and copies ran while one was open for 0% of the time, Pallas kernels for 7%

profile of v8, /device:TPU:1, one launch (start us, length us, event | category | flops | bytes accessed | tf_op | source)
XLA Modules:
  0.0 68.4 jit_solution(457072574788303383)
XLA Ops:
  0.7 1.8 %project.1 = bf16[16,8,3200]{2,1,0:T(8,128)(2,1)S(1)} custom-call(bf16[128,128]{1,0:T(8,128)(2,1)} %tokens.3, f32[1,128]{1,0:T(1,128)} %bitcast.19, bf16[128,512]{1,0:T(8,128)(2,1)} %wq.1, bf16[128,512]{1,0:T(8,128)(2,1)} %wk.1, bf16[128,1024]{1,0:T(8,128)(2,1)} %wv.1, bf16[128,1024]{1,0:T(8,128)(2,1)} %wo.1, bf16[16,2048]{1,0:T(8,128)(2,1)} %bitcast.17), custom_call_target="tpu_custom_call" | custom-call | flops 10000000000 | bytes 10000000 | tf_op jit(solution)/shard_map/project/pallas_call | solution.py:70
  2.5 0.0 copy-start.1
  2.5 0.0 copy-start.2
  2.5 0.0 copy-start.3
  2.5 0.0 copy-start.4
  2.5 22.4 %all_to_all.20.refs_0_ = bf16[16,8,3200]{2,1,0:T(8,128)(2,1)S(1)} all-to-all(bf16[16,8,3200]{2,1,0:T(8,128)(2,1)S(1)} %project.1), channel_id=1, replica_groups=mesh['dp'=4,'kv'=16,'tp'=2] {'kv'}, dimensions={0} | all-to-all | bytes 1638400 | tf_op jit(solution)/shard_map/all_to_all | solution.py:389
  24.9 0.6 state.1
  25.6 10.7 %all_to_all.21.heads = bf16[16,8,1024]{2,1,0:T(8,128)(2,1)S(1)} all-to-all(bf16[16,8,1024]{2,1,0:T(8,128)(2,1)S(1)} %get-tuple-element.40), channel_id=1, replica_groups=mesh['dp'=4,'kv'=16,'tp'=2] {'kv'}, dimensions={0} | all-to-all | bytes 524288 | tf_op jit(solution)/shard_map/all_to_all | solution.py:389
  36.3 0.0 copy-start.5
  36.3 0.3 branch.1
  36.6 2.7 %collective-permute-start = (bf16[64,128]{1,0:T(8,128)(2,1)S(1)}, bf16[64,128]{1,0:T(8,128)(2,1)S(1)}, u32[]{:S(2)}, u32[]{:S(2)}) collective-permute-start(bf16[64,128]{1,0:T(8,128)(2,1)S(1)} %get-tuple-element.42), channel_id=1, source_target_pairs={{0,1},{1,0},{2,3},{3,2},{4,5},{5,4},{6,7},{7,6},{8,9},{9,8},{10,11... | collective-permute-start | bytes 49160 | tf_op jit(solution)/shard_map/ppermute | solution.py:385
  39.3 1.3 %memory.3 = (f32[8,4,128,256]{3,2,1,0:T(8,128)}, f32[8,4,128]{2,1,0:T(4,128)}, f32[4,8]{1,0:T(4,128)}, bf16[2,176,1024]{2,1,0:T(8,128)(2,1)S(1)}, bf16[2,176,1024]{2,1,0:T(8,128)(2,1)S(1)}) custom-call(f32[8,4,128,256]{3,2,1,0:T(8,128)S(1)} %copy-done, f32[8,4,128]{2,1,0:T(4,128)S(1)} %get-tuple-element.61.refs_1_, ...), custom_call_target="tpu_custom_call" | custom-call | tf_op jit(solution)/shard_map/memory/pallas_call | solution.py:263
  40.6 0.0 collective-permute-done.got
  40.6 0.1 residual.1
  40.8 11.1 %all_to_all.22.refs_5_ = bf16[16,64,128]{2,1,0:T(8,128)(2,1)S(1)} all-to-all(bf16[16,64,128]{2,1,0:T(8,128)(2,1)S(1)} %get-tuple-element.49), channel_id=1, replica_groups=mesh['dp'=4,'kv'=16,'tp'=2] {'kv'}, dimensions={0} | all-to-all | bytes 524288 | tf_op jit(solution)/shard_map/all_to_all | solution.py:389
  51.9 1.2 %collective-permute-start.1 = (bf16[16,64,128]{2,1,0:T(8,128)(2,1)S(1)}, bf16[16,64,128]{2,1,0:T(8,128)(2,1)S(1)}, u32[]{:S(2)}, u32[]{:S(2)}) collective-permute-start(bf16[16,64,128]{2,1,0:T(8,128)(2,1)S(1)} %all_to_all.22.refs_5_), channel_id=1, source_target_pairs={{0,1},{1,0},{2,3},{3,2},{4,5},{5,4},{6,7},{7,6},{8,9},{9,8},{10,11... | collective-permute-start | bytes 786440 | tf_op jit(solution)/shard_map/ppermute | solution.py:385
  53.0 1.6 %memory.4 = (f32[8,4,128,256]{3,2,1,0:T(8,128)}, bf16[16,128,176]{2,1,0:T(8,128)(2,1)S(1)}, f32[176,128]{1,0:T(8,128)S(1)}, f32[176,128]{1,0:T(8,128)S(1)}, f32[64,128]{1,0:T(8,128)S(1)}) custom-call(f32[8,4,128,256]{3,2,1,0:T(8,128)S(1)} %copy-done, f32[8,4,128]{2,1,0:T(4,128)S(1)} %get-tuple-element.61.refs_1_, ...), custom_call_target="tpu_custom_call", output_to_operand_aliasing={{0}: (8, {})} | custom-call | tf_op jit(solution)/shard_map/memory/pallas_call | solution.py:263
  54.6 0.7 %mixer.1 = (bf16[16,64,128]{2,1,0:T(8,128)(2,1)S(1)}, bf16[176,128]{1,0:T(8,128)(2,1)S(1)}) custom-call(bf16[16,64,128]{2,1,0:T(8,128)(2,1)S(1)} %collective-permute-done.1.other, f32[8,4,128,256]{3,2,1,0:T(8,128)} %get-tuple-element.55.after.refs_6_, f32[176,128]{1,0:T(8,128)S(1)} %get-tuple-element.56.near_gate, f32[176,128]{1,0:T(8,128)S(1)} %get-tuple-element.57.near_up, ...), custom_call_target="tpu_custom_call" | custom-call | tf_op jit(solution)/shard_map/mixer/pallas_call | solution.py:294
  55.3 0.1 collective-permute-start.2
  55.4 1.6 %memory.5 = (f32[8,4,128,256]{3,2,1,0:T(8,128)}, bf16[16,64,128]{2,1,0:T(8,128)(2,1)S(1)}) custom-call(f32[8,4,128,256]{3,2,1,0:T(8,128)S(1)} %copy-done, f32[8,4,128]{2,1,0:T(4,128)S(1)} %get-tuple-element.61.refs_1_, f32[8,4,128]{2,1,0:T(4,128)S(1)} %get-tuple-element.62.refs_2_, ...), custom_call_target="tpu_custom_call", output_to_operand_aliasing={{0}: (6, {})} | custom-call | tf_op jit(solution)/shard_map/memory/pallas_call | solution.py:263
  57.1 0.0 collective-permute-done.2.got
  57.1 0.1 pair.1
  57.1 10.6 %all_to_all.23.recv = bf16[16,64,128]{2,1,0:T(8,128)(2,1)S(1)} all-to-all(bf16[16,64,128]{2,1,0:T(8,128)(2,1)S(1)} %pair.1), channel_id=1, replica_groups=mesh['dp'=4,'kv'=16,'tp'=2] {'kv'}, dimensions={0} | all-to-all | bytes 524288 | tf_op jit(solution)/shard_map/all_to_all | solution.py:389
  67.8 0.6 finish.1
  (18 shorter events, 0.0 us)
Async XLA Ops:
  0.6 24.3 %copy-start = (f32[8,4,128,256]{3,2,1,0:T(8,128)S(1)}, f32[8,4,128,256]{3,2,1,0:T(8,128)}, u32[]{:S(2)}) copy-start(f32[8,4,128,256]{3,2,1,0:T(8,128)} %refs_0_.5) | copy-start | bytes 12582916
  0.6 24.3 %copy-start.6 = (f32[8,4,128]{2,1,0:T(4,128)S(1)}, f32[8,4,128]{2,1,0:T(4,128)}, u32[]{:S(2)}) copy-start(f32[8,4,128]{2,1,0:T(4,128)} %refs_3_.1) | copy-start | bytes 49156
  0.7 24.3 %copy-start.8 = (f32[4,256]{1,0:T(4,128)S(1)}, f32[4,256]{1,0:T(4,128)}, u32[]{:S(2)}) copy-start(f32[4,256]{1,0:T(4,128)} %refs_5_.1) | copy-start | bytes 12292
  0.7 24.3 %copy-start.9 = (f32[8,4]{0,1:T(4,128)S(1)}, f32[8,4]{0,1:T(4,128)}, u32[]{:S(2)}) copy-start(f32[8,4]{0,1:T(4,128)} %param.27) | copy-start | bytes 388
  0.7 24.3 %copy-start.10 = (f32[4]{0:T(128)S(1)}, f32[4]{0:T(128)}, u32[]{:S(2)}) copy-start(f32[4]{0:T(128)} %param.24) | copy-start | bytes 52
  2.5 33.8 %copy-start.1 = (bf16[2048,176]{0,1:T(8,128)(2,1)S(1)}, bf16[2048,176]{0,1:T(8,128)(2,1)}, u32[]{:S(2)}) copy-start(bf16[2048,176]{0,1:T(8,128)(2,1)} %param.31) | copy-start | bytes 2162692
  2.5 33.8 %copy-start.2 = (bf16[2048,176]{0,1:T(8,128)(2,1)S(1)}, bf16[2048,176]{0,1:T(8,128)(2,1)}, u32[]{:S(2)}) copy-start(bf16[2048,176]{0,1:T(8,128)(2,1)} %param.32) | copy-start | bytes 2162692
  2.5 33.8 %copy-start.3 = (bf16[176,2048]{1,0:T(8,128)(2,1)S(1)}, bf16[176,2048]{1,0:T(8,128)(2,1)}, u32[]{:S(2)}) copy-start(bf16[176,2048]{1,0:T(8,128)(2,1)} %refs_4_.1) | copy-start | bytes 2162692
  2.5 33.8 %copy-start.4 = (bf16[1024,128]{1,0:T(8,128)(2,1)S(1)}, bf16[1024,128]{1,0:T(8,128)(2,1)}, u32[]{:S(2)}) copy-start(bf16[1024,128]{1,0:T(8,128)(2,1)} %w_out.1) | copy-start | bytes 786436
  24.9 14.4 %copy-start.7 = (f32[2048]{0:T(1024)S(1)}, f32[2048]{0:T(1024)}, u32[]{:S(2)}) copy-start(f32[2048]{0:T(1024)} %param.30) | copy-start | bytes 24580
  36.3 4.3 %copy-start.5 = (bf16[128,128]{1,0:T(8,128)(2,1)S(1)}, bf16[128,128]{1,0:T(8,128)(2,1)}, u32[]{:S(2)}) copy-start(bf16[128,128]{1,0:T(8,128)(2,1)} %tokens.3) | copy-start | bytes 98308
  36.6 4.0 %collective-permute-start = (bf16[64,128]{1,0:T(8,128)(2,1)S(1)}, bf16[64,128]{1,0:T(8,128)(2,1)S(1)}, u32[]{:S(2)}, u32[]{:S(2)}) collective-permute-start(bf16[64,128]{1,0:T(8,128)(2,1)S(1)} %get-tuple-element.42), channel_id=1, source_target_pairs={{0,1},{1,0},{2,3},{3,2},{4,5},{5,4},{6,7},{7,6},{8,9},{9,8},{10,11... | collective-permute-start | bytes 49160 | tf_op jit(solution)/shard_map/ppermute | solution.py:385
  51.9 2.8 %collective-permute-start.1 = (bf16[16,64,128]{2,1,0:T(8,128)(2,1)S(1)}, bf16[16,64,128]{2,1,0:T(8,128)(2,1)S(1)}, u32[]{:S(2)}, u32[]{:S(2)}) collective-permute-start(bf16[16,64,128]{2,1,0:T(8,128)(2,1)S(1)} %all_to_all.22.refs_5_), channel_id=1, source_target_pairs={{0,1},{1,0},{2,3},{3,2},{4,5},{5,4},{6,7},{7,6},{8,9},{9,8},{10,11... | collective-permute-start | bytes 786440 | tf_op jit(solution)/shard_map/ppermute | solution.py:385
  55.3 1.7 %collective-permute-start.2 = (bf16[16,64,128]{2,1,0:T(8,128)(2,1)S(1)}, bf16[16,64,128]{2,1,0:T(8,128)(2,1)S(1)}, u32[]{:S(2)}, u32[]{:S(2)}) collective-permute-start(bf16[16,64,128]{2,1,0:T(8,128)(2,1)S(1)} %get-tuple-element.60), channel_id=1, source_target_pairs={{0,1},{1,0},{2,3},{3,2},{4,5},{5,4},{6,7},{7,6},{8,9},{9,8},{10,11... | collective-permute-start | bytes 786440 | tf_op jit(solution)/shard_map/ppermute | solution.py:385

commit v9 on v8

--- a/solution.py
+++ b/solution.py
@@ -311,7 +311,7 @@
     return jnp.where(low, first, second), jnp.where(low, second, first)
 
 
-def branch_kernel(heads, w_out, wg, wu, wd, keep, give):
+def branch_kernel(heads, w_out, keep, give):
     rows = heads[...].reshape(heads.shape[0] * heads.shape[1], w_out.shape[0])
     mine, other = halves(jnp.dot(rows, w_out[...], preferred_element_type=F32).T)
     keep[...] = mine.astype(BF16)
@@ -427,7 +427,7 @@
     units = memory.shape[0] * memory.shape[1]
     early, share = 7 * units // 32, 11 * units // 32
     wg, wu = w_gate.T, w_up.T
-    keep, give = branch_step(exchanged(heads), w_out, wg, wu, w_down)
+    keep, give = branch_step(exchanged(heads), w_out)
     sets = (2, wg.shape[0], wg.shape[1] // 2)
     part, new_normalizer, new_stabilizer, gate_sets, up_sets = memory_step(
         memory, *behind(give), 0, early, split_job, (mlp_gain[None], wg, wu),

time: 68.9 us -> 69 us (level)
  no operation moved by 1% of the time
where the time goes in v9:
time: 69 us; the launch traced here: 68.4 us
  blocking collectives  54.8 us (79%)
  Pallas kernels  8.77 us (13%)
  starting transfers between devices  3.98 us (6%)
  between operations  0.85 us (1%)
    all_to_all x4, blocking collectives, exchanged(): return lax.all_to_all(blocks, 'kv', 0, 0, tiled=True)  54.8 us
    pallas_call x3, Pallas kernels, memory_step(): pl.pallas_call(kernel, out_shape=outs, in_specs=[spec(VMEM)] * len(near)...  4.54 us
    ppermute x3, starting transfers between devices, other_core(): return lax.ppermute(value, 'tp', [(0, 1), (1, 0)])  3.98 us
    pallas_call x1, Pallas kernels, project(): pl.pallas_call(project_kernel, out_shape=jax.ShapeDtypeStruct((blocks, ro...  1.77 us
  transfers between devices with their start and end apart: 3, of which 0 were waited for; matrix products, arithmetic and copies ran while one was open for 0% of the time, Pallas kernels for 7%

profile of v9, /device:TPU:1, one launch (start us, length us, event | category | flops | bytes accessed | tf_op | source)
XLA Modules:
  0.0 68.4 jit_solution(7223728201661134718)
XLA Ops:
  0.7 1.8 %project.1 = bf16[16,8,3200]{2,1,0:T(8,128)(2,1)S(1)} custom-call(bf16[128,128]{1,0:T(8,128)(2,1)} %tokens.3, f32[1,128]{1,0:T(1,128)} %bitcast.17, bf16[128,512]{1,0:T(8,128)(2,1)} %wq.1, bf16[128,512]{1,0:T(8,128)(2,1)} %wk.1, bf16[128,1024]{1,0:T(8,128)(2,1)} %wv.1, bf16[128,1024]{1,0:T(8,128)(2,1)} %wo.1, bf16[16,2048]{1,0:T(8,128)(2,1)} %bitcast.15), custom_call_target="tpu_custom_call" | custom-call | flops 10000000000 | bytes 10000000 | tf_op jit(solution)/shard_map/project/pallas_call | solution.py:70
  2.5 0.0 copy-start.4
  2.5 0.0 copy-start.1
  2.5 0.0 copy-start.2
  2.5 0.0 copy-start.7
  2.5 22.4 %all_to_all.20.refs_0_ = bf16[16,8,3200]{2,1,0:T(8,128)(2,1)S(1)} all-to-all(bf16[16,8,3200]{2,1,0:T(8,128)(2,1)S(1)} %project.1), channel_id=1, replica_groups=mesh['dp'=4,'kv'=16,'tp'=2] {'kv'}, dimensions={0} | all-to-all | bytes 1638400 | tf_op jit(solution)/shard_map/all_to_all | solution.py:389
  24.9 0.6 state.1
  25.6 0.0 copy-start.5
  25.6 10.7 %all_to_all.21.heads = bf16[16,8,1024]{2,1,0:T(8,128)(2,1)S(1)} all-to-all(bf16[16,8,1024]{2,1,0:T(8,128)(2,1)S(1)} %get-tuple-element.40), channel_id=1, replica_groups=mesh['dp'=4,'kv'=16,'tp'=2] {'kv'}, dimensions={0} | all-to-all | bytes 524288 | tf_op jit(solution)/shard_map/all_to_all | solution.py:389
  36.3 0.3 branch.1
  36.6 2.7 %collective-permute-start = (bf16[64,128]{1,0:T(8,128)(2,1)S(1)}, bf16[64,128]{1,0:T(8,128)(2,1)S(1)}, u32[]{:S(2)}, u32[]{:S(2)}) collective-permute-start(bf16[64,128]{1,0:T(8,128)(2,1)S(1)} %get-tuple-element.42), channel_id=1, source_target_pairs={{0,1},{1,0},{2,3},{3,2},{4,5},{5,4},{6,7},{7,6},{8,9},{9,8},{10,11... | collective-permute-start | bytes 49160 | tf_op jit(solution)/shard_map/ppermute | solution.py:385
  39.3 1.3 %memory.3 = (f32[8,4,128,256]{3,2,1,0:T(8,128)}, f32[8,4,128]{2,1,0:T(4,128)}, f32[4,8]{1,0:T(4,128)}, bf16[2,176,1024]{2,1,0:T(8,128)(2,1)S(1)}, bf16[2,176,1024]{2,1,0:T(8,128)(2,1)S(1)}) custom-call(f32[8,4,128,256]{3,2,1,0:T(8,128)S(1)} %copy-done, f32[8,4,128]{2,1,0:T(4,128)S(1)} %get-tuple-element.61.refs_1_, ...), custom_call_target="tpu_custom_call" | custom-call | tf_op jit(solution)/shard_map/memory/pallas_call | solution.py:263
  40.6 0.0 collective-permute-done.got
  40.6 0.1 residual.1
  40.8 11.1 %all_to_all.22.refs_5_ = bf16[16,64,128]{2,1,0:T(8,128)(2,1)S(1)} all-to-all(bf16[16,64,128]{2,1,0:T(8,128)(2,1)S(1)} %get-tuple-element.49), channel_id=1, replica_groups=mesh['dp'=4,'kv'=16,'tp'=2] {'kv'}, dimensions={0} | all-to-all | bytes 524288 | tf_op jit(solution)/shard_map/all_to_all | solution.py:389
  51.8 1.2 %collective-permute-start.1 = (bf16[16,64,128]{2,1,0:T(8,128)(2,1)S(1)}, bf16[16,64,128]{2,1,0:T(8,128)(2,1)S(1)}, u32[]{:S(2)}, u32[]{:S(2)}) collective-permute-start(bf16[16,64,128]{2,1,0:T(8,128)(2,1)S(1)} %all_to_all.22.refs_5_), channel_id=1, source_target_pairs={{0,1},{1,0},{2,3},{3,2},{4,5},{5,4},{6,7},{7,6},{8,9},{9,8},{10,11... | collective-permute-start | bytes 786440 | tf_op jit(solution)/shard_map/ppermute | solution.py:385
  53.0 1.6 %memory.4 = (f32[8,4,128,256]{3,2,1,0:T(8,128)}, bf16[16,128,176]{2,1,0:T(8,128)(2,1)S(1)}, f32[176,128]{1,0:T(8,128)S(1)}, f32[176,128]{1,0:T(8,128)S(1)}, f32[64,128]{1,0:T(8,128)S(1)}) custom-call(f32[8,4,128,256]{3,2,1,0:T(8,128)S(1)} %copy-done, f32[8,4,128]{2,1,0:T(4,128)S(1)} %get-tuple-element.61.refs_1_, ...), custom_call_target="tpu_custom_call", output_to_operand_aliasing={{0}: (8, {})} | custom-call | tf_op jit(solution)/shard_map/memory/pallas_call | solution.py:263
  54.6 0.0 collective-permute-done.1.other
  54.6 0.7 %mixer.1 = (bf16[16,64,128]{2,1,0:T(8,128)(2,1)S(1)}, bf16[176,128]{1,0:T(8,128)(2,1)S(1)}) custom-call(bf16[16,64,128]{2,1,0:T(8,128)(2,1)S(1)} %collective-permute-done.1.other, f32[8,4,128,256]{3,2,1,0:T(8,128)} %get-tuple-element.55.after.refs_6_, f32[176,128]{1,0:T(8,128)S(1)} %get-tuple-element.56.near_gate, f32[176,128]{1,0:T(8,128)S(1)} %get-tuple-element.57.near_up, ...), custom_call_target="tpu_custom_call" | custom-call | tf_op jit(solution)/shard_map/mixer/pallas_call | solution.py:294
  55.4 0.1 collective-permute-start.2
  55.4 1.6 %memory.5 = (f32[8,4,128,256]{3,2,1,0:T(8,128)}, bf16[16,64,128]{2,1,0:T(8,128)(2,1)S(1)}) custom-call(f32[8,4,128,256]{3,2,1,0:T(8,128)S(1)} %copy-done, f32[8,4,128]{2,1,0:T(4,128)S(1)} %get-tuple-element.61.refs_1_, f32[8,4,128]{2,1,0:T(4,128)S(1)} %get-tuple-element.62.refs_2_, ...), custom_call_target="tpu_custom_call", output_to_operand_aliasing={{0}: (6, {})} | custom-call | tf_op jit(solution)/shard_map/memory/pallas_call | solution.py:263
  57.1 0.1 pair.1
  57.2 10.6 %all_to_all.23.recv = bf16[16,64,128]{2,1,0:T(8,128)(2,1)S(1)} all-to-all(bf16[16,64,128]{2,1,0:T(8,128)(2,1)S(1)} %pair.1), channel_id=1, replica_groups=mesh['dp'=4,'kv'=16,'tp'=2] {'kv'}, dimensions={0} | all-to-all | bytes 524288 | tf_op jit(solution)/shard_map/all_to_all | solution.py:389
  67.8 0.6 finish.1
  (18 shorter events, 0.0 us)
Async XLA Ops:
  0.6 24.3 %copy-start = (f32[8,4,128,256]{3,2,1,0:T(8,128)S(1)}, f32[8,4,128,256]{3,2,1,0:T(8,128)}, u32[]{:S(2)}) copy-start(f32[8,4,128,256]{3,2,1,0:T(8,128)} %refs_0_.5) | copy-start | bytes 12582916
  0.6 24.3 %copy-start.6 = (f32[8,4,128]{2,1,0:T(4,128)S(1)}, f32[8,4,128]{2,1,0:T(4,128)}, u32[]{:S(2)}) copy-start(f32[8,4,128]{2,1,0:T(4,128)} %refs_3_.1) | copy-start | bytes 49156
  0.7 24.3 %copy-start.8 = (f32[4,256]{1,0:T(4,128)S(1)}, f32[4,256]{1,0:T(4,128)}, u32[]{:S(2)}) copy-start(f32[4,256]{1,0:T(4,128)} %refs_5_.1) | copy-start | bytes 12292
  0.7 24.3 %copy-start.9 = (f32[8,4]{0,1:T(4,128)S(1)}, f32[8,4]{0,1:T(4,128)}, u32[]{:S(2)}) copy-start(f32[8,4]{0,1:T(4,128)} %param.27) | copy-start | bytes 388
  0.7 24.3 %copy-start.10 = (f32[4]{0:T(128)S(1)}, f32[4]{0:T(128)}, u32[]{:S(2)}) copy-start(f32[4]{0:T(128)} %param.24) | copy-start | bytes 52
  2.5 33.8 %copy-start.4 = (bf16[1024,128]{1,0:T(8,128)(2,1)S(1)}, bf16[1024,128]{1,0:T(8,128)(2,1)}, u32[]{:S(2)}) copy-start(bf16[1024,128]{1,0:T(8,128)(2,1)} %w_out.1) | copy-start | bytes 786436
  2.5 36.8 %copy-start.1 = (bf16[2048,176]{0,1:T(8,128)(2,1)S(1)}, bf16[2048,176]{0,1:T(8,128)(2,1)}, u32[]{:S(2)}) copy-start(bf16[2048,176]{0,1:T(8,128)(2,1)} %param.31) | copy-start | bytes 2162692
  2.5 36.8 %copy-start.2 = (bf16[2048,176]{0,1:T(8,128)(2,1)S(1)}, bf16[2048,176]{0,1:T(8,128)(2,1)}, u32[]{:S(2)}) copy-start(bf16[2048,176]{0,1:T(8,128)(2,1)} %param.32) | copy-start | bytes 2162692
  2.5 36.8 %copy-start.7 = (f32[2048]{0:T(1024)S(1)}, f32[2048]{0:T(1024)}, u32[]{:S(2)}) copy-start(f32[2048]{0:T(1024)} %param.30) | copy-start | bytes 24580
  25.6 15.0 %copy-start.5 = (bf16[128,128]{1,0:T(8,128)(2,1)S(1)}, bf16[128,128]{1,0:T(8,128)(2,1)}, u32[]{:S(2)}) copy-start(bf16[128,128]{1,0:T(8,128)(2,1)} %tokens.3) | copy-start | bytes 98308
  36.6 4.1 %collective-permute-start = (bf16[64,128]{1,0:T(8,128)(2,1)S(1)}, bf16[64,128]{1,0:T(8,128)(2,1)S(1)}, u32[]{:S(2)}, u32[]{:S(2)}) collective-permute-start(bf16[64,128]{1,0:T(8,128)(2,1)S(1)} %get-tuple-element.42), channel_id=1, source_target_pairs={{0,1},{1,0},{2,3},{3,2},{4,5},{5,4},{6,7},{7,6},{8,9},{9,8},{10,11... | collective-permute-start | bytes 49160 | tf_op jit(solution)/shard_map/ppermute | solution.py:385
  39.3 13.7 %copy-start.3 = (bf16[176,2048]{1,0:T(8,128)(2,1)S(1)}, bf16[176,2048]{1,0:T(8,128)(2,1)}, u32[]{:S(2)}) copy-start(bf16[176,2048]{1,0:T(8,128)(2,1)} %refs_4_.1) | copy-start | bytes 2162692
  51.8 2.8 %collective-permute-start.1 = (bf16[16,64,128]{2,1,0:T(8,128)(2,1)S(1)}, bf16[16,64,128]{2,1,0:T(8,128)(2,1)S(1)}, u32[]{:S(2)}, u32[]{:S(2)}) collective-permute-start(bf16[16,64,128]{2,1,0:T(8,128)(2,1)S(1)} %all_to_all.22.refs_5_), channel_id=1, source_target_pairs={{0,1},{1,0},{2,3},{3,2},{4,5},{5,4},{6,7},{7,6},{8,9},{9,8},{10,11... | collective-permute-start | bytes 786440 | tf_op jit(solution)/shard_map/ppermute | solution.py:385
  55.4 1.7 %collective-permute-start.2 = (bf16[16,64,128]{2,1,0:T(8,128)(2,1)S(1)}, bf16[16,64,128]{2,1,0:T(8,128)(2,1)S(1)}, u32[]{:S(2)}, u32[]{:S(2)}) collective-permute-start(bf16[16,64,128]{2,1,0:T(8,128)(2,1)S(1)} %get-tuple-element.60), channel_id=1, source_target_pairs={{0,1},{1,0},{2,3},{3,2},{4,5},{5,4},{6,7},{7,6},{8,9},{9,8},{10,11... | collective-permute-start | bytes 786440 | tf_op jit(solution)/shard_map/ppermute | solution.py:385
